TPU v7x, 256 devices: a whole 4x4x8 slice. The times are simulated.
256 devices in a mesh: sp: 64 (over z, x, core), tp: 4 (over y).
Axes of the slice: x: 4, y: 4, z: 8, core: 2. Of those that a mesh axis runs over, the one named last changes fastest.
Arguments:
- mixer_input: bfloat16 [8192, 512], P('sp', 'tp'), may hold values from -8 to 8
- step_shift: float32 [8192, 32], P('sp', 'tp')
- log_step: float32 [32], P('tp'), may hold values from -12 to -1
- decay_real: float32 [32, 64], P('tp'), may hold values from -0.7 to -0.35
- freq_imag: float32 [32, 64], P('tp'), may hold values from 0 to 201.0624
- in_real: float32 [32, 64, 16], P('tp'), may hold values from -1 to 1
- in_imag: float32 [32, 64, 16], P('tp'), may hold values from -1 to 1
- out_real: float32 [32, 16, 64], P('tp'), may hold values from -0.75 to 0.75
- out_imag: float32 [32, 16, 64], P('tp'), may hold values from -0.75 to 0.75
- skip_gain: float32 [512], P('tp'), may hold values from -4 to 4
- out_weight: bfloat16 [512, 2048], P('tp'), may hold values from -0.25 to 0.25
- residual: bfloat16 [8192, 2048], P(('sp', 'tp')), may hold values from -6 to 6
- post_gain: float32 [2048], replicated, may hold values from 0.1 to 1.9
- pre_gain: float32 [2048], replicated, may hold values from 0.1 to 1.9
- final_gain: float32 [2048], replicated, may hold values from 0.1 to 1.9
- route_ids: int32 [8192, 2], P('sp'), may hold values from 0 to 63, all different within a row; in each aligned block of 32 rows (0 to 31, 32 to 63, ...) at most 2 rows name the same one
- route_logits: float32 [8192, 2], P('sp'), may hold values from -8 to 8
- expert_gate: bfloat16 [64, 2048, 3584], P('sp', None, 'tp'), may hold values from -0.125 to 0.125
- expert_up: bfloat16 [64, 2048, 3584], P('sp', None, 'tp'), may hold values from -0.125 to 0.125
- expert_down: bfloat16 [64, 3584, 2048], P('sp', 'tp'), may hold values from -0.09375 to 0.09375
Outputs:
- layer_out: bfloat16 [8192, 2048], P(('sp', 'tp'))
Inputs may be any that keep to these rules, and one draw needn't show every extreme that they name: `route_ids`: each row names 2 different experts; in the 32 rows of one device no expert is named more than 2 times, a bound that some block reaches in some devices' rows.
All inputs are finite; a program needn't handle non-finite values.
Results may differ from a plain program's by a relative error of at most 0.0095.
Values may be sent and summed in bfloat16 or wider, within the bound.
No kernel may reach another device: no remote copies, remote signals or barrier semaphores. Data moves between devices by JAX's collectives and lax.ppermute only.
A program may use at most 64 MiB of HBM per device.

v0:
```python
import functools

import jax
import jax.numpy as jnp
from jax import lax
from jax.sharding import PartitionSpec as P


def copy_for_each(shard, axis):
    copies = jnp.broadcast_to(shard, (lax.axis_size(axis), *shard.shape))
    return lax.all_to_all(copies, axis, split_axis=0, concat_axis=0, tiled=True)


def combined_pairwise(pieces, combine):
    while len(jax.tree.leaves(pieces)[0]) > 1:
        pieces = jax.vmap(combine)(
            *(jax.tree.map(lambda part: part[side::2], pieces) for side in (0, 1))
        )
    return jax.tree.map(lambda part: part[0], pieces)


def prefix_2(shard, axis, combine, identity):
    devices, mine = (lax.axis_size(axis), lax.axis_index(axis))
    passed = jnp.arange(devices) < mine

    def kept(part, zero, own):
        part = jnp.where(
            passed.reshape(-1, *(1 for _ in own.shape)), part, jnp.asarray(zero, own.dtype)
        )
        return part

    pieces = jax.tree.map(lambda part: copy_for_each(part, axis), shard)
    return combined_pairwise(jax.tree.map(kept, pieces, identity, shard), combine)


def in_blocks(shard, dim, devices):
    before, after = (shard.shape[:dim], shard.shape[dim + 1 :])
    return jnp.moveaxis(shard.reshape(*before, devices, -1, *after), dim, 0)


def sum_at_owner(shard, axis, dim):
    devices = lax.axis_size(axis)
    blocks = lax.all_to_all(in_blocks(shard, dim, devices), axis, 0, 0, tiled=True)
    return jnp.sum(blocks.astype(jnp.float32), axis=0)


def in_order(blocks, dim):
    lengths = list(blocks.shape[1:])
    lengths[dim] *= blocks.shape[0]
    return jnp.moveaxis(blocks, 0, dim).reshape(lengths)


def gather_directly(shard, axis, dim):
    return in_order(copy_for_each(shard, axis), dim)


def combine(first_pair, second_pair):
    one_rot_real, one_rot_imag, one_state_real, one_state_imag = first_pair
    two_rot_real, two_rot_imag, two_state_real, two_state_imag = second_pair
    return (
        two_rot_real * one_rot_real - two_rot_imag * one_rot_imag,
        two_rot_real * one_rot_imag + two_rot_imag * one_rot_real,
        two_rot_real * one_state_real - two_rot_imag * one_state_imag + two_state_real,
        two_rot_real * one_state_imag + two_rot_imag * one_state_real + two_state_imag,
    )


def scaled(values, gain_vec):
    return values * lax.rsqrt(jnp.mean(values * values, axis=-1, keepdims=True) + 1e-06) * gain_vec


def blocked_prefix(flat_parts):
    length, columns = flat_parts[0].shape
    span = 16
    blocked = tuple((part.reshape(length // span, span, columns) for part in flat_parts))
    start = (
        jnp.ones((columns,), jnp.float32),
        jnp.zeros((columns,), jnp.float32),
        jnp.zeros((columns,), jnp.float32),
        jnp.zeros((columns,), jnp.float32),
    )

    def block_step(carry, block):
        outputs = []
        for inner in range(span):
            carry = combine(carry, tuple((member[inner] for member in block)))
            outputs.append(carry)
        stacked = tuple(
            (jnp.stack([entry[which] for entry in outputs], axis=0) for which in range(4))
        )
        return (carry, stacked)

    final_carry, prefix = lax.scan(block_step, start, blocked)
    return tuple((member.reshape(length, columns) for member in prefix))


def mixer_block(
    mixer_input,
    step_shift,
    log_step,
    decay_real,
    freq_imag,
    in_real,
    in_imag,
    out_real,
    out_imag,
    skip_gain,
):
    inputs = mixer_input.astype(jnp.float32)
    length, groups = step_shift.shape
    channels = in_real.shape[2]
    states = in_real.shape[1]
    step_size = jnp.exp(log_step[None, :] + step_shift)[:, :, None]
    magnitude = jnp.exp(decay_real[None] * step_size)
    rot_angle = freq_imag[None] * step_size
    rot_real = magnitude * jnp.cos(rot_angle)
    rot_imag = magnitude * jnp.sin(rot_angle)
    denominator = decay_real * decay_real + freq_imag * freq_imag
    minus_one = rot_real - 1.0
    coef_real = (minus_one * decay_real + rot_imag * freq_imag) / denominator
    coef_imag = (rot_imag * decay_real - minus_one * freq_imag) / denominator
    grouped = inputs.reshape(length, groups, channels)
    into_real = jnp.einsum("tgc,gnc->tgn", grouped, in_real, precision=lax.Precision.HIGHEST)
    into_imag = jnp.einsum("tgc,gnc->tgn", grouped, in_imag, precision=lax.Precision.HIGHEST)
    drive_real = coef_real * into_real - coef_imag * into_imag
    drive_imag = coef_real * into_imag + coef_imag * into_real
    flat_parts = tuple(
        (
            part.reshape(length, groups * states)
            for part in (rot_real, rot_imag, drive_real, drive_imag)
        )
    )
    cum_real, cum_imag, local_real, local_imag = blocked_prefix(flat_parts)
    summary = (cum_real[-1], cum_imag[-1], local_real[-1], local_imag[-1])
    identity = (
        jnp.ones_like(summary[0]),
        jnp.zeros_like(summary[1]),
        jnp.zeros_like(summary[2]),
        jnp.zeros_like(summary[3]),
    )
    carried = prefix_2(summary, "sp", combine, identity)
    carry_real = carried[2][None]
    carry_imag = carried[3][None]
    state_real = local_real + cum_real * carry_real - cum_imag * carry_imag
    state_imag = local_imag + cum_real * carry_imag + cum_imag * carry_real
    readout = jnp.einsum(
        "tgn,gcn->tgc",
        state_real.reshape(length, groups, states),
        out_real,
        precision=lax.Precision.HIGHEST,
    ) - jnp.einsum(
        "tgn,gcn->tgc",
        state_imag.reshape(length, groups, states),
        out_imag,
        precision=lax.Precision.HIGHEST,
    )
    result = readout.reshape(length, groups * channels) + skip_gain[None, :] * inputs
    return jax.nn.gelu(result).astype(jnp.bfloat16)


def slot_table(capacity, experts, block_ids):
    flat_ids = block_ids.reshape(-1)
    assigned = flat_ids.shape[0]
    onehot = (flat_ids[:, None] == jnp.arange(experts, dtype=jnp.int32)[None, :]).astype(jnp.int32)
    position = jnp.sum(jnp.cumsum(onehot, axis=0) * onehot, axis=1) - 1
    target = flat_ids * capacity + position
    slot_source = (
        jnp.full((experts * capacity,), assigned, jnp.int32)
        .at[target]
        .set(jnp.arange(assigned, dtype=jnp.int32))
    )
    return (slot_source.reshape(experts, capacity), target)


def run_expert(expert_gate, expert_up, expert_down, arrived):
    layout = arrived.shape
    flat_rows = arrived.reshape(-1, layout[-1])
    gate_hidden = jnp.dot(flat_rows, expert_gate[0], preferred_element_type=jnp.float32)
    up_hidden = jnp.dot(flat_rows, expert_up[0], preferred_element_type=jnp.float32)
    active = (jax.nn.silu(gate_hidden) * up_hidden).astype(jnp.bfloat16)
    partial_out = jnp.dot(active, expert_down[0], preferred_element_type=jnp.float32).reshape(
        layout
    )
    summed = sum_at_owner(partial_out.astype(jnp.bfloat16), "tp", 1)
    return lax.all_to_all(
        summed.astype(jnp.bfloat16), "sp", split_axis=0, concat_axis=0, tiled=True
    )


def run_quarter(expert_gate, expert_up, expert_down, arrived):
    grouped = gather_directly(arrived[:, None], "tp", 1)
    return run_expert(expert_gate, expert_up, expert_down, grouped)[:, 0]


def on_device(
    mixer_input,
    step_shift,
    log_step,
    decay_real,
    freq_imag,
    in_real,
    in_imag,
    out_real,
    out_imag,
    skip_gain,
    out_weight,
    residual,
    post_gain,
    pre_gain,
    final_gain,
    route_ids,
    route_logits,
    expert_gate,
    expert_up,
    expert_down,
):
    mixed_out = mixer_block(
        mixer_input,
        step_shift,
        log_step,
        decay_real,
        freq_imag,
        in_real,
        in_imag,
        out_real,
        out_imag,
        skip_gain,
    )
    experts = lax.axis_size("sp")
    rows_here = residual.shape[0]
    capacity = max(2, 4 * rows_here // experts)
    quarter = lax.axis_index("tp")
    row_start = quarter * rows_here
    own_logits = lax.dynamic_slice_in_dim(route_logits, row_start, rows_here, 0)
    tokens_view = lax.all_to_all(mixed_out, "tp", split_axis=0, concat_axis=1, tiled=True)
    weight_all = gather_directly(out_weight, "tp", 0)
    projected = jnp.dot(tokens_view, weight_all, preferred_element_type=jnp.float32)
    own_stream = (residual.astype(jnp.float32) + scaled(projected, post_gain)).astype(jnp.bfloat16)
    normed = scaled(own_stream.astype(jnp.float32), pre_gain).astype(jnp.bfloat16)
    own_ids = lax.dynamic_slice_in_dim(route_ids, row_start, rows_here, 0)
    sources, own_targets = slot_table(capacity, experts, own_ids)
    row_index = jnp.where(sources < 2 * rows_here, sources // 2, rows_here)
    padded = jnp.concatenate([normed, jnp.zeros((1, normed.shape[1]), jnp.bfloat16)], axis=0)
    outgoing = padded[row_index]
    quarter_call = functools.partial(run_quarter, expert_gate, expert_up, expert_down)
    results = quarter_call(lax.all_to_all(outgoing, "sp", split_axis=0, concat_axis=0, tiled=True))
    flat_results = results.reshape(-1, results.shape[-1])
    slot_picks = own_targets.reshape(rows_here, 2)
    first_weight = jax.nn.sigmoid(own_logits[:, 0] - own_logits[:, 1])[:, None]
    mixture = first_weight * flat_results[slot_picks[:, 0]].astype(jnp.float32) + (
        1.0 - first_weight
    ) * flat_results[slot_picks[:, 1]].astype(jnp.float32)
    return (own_stream.astype(jnp.float32) + scaled(mixture, final_gain)).astype(jnp.bfloat16)


def solution(mesh):
    in_specs = (
        P("sp", "tp"),
        P("sp", "tp"),
        P("tp"),
        P("tp", None),
        P("tp", None),
        P("tp", None, None),
        P("tp", None, None),
        P("tp", None, None),
        P("tp", None, None),
        P("tp"),
        P("tp", None),
        P(("sp", "tp"), None),
        P(),
        P(),
        P(),
        P("sp", None),
        P("sp", None),
        P("sp", None, "tp"),
        P("sp", None, "tp"),
        P("sp", "tp", None),
    )
    out_specs = P(("sp", "tp"), None)
    return jax.shard_map(
        on_device, mesh=mesh, in_specs=in_specs, out_specs=out_specs, check_vma=False
    )
```

profile of v0, /device:TPU:1, one launch (start us, length us, event | category | flops | bytes accessed | tf_op | source)
XLA Modules:
  0.0 265.2 jit_solution(18184891280422010230)
XLA Ops:
  0.0 0.8 mul.784
  0.8 0.8 mul.789
  1.6 0.7 multiply_add_fusion.23
  2.3 0.9 copy.46
  3.2 0.8 add_exponential_fusion
  4.0 1.2 convolution_bitcast_fusion.1
  5.3 2.5 multiply_add_fusion.18
  8.9 1.0 sine_multiply_fusion
  9.9 9.5 %while.25 = (s32[]{:T(128)}, f32[512]{0:T(512)S(1)}, f32[512]{0:T(512)S(1)}, f32[512]{0:T(512)S(1)}, f32[512]{0:T(512)S(1)}, /*index=5*/f32[8,16,512]{2,1,0:T(8,...) while((s32[]{:T(128)}, f32[512]{0:T(512)S(1)}, ...), condition=%wide.region_1.2_spmd.clone, body=%wide.region_0.1_spmd.clone.sunk | while | flops 116754 | bytes 1135316 | solution.py:93
  19.5 0.7 broadcast_in_dim.95
  20.2 13.0 %all-to-all-start.3 = ((f32[64,1,512]{2,1,0:T(1,128)}), f32[64,1,512]{2,1,0:T(1,128)S(1)}, u32[]{:S(2)}, u32[]{:S(2)}) async-start(f32[64,1,512]{2,1,0:T(1,128)} %broadcast_in_dim.95), calls=%async_computation.3 | async-start | bytes 262144 | tf_op jit(solution)/shard_map/all_to_all | solution.py:11
  33.2 11.1 %all-to-all-done.3 = f32[64,1,512]{2,1,0:T(1,128)S(1)} async-done(((f32[64,1,512]{2,1,0:T(1,128)}), f32[64,1,512]{2,1,0:T(1,128)S(1)}, u32[]{:S(2)}, u32[]{:S(2)}) %all-to-all-start.3) | async-done | bytes 131104 | tf_op jit(solution)/shard_map/all_to_all | solution.py:11
  44.3 0.7 broadcast_in_dim.90
  45.0 4.4 %all-to-all-start = ((f32[64,1,512]{2,1,0:T(1,128)}), f32[64,1,512]{2,1,0:T(1,128)S(1)}, u32[]{:S(2)}, u32[]{:S(2)}) async-start(f32[64,1,512]{2,1,0:T(1,128)} %broadcast_in_dim.90), calls=%async_computation | async-start | bytes 262144 | tf_op jit(solution)/shard_map/all_to_all | solution.py:11
  49.5 11.3 %all-to-all-done = f32[64,1,512]{2,1,0:T(1,128)S(1)} async-done(((f32[64,1,512]{2,1,0:T(1,128)}), f32[64,1,512]{2,1,0:T(1,128)S(1)}, u32[]{:S(2)}, u32[]{:S(2)}) %all-to-all-start) | async-done | bytes 131104 | tf_op jit(solution)/shard_map/all_to_all | solution.py:11
  60.8 0.7 broadcast_in_dim.92
  61.5 4.4 %all-to-all-start.1 = ((f32[64,1,512]{2,1,0:T(1,128)}), f32[64,1,512]{2,1,0:T(1,128)S(1)}, u32[]{:S(2)}, u32[]{:S(2)}) async-start(f32[64,1,512]{2,1,0:T(1,128)} %broadcast_in_dim.92), calls=%async_computation.1 | async-start | bytes 262144 | tf_op jit(solution)/shard_map/all_to_all | solution.py:11
  66.0 11.3 %all-to-all-done.1 = f32[64,1,512]{2,1,0:T(1,128)S(1)} async-done(((f32[64,1,512]{2,1,0:T(1,128)}), f32[64,1,512]{2,1,0:T(1,128)S(1)}, u32[]{:S(2)}, u32[]{:S(2)}) %all-to-all-start.1) | async-done | bytes 131104 | tf_op jit(solution)/shard_map/all_to_all | solution.py:11
  77.3 0.7 broadcast_in_dim.94
  78.0 4.4 %all-to-all-start.2 = ((f32[64,1,512]{2,1,0:T(1,128)}), f32[64,1,512]{2,1,0:T(1,128)S(1)}, u32[]{:S(2)}, u32[]{:S(2)}) async-start(f32[64,1,512]{2,1,0:T(1,128)} %broadcast_in_dim.94), calls=%async_computation.2 | async-start | bytes 262144 | tf_op jit(solution)/shard_map/all_to_all | solution.py:11
  83.0 10.8 %all-to-all-done.2 = f32[64,1,512]{2,1,0:T(1,128)S(1)} async-done(((f32[64,1,512]{2,1,0:T(1,128)}), f32[64,1,512]{2,1,0:T(1,128)S(1)}, u32[]{:S(2)}, u32[]{:S(2)}) %all-to-all-start.2) | async-done | bytes 131104 | tf_op jit(solution)/shard_map/all_to_all | solution.py:11
  95.3 0.9 fusion.16
  96.3 1.0 convolution_subtract_fusion
  97.4 8.3 %all_to_all.77 = bf16[4,32,128]{2,1,0:T(8,128)(2,1)S(1)} all-to-all(bf16[4,32,128]{2,1,0:T(8,128)(2,1)S(1)} %bitcast.649), channel_id=1, replica_groups=mesh['sp'=64,'tp'=4] {'tp'}, dimensions={0} | all-to-all | bytes 65536 | tf_op jit(solution)/shard_map/all_to_all | solution.py:235
  105.7 1.6 broadcast_in_dim.96
  107.3 3.7 %all-to-all-start.5 = ((bf16[4,128,2048]{2,1,0:T(8,128)(2,1)}), bf16[4,128,2048]{2,1,0:T(8,128)(2,1)S(1)}, u32[]{:S(2)}, u32[]{:S(2)}) async-start(bf16[4,128,2048]{2,1,0:T(8,128)(2,1)} %broadcast_in_dim.96), calls=%async_computation.5 | async-start | bytes 4194304 | tf_op jit(solution)/shard_map/all_to_all | solution.py:11
  112.0 1.0 scatter_custom_fusion
  113.3 22.3 %all-to-all-done.5 = bf16[4,128,2048]{2,1,0:T(8,128)(2,1)S(1)} async-done(((bf16[4,128,2048]{2,1,0:T(8,128)(2,1)}), bf16[4,128,2048]{2,1,0:T(8,128)(2,1)S(1)}, u32[]{:S(2)}, u32[]{:S(2)}) %all-to-all-start.5) | async-done | bytes 2097184 | tf_op jit(solution)/shard_map/all_to_all | solution.py:11
  135.6 0.6 multiply_reduce_fusion.1
  136.6 0.9 gather_fusion
  137.5 0.3 reshape.414
  137.9 23.7 %all_to_all.78 = bf16[64,2,2048]{2,1,0:T(2,128)(2,1)S(1)} all-to-all(bf16[64,2,2048]{2,1,0:T(2,128)(2,1)S(1)} %reshape.414), channel_id=1, replica_groups=mesh['sp'=64,'tp'=4] {'sp'}, dimensions={0} | all-to-all | bytes 1048576 | tf_op jit(solution)/shard_map/all_to_all | solution.py:246
  161.6 1.3 broadcast_in_dim.99
  162.9 28.5 %all_to_all.79 = bf16[4,64,1,2,2048]{4,3,1,2,0:T(2,128)(2,1)S(1)} all-to-all(bf16[4,64,1,2,2048]{4,3,1,2,0:T(2,128)(2,1)S(1)} %broadcast_in_dim.99), channel_id=1, replica_groups=mesh['sp'=64,'tp'=4] {'tp'}, dimensions={0} | all-to-all | bytes 4194304 | tf_op jit(solution)/shard_map/all_to_all | solution.py:11
  191.4 2.5 copy.53
  193.9 2.2 reshape_reshape.13
  196.1 5.1 %fusion.4 = f32[512,896]{1,0:T(8,128)S(1)} fusion(bf16[512,2048]{1,0:T(8,128)(2,1)} %reshape_reshape.13, bf16[1,2048,896]{2,1,0:T(8,128)(2,1)} %param.39), kind=kOutput, calls=%fused_computation.140 | convolution fusion | flops 1879048192 | bytes 7602176 | tf_op jit(solution)/shard_map/dot_general | solution.py:178
  201.3 2.4 multiply_convert_fusion
  203.7 0.3 dot_general.33
  204.1 4.4 %fusion.9 = bf16[4,64,1,2,2048]{4,1,3,2,0:T(8,128)(2,1)S(1)} fusion(bf16[1,896,2048]{2,1,0:T(8,128)(2,1)} %param.41, bf16[64,4,2,896]{3,2,1,0:T(2,128)(2,1)S(1)} %dot_general.33), kind=kOutput, calls=%fused_computation.143 | convolution fusion | flops 1880096768 | bytes 6684672 | tf_op jit(solution)/shard_map/dot_general | solution.py:181
  208.4 27.6 %all_to_all.80 = bf16[4,64,1,2,2048]{4,1,3,2,0:T(8,128)(2,1)S(1)} all-to-all(bf16[4,64,1,2,2048]{4,1,3,2,0:T(8,128)(2,1)S(1)} %fusion.9), channel_id=1, replica_groups=mesh['sp'=64,'tp'=4] {'tp'}, dimensions={0} | all-to-all | bytes 4194304 | tf_op jit(solution)/shard_map/all_to_all | solution.py:43
  236.1 0.4 bitcast_reduce_fusion
  236.5 1.3 copy.57
  237.8 7.1 %all-to-all-start.9 = ((bf16[64,1,2,2048]{3,2,1,0:T(2,128)(2,1)}), bf16[64,1,2,2048]{3,2,1,0:T(2,128)(2,1)S(1)}, u32[]{:S(2)}, u32[]{:S(2)}) async-start(bf16[64,1,2,2048]{3,2,1,0:T(2,128)(2,1)} %copy.57), calls=%async_computation.9 | async-start | bytes 1048576 | tf_op jit(solution)/shard_map/all_to_all | solution.py:185
  245.2 17.4 %all-to-all-done.9 = bf16[64,1,2,2048]{3,2,1,0:T(2,128)(2,1)S(1)} async-done(((bf16[64,1,2,2048]{3,2,1,0:T(2,128)(2,1)}), bf16[64,1,2,2048]{3,2,1,0:T(2,128)(2,1)S(1)}, u32[]{:S(2)}, u32[]{:S(2)}) %all-to-all-start.9) | async-done | bytes 524320 | tf_op jit(solution)/shard_map/all_to_all | solution.py:185
  262.8 0.7 gather_fusion.2
  263.5 0.7 gather_fusion.1
  264.4 0.8 fusion.24
  (237 shorter events, 14.5 us)
Async XLA Ops:
  0.0 5.3 %copy-start = (f32[8,64,16]{1,2,0:T(8,128)S(1)}, f32[8,64,16]{1,2,0:T(8,128)}, u32[]{:S(2)}) copy-start(f32[8,64,16]{1,2,0:T(8,128)} %param.27) | copy-start | bytes 98308
  20.2 24.1 %all-to-all-start.3 = ((f32[64,1,512]{2,1,0:T(1,128)}), f32[64,1,512]{2,1,0:T(1,128)S(1)}, u32[]{:S(2)}, u32[]{:S(2)}) async-start(f32[64,1,512]{2,1,0:T(1,128)} %broadcast_in_dim.95), calls=%async_computation.3 | async-start | bytes 262144 | tf_op jit(solution)/shard_map/all_to_all | solution.py:11
  45.0 15.8 %all-to-all-start = ((f32[64,1,512]{2,1,0:T(1,128)}), f32[64,1,512]{2,1,0:T(1,128)S(1)}, u32[]{:S(2)}, u32[]{:S(2)}) async-start(f32[64,1,512]{2,1,0:T(1,128)} %broadcast_in_dim.90), calls=%async_computation | async-start | bytes 262144 | tf_op jit(solution)/shard_map/all_to_all | solution.py:11
  61.5 15.8 %all-to-all-start.1 = ((f32[64,1,512]{2,1,0:T(1,128)}), f32[64,1,512]{2,1,0:T(1,128)S(1)}, u32[]{:S(2)}, u32[]{:S(2)}) async-start(f32[64,1,512]{2,1,0:T(1,128)} %broadcast_in_dim.92), calls=%async_computation.1 | async-start | bytes 262144 | tf_op jit(solution)/shard_map/all_to_all | solution.py:11
  78.0 15.8 %all-to-all-start.2 = ((f32[64,1,512]{2,1,0:T(1,128)}), f32[64,1,512]{2,1,0:T(1,128)S(1)}, u32[]{:S(2)}, u32[]{:S(2)}) async-start(f32[64,1,512]{2,1,0:T(1,128)} %broadcast_in_dim.94), calls=%async_computation.2 | async-start | bytes 262144 | tf_op jit(solution)/shard_map/all_to_all | solution.py:11
  94.4 0.9 copy-start.5
  94.6 1.7 copy-start.6
  95.2 2.2 copy-start.3
  95.2 2.2 copy-start.12
  95.2 10.5 %copy-start.2 = (bf16[128,2048]{1,0:T(8,128)(2,1)S(1)}, bf16[128,2048]{1,0:T(8,128)(2,1)}, u32[]{:S(2)}) copy-start(bf16[128,2048]{1,0:T(8,128)(2,1)} %param.32) | copy-start | bytes 1572868
  107.3 3.8 %copy-start.10 = (s32[128,2]{0,1:T(2,128)S(1)}, s32[128,2]{0,1:T(2,128)}, u32[]{:S(2)}) copy-start(s32[128,2]{0,1:T(2,128)} %param.37) | copy-start | bytes 3076
  107.3 28.3 %all-to-all-start.5 = ((bf16[4,128,2048]{2,1,0:T(8,128)(2,1)}), bf16[4,128,2048]{2,1,0:T(8,128)(2,1)S(1)}, u32[]{:S(2)}, u32[]{:S(2)}) async-start(bf16[4,128,2048]{2,1,0:T(8,128)(2,1)} %broadcast_in_dim.96), calls=%async_computation.5 | async-start | bytes 4194304 | tf_op jit(solution)/shard_map/all_to_all | solution.py:11
  111.1 25.2 %copy-start.4 = (bf16[32,2048]{1,0:T(8,128)(2,1)S(1)}, bf16[32,2048]{1,0:T(8,128)(2,1)}, u32[]{:S(2)}) copy-start(bf16[32,2048]{1,0:T(8,128)(2,1)} %param.33) | copy-start | bytes 393220
  111.1 25.2 %copy-start.7 = (f32[2048]{0:T(1024)S(1)}, f32[2048]{0:T(1024)}, u32[]{:S(2)}) copy-start(f32[2048]{0:T(1024)} %param.34) | copy-start | bytes 24580
  111.1 25.4 %copy-start.9 = (f32[2048]{0:T(1024)S(1)}, f32[2048]{0:T(1024)}, u32[]{:S(2)}) copy-start(f32[2048]{0:T(1024)} %param.35) | copy-start | bytes 24580
  196.1 5.2 %copy-start.1 = (bf16[512,2048]{1,0:T(8,128)(2,1)S(1)}, bf16[512,2048]{1,0:T(8,128)(2,1)}, u32[]{:S(2)}) copy-start(bf16[512,2048]{1,0:T(8,128)(2,1)} %reshape_reshape.13) | copy-start | bytes 6291460
  196.1 5.2 %copy-start.13 = (bf16[1,2048,896]{2,1,0:T(8,128)(2,1)S(1)}, bf16[1,2048,896]{2,1,0:T(8,128)(2,1)}, u32[]{:S(2)}) copy-start(bf16[1,2048,896]{2,1,0:T(8,128)(2,1)} %param.40) | copy-start | bytes 11010052
  236.1 8.8 %copy-start.11 = (f32[128,2]{0,1:T(2,128)S(1)}, f32[128,2]{0,1:T(2,128)}, u32[]{:S(2)}) copy-start(f32[128,2]{0,1:T(2,128)} %param.38) | copy-start | bytes 3076
  237.8 24.8 %all-to-all-start.9 = ((bf16[64,1,2,2048]{3,2,1,0:T(2,128)(2,1)}), bf16[64,1,2,2048]{3,2,1,0:T(2,128)(2,1)S(1)}, u32[]{:S(2)}, u32[]{:S(2)}) async-start(bf16[64,1,2,2048]{3,2,1,0:T(2,128)(2,1)} %copy.57), calls=%async_computation.9 | async-start | bytes 1048576 | tf_op jit(solution)/shard_map/all_to_all | solution.py:185
  244.9 19.4 %copy-start.8 = (f32[2048]{0:T(1024)S(1)}, f32[2048]{0:T(1024)}, u32[]{:S(2)}) copy-start(f32[2048]{0:T(1024)} %param.36) | copy-start | bytes 24580
where the time goes:
time: 266 us; the launch traced here: 265 us
  blocking collectives  88.2 us (33%)
  waiting for transfers between devices  84.2 us (32%)
  starting transfers between devices  37.2 us (14%)
  local copies, waits for them, and re-layouts  27.9 us (10%)
  matrix products  18.1 us (7%)
  other arithmetic  8.38 us (3%)
    all_to_all x5, waiting for transfers between devices, copy_for_each(): return lax.all_to_all(copies, axis, split_axis=0, concat_axis=0, tiled=True)  66.8 us
    all_to_all x5, starting transfers between devices, copy_for_each(): return lax.all_to_all(copies, axis, split_axis=0, concat_axis=0, tiled=True)  30 us
    all_to_all x1, blocking collectives, copy_for_each(): return lax.all_to_all(copies, axis, split_axis=0, concat_axis=0, tiled=True)  28.5 us
    all_to_all x1, blocking collectives, sum_at_owner(): lax.all_to_all(in_blocks(shard, dim, devices), axis, 0, 0, tiled=True)  27.6 us
    all_to_all x1, blocking collectives, on_device(): lax.all_to_all(outgoing, 'sp', split_axis=0, concat_axis=0, tiled=True)  23.7 us
    all_to_all x1, waiting for transfers between devices, run_expert(): lax.all_to_all(summed.astype(jnp.bfloat16), 'sp', split_axis=0, concat_ax...  17.4 us
    all_to_all x1, blocking collectives, on_device(): lax.all_to_all(mixed_out, 'tp', split_axis=0, concat_axis=1, tiled=True)  8.28 us
    all_to_all x1, starting transfers between devices, run_expert(): lax.all_to_all(summed.astype(jnp.bfloat16), 'sp', split_axis=0, concat_ax...  7.1 us
  transfers between devices with their start and end apart: 6, of which 6 were waited for; matrix products, arithmetic and copies ran while one was open for 1% of the time, Pallas kernels for 0%

commit v1 on v0

v1 whole, which is shorter than its diff:
```python
import jax
import jax.numpy as jnp
from jax import lax
from jax.experimental import pallas as pl
from jax.experimental.pallas import tpu as pltpu
from jax.sharding import PartitionSpec as P


F32 = jnp.float32
BF16 = jnp.bfloat16
EXACT = lax.Precision.HIGHEST
EPS = 1e-06
STEP_LIMIT = 300.0
MESSAGE = (8, 256)


def dot(first, second, over=(1, 0), precision=None):
    dims = (((over[0],), (over[1],)), ((), ()))
    return lax.dot_general(first, second, dims, precision=precision, preferred_element_type=F32)


def iota(shape, dim):
    return lax.broadcasted_iota(jnp.int32, shape, dim)


def ones_where(mask, dtype=F32):
    return jnp.where(mask, 1.0, 0.0).astype(dtype)


def sine_cosine(angle):
    quarter = jnp.floor(angle * 0.6366197723675814 + 0.5)
    rest = angle - quarter * 1.5703125
    rest = rest - quarter * 0.0004825592041015625
    rest = rest - quarter * 1.26759079e-06
    square = rest * rest
    sine = ((-1.9515295891e-4 * square + 8.3321608736e-3) * square - 1.6666654611e-1) * square
    sine = sine * rest + rest
    cosine = (2.443315711809948e-5 * square - 1.388731625493765e-3) * square
    cosine = (cosine + 4.166664568298827e-2) * square * square - 0.5 * square + 1.0
    turn = quarter.astype(jnp.int32)
    odd = (turn & 1) == 1
    first, second = (jnp.where(odd, cosine, sine), jnp.where(odd, sine, cosine))
    return (
        jnp.where((turn & 2) == 2, -first, first),
        jnp.where(((turn + 1) & 2) == 2, -second, second),
    )


def rotation(decay, freq, step):
    sine, cosine = sine_cosine(freq * step)
    magnitude = jnp.exp(decay * step)
    return (magnitude * cosine, magnitude * sine)


def delayed(values, by, fill):
    if by >= 8:
        head = jnp.full((by, values.shape[1]), fill, F32)
        return jnp.concatenate([head, values[: values.shape[0] - by]], axis=0)
    return jnp.where(iota(values.shape, 0) >= by, pltpu.roll(values, by, 0), fill)


def mixer_kernel(
    shift, inputs, log_step, decay_real, freq_imag, in_real, in_imag, out_real, out_imag, skip,
    message, rates, read_real, read_imag, cum_real, cum_imag, local_out,
):
    groups, length = shift.shape
    states = decay_real.shape[1]
    channels = in_real.shape[1]
    width = groups * states
    own = ones_where(iota((groups, width), 1) // states == iota((groups, width), 0))
    repeat = ones_where(iota((states, width), 1) % states == iota((states, width), 0))
    square = (groups, groups)
    log_column = jnp.sum(
        jnp.where(iota(square, 0) == iota(square, 1), log_step[...], 0.0), axis=1, keepdims=True
    )
    small_step = jnp.minimum(jnp.exp(log_column + shift[...]), STEP_LIMIT)
    step = dot(small_step.T, own, precision=EXACT)
    decay = jnp.sum(dot(decay_real[...], repeat, precision=EXACT) * own, axis=0, keepdims=True)
    freq = jnp.sum(dot(freq_imag[...], repeat, precision=EXACT) * own, axis=0, keepdims=True)
    rates[...] = jnp.concatenate([decay, freq, jnp.zeros((6, width), F32)], axis=0)
    wide = (groups * channels, width)
    block = ones_where(iota(wide, 0) // channels == iota(wide, 1) // states)

    def spread(ref):
        return dot(ref[...].reshape(wide[0], states), repeat, precision=EXACT) * block

    values = inputs[...].astype(F32)
    into_real = dot(values, spread(in_real), precision=EXACT)
    into_imag = dot(values, spread(in_imag), precision=EXACT)
    read_real[...] = spread(out_real)
    read_imag[...] = spread(out_imag)
    inverse = 1.0 / (decay * decay + freq * freq)
    last_real, last_imag = ([], [])
    result = skip[...] * values
    for start in range(0, width, 128):
        cut = slice(start, start + 128)
        a_real, a_imag = rotation(decay[:, cut], freq[:, cut], step[:, cut])
        minus_one = a_real - 1.0
        coef_real = (minus_one * decay[:, cut] + a_imag * freq[:, cut]) * inverse[:, cut]
        coef_imag = (a_imag * decay[:, cut] - minus_one * freq[:, cut]) * inverse[:, cut]
        s_real = coef_real * into_real[:, cut] - coef_imag * into_imag[:, cut]
        s_imag = coef_real * into_imag[:, cut] + coef_imag * into_real[:, cut]
        by = 1
        while by < length:
            p_real, p_imag = (delayed(s_real, by, 0.0), delayed(s_imag, by, 0.0))
            b_real, b_imag = (delayed(a_real, by, 1.0), delayed(a_imag, by, 0.0))
            s_real, s_imag = (
                s_real + a_real * p_real - a_imag * p_imag,
                s_imag + a_real * p_imag + a_imag * p_real,
            )
            a_real, a_imag = (a_real * b_real - a_imag * b_imag, a_real * b_imag + a_imag * b_real)
            by *= 2
        cum_real[:, cut] = a_real
        cum_imag[:, cut] = a_imag
        last_real.append(s_real[length - 1 :])
        last_imag.append(s_imag[length - 1 :])
        result = result + dot(s_real, read_real[:, cut], (1, 1), EXACT)
        result = result - dot(s_imag, read_imag[:, cut], (1, 1), EXACT)
    local_out[...] = result
    rows, lanes = MESSAGE
    pick = (width, lanes)
    compress = ones_where(
        (iota(pick, 0) == (iota(pick, 1) % groups) * states) & (iota(pick, 1) < 3 * groups)
    )
    total = dot(jnp.sum(step, axis=0, keepdims=True), compress, precision=EXACT)
    first = total.astype(BF16).astype(F32)
    second = (total - first).astype(BF16).astype(F32)
    third = total - first - second
    lane = iota(total.shape, 1)
    total = jnp.where(lane < groups, first, jnp.where(lane < 2 * groups, second, third))
    per = lanes // 128
    lines = [
        jnp.concatenate(part[k : k + per], axis=1)
        for part in (last_real, last_imag)
        for k in range(0, len(part), per)
    ]
    lines.append(total)
    lines.append(jnp.zeros((rows - len(lines), lanes), F32))
    sent = jnp.concatenate(lines, axis=0).astype(BF16)
    message[...] = jnp.broadcast_to(sent[None], message.shape)


def carry_kernel(got, rates, read_real, read_imag, cum_real, cum_imag, local_out, mixed):
    rows, lanes = MESSAGE
    devices = got.shape[0] // rows
    width = rates.shape[1]
    groups = 8
    states = width // groups
    mine = lax.axis_index("sp")
    decay, freq = (rates[0:1, :], rates[1:2, :])
    pick = (devices, devices * rows)
    everything = got[...]

    def line(k):
        return dot(ones_where(iota(pick, 1) == iota(pick, 0) * rows + k, BF16), everything)

    per = width // lanes
    got_real = jnp.concatenate([line(k) for k in range(per)], axis=1)
    got_imag = jnp.concatenate([line(per + k) for k in range(per)], axis=1)
    wide = (lanes, width)
    spread = ones_where(
        (iota(wide, 0) < 3 * groups) & (iota(wide, 0) % groups == iota(wide, 1) // states), BF16
    )
    steps = dot(line(2 * per).astype(BF16), spread)
    square = (devices, devices)
    between = ones_where((iota(square, 0) < iota(square, 1)) & (iota(square, 1) < mine))
    elapsed = jnp.minimum(dot(between, steps, precision=EXACT), STEP_LIMIT)
    weight_real, weight_imag = rotation(decay, freq, elapsed)
    earlier = iota((devices, width), 0) < mine
    weight_real = jnp.where(earlier, weight_real, 0.0)
    weight_imag = jnp.where(earlier, weight_imag, 0.0)
    carry_real = jnp.sum(weight_real * got_real - weight_imag * got_imag, axis=0, keepdims=True)
    carry_imag = jnp.sum(weight_real * got_imag + weight_imag * got_real, axis=0, keepdims=True)
    c_real, c_imag = (cum_real[...], cum_imag[...])
    result = local_out[...]
    result = result + dot(c_real * carry_real - c_imag * carry_imag, read_real[...], (1, 1), EXACT)
    result = result - dot(c_real * carry_imag + c_imag * carry_real, read_imag[...], (1, 1), EXACT)
    mixed[...] = jax.nn.gelu(result).astype(BF16)


def route_kernel(ids, logits, place, weigh):
    slots = weigh.shape[1] // 4
    tall = (slots, slots)
    rows = slots // 4
    member, lane = (iota(tall, 0) % rows, iota(tall, 1))
    here = lane == lax.axis_index("tp") * rows + member

    def column(line):
        return jnp.sum(jnp.where(here, line, 0.0), axis=1, keepdims=True)

    named = ids[...].astype(F32)
    expert = (lane // 2).astype(F32)
    is_first = ones_where(column(named[0:1]) == expert)
    is_second = ones_where(column(named[1:2]) == expert)
    before = ones_where((lane % rows < member) & (lane // rows == iota(tall, 0) // rows), BF16)
    count = dot(before, (is_first + is_second).astype(BF16))
    kept = ones_where(count == (lane % 2).astype(F32))
    first = jax.nn.sigmoid(column(logits[0:1, :]) - column(logits[1:2, :]))
    long = (slots * 4, slots)
    repeat = ones_where(iota(long, 0) // 4 == iota(long, 1), BF16)
    put = dot(repeat, ((is_first + is_second) * kept).astype(BF16), (1, 1))
    place[...] = jnp.where(iota(long, 0) % 4 == iota(long, 1) // rows, put, 0.0).astype(BF16)
    weight = (is_first * first + is_second * (1.0 - first)) * kept
    back = (slots, slots * 4)
    repeat = ones_where(iota(back, 1) // 4 == iota(back, 0))
    took = dot(weight, repeat, precision=EXACT)
    weigh[...] = jnp.where(iota(back, 1) % 4 == iota(back, 0) // rows, took, 0.0)


def normalized(values, gain):
    return values * lax.rsqrt(jnp.mean(values * values, axis=-1, keepdims=True) + EPS) * gain


def project_kernel(
    tokens, weight_0, weight_1, weight_2, weight_3, residual, post_gain, pre_gain, place,
    stream, outgoing,
):
    rows, width = residual.shape
    quarter = lax.axis_index("tp")
    projected = jnp.zeros((rows, width), F32)
    for by, weight in enumerate((weight_0, weight_1, weight_2, weight_3)):
        source = lax.rem(quarter + 4 - by, 4)
        part = tokens[pl.ds(pl.multiple_of(source * rows, rows), rows), :]
        projected = projected + dot(part, weight[...])
    own = (residual[...].astype(F32) + normalized(projected, post_gain[...])).astype(BF16)
    stream[...] = own
    normed = normalized(own.astype(F32), pre_gain[...]).astype(BF16)
    cut = width // 4
    stacked = jnp.concatenate([normed[:, q * cut : (q + 1) * cut] for q in range(4)], axis=0)
    outgoing[...] = dot(place[...], stacked).astype(BF16)


def expert_kernel(halves, weights, results, arrived=lambda which, q: None):
    gate, up, down = weights
    count = len(halves) // 2
    lines, cut = (2 * halves[0].shape[0], halves[0].shape[1])
    slots = lines // 4
    whole = [
        jnp.concatenate([halves[2 * k][...], halves[2 * k + 1][...]], axis=0) for k in range(count)
    ]
    pick = (slots, lines)
    gate_hidden = up_hidden = None
    for q in range(4):
        chosen = ones_where(iota(pick, 1) == iota(pick, 0) * 4 + q, BF16)
        part = jnp.concatenate([dot(chosen, rows).astype(BF16) for rows in whole], axis=0)
        span = slice(q * cut, (q + 1) * cut)
        arrived(0, q)
        gate_part = dot(part, gate[0, span, :])
        arrived(1, q)
        up_part = dot(part, up[0, span, :])
        gate_hidden = gate_part if q == 0 else gate_hidden + gate_part
        up_hidden = up_part if q == 0 else up_hidden + up_part
    active = (jax.nn.silu(gate_hidden) * up_hidden).astype(BF16)
    made = []
    for q in range(4):
        arrived(2, q)
        made.append(dot(active, down[0, :, q * cut : (q + 1) * cut]).astype(BF16))
    half = (lines // 2, lines)
    for k in range(count):
        stacked = jnp.concatenate([m[k * slots : (k + 1) * slots] for m in made], axis=0)
        for side in range(2):
            line = iota(half, 0) + side * (lines // 2)
            order = ones_where(iota(half, 1) == (line % 4) * slots + line // 4, BF16)
            results[2 * k + side][...] = dot(order, stacked).astype(BF16)


def own_rows_kernel(first, last, gate, up, down, made_first, made_last, *held):
    *weights, semaphores = held
    cut = first.shape[1]

    def fetch(which, q):
        source = (gate, up, down)[which]
        span = pl.ds(q * cut, cut)
        place = (0, slice(None), span) if which == 2 else (0, span, slice(None))
        return pltpu.make_async_copy(
            source.at[place], weights[which].at[place], semaphores.at[which * 4 + q]
        )

    for q in range(4):
        fetch(0, q).start()
        fetch(1, q).start()
    for q in range(4):
        fetch(2, q).start()
    expert_kernel(
        (first, last), weights, (made_first, made_last), lambda which, q: fetch(which, q).wait()
    )


def other_rows_kernel(count, *refs):
    expert_kernel(refs[:count], refs[count : count + 3], refs[count + 3 : 2 * count + 3])


def combine_kernel(results, weigh, stream, final_gain, out):
    rows = stream.shape[0]
    mixture = dot(weigh[...], results[...].astype(F32), precision=EXACT)
    mixture = jnp.concatenate([mixture[q * rows : (q + 1) * rows] for q in range(4)], axis=1)
    out[...] = (stream[...].astype(F32) + normalized(mixture, final_gain[...])).astype(BF16)


def call(kernel, outs, *args, flops=0, in_place=(), scratch=()):
    whole = pl.BlockSpec(memory_space=pltpu.VMEM)
    left = pl.BlockSpec(memory_space=pl.ANY)
    single = not isinstance(outs, list)
    shapes = [
        jax.ShapeDtypeStruct(*out) if isinstance(out, tuple) else out
        for out in ([outs] if single else outs)
    ]
    made = pl.pallas_call(
        kernel,
        out_shape=shapes,
        in_specs=[left if k in in_place else whole for k in range(len(args))],
        out_specs=[whole] * len(shapes),
        scratch_shapes=list(scratch),
        cost_estimate=pl.CostEstimate(flops=flops, bytes_accessed=0, transcendentals=0),
        compiler_params=pltpu.CompilerParams(vmem_limit_bytes=VMEM_LIMIT),
    )(*args)
    return made[0] if single else made


VMEM_LIMIT = 24 * 2**20


def in_hbm(value):
    return pltpu.with_memory_space_constraint(value, pltpu.HBM)


def across_sp(pieces):
    return lax.all_to_all(pieces, "sp", split_axis=0, concat_axis=0, tiled=True)


def shifted(part, by):
    size = lax.axis_size("tp")
    return lax.ppermute(part, "tp", [(i, (i + by) % size) for i in range(size)])


def added(first, second):
    return (first.astype(F32) + second.astype(F32)).astype(BF16)


def run_expert(weights, own):
    lines, cut = own.shape
    half = (lines // 2, cut)
    work = 2 * (lines // 4) * 3 * weights[0].shape[1] * weights[0].shape[2]
    first, last = (own[: half[0]], own[half[0] :])
    left_first, right_last = (shifted(first, 1), shifted(last, -1))
    left_last, right_first = (shifted(last, 1), shifted(first, -1))
    across_first, across_last = (shifted(left_first, 1), shifted(right_last, -1))
    own_first, own_last, *held = call(
        own_rows_kernel,
        [(half, BF16), (half, BF16), *(pltpu.VMEM(w.shape, w.dtype) for w in weights)],
        first,
        last,
        *(in_hbm(w) for w in weights),
        flops=work,
        in_place=(2, 3, 4),
        scratch=[pltpu.SemaphoreType.DMA((12,))],
    )

    def part(*halves):
        count = len(halves)
        return call(
            lambda *refs: other_rows_kernel(count, *refs), [(half, BF16)] * count,
            *halves, *held, flops=work * count // 2,
        )

    to_left_first, to_left_last, to_right_first, to_right_last = part(
        left_first, left_last, right_first, right_last
    )
    from_left_last, from_right_first = (shifted(to_right_last, 1), shifted(to_left_first, -1))
    far_first, far_last = part(across_first, across_last)
    to_right_first = added(to_right_first, shifted(far_first, 1))
    to_left_last = added(to_left_last, shifted(far_last, -1))
    from_left_first, from_right_last = (shifted(to_right_first, 1), shifted(to_left_last, -1))

    def total(*parts):
        return sum(part.astype(F32) for part in parts).astype(BF16)

    return jnp.concatenate(
        [
            total(own_first, from_left_first, from_right_first),
            total(own_last, from_left_last, from_right_last),
        ]
    )


def on_device(
    mixer_input,
    step_shift,
    log_step,
    decay_real,
    freq_imag,
    in_real,
    in_imag,
    out_real,
    out_imag,
    skip_gain,
    out_weight,
    residual,
    post_gain,
    pre_gain,
    final_gain,
    route_ids,
    route_logits,
    expert_gate,
    expert_up,
    expert_down,
):
    devices, quarters = (lax.axis_size("sp"), lax.axis_size("tp"))
    rows, width = residual.shape
    length, wide = (mixer_input.shape[0], decay_real.size)
    channels = mixer_input.shape[1]
    slots = 2 * devices
    gathered = [out_weight, *(shifted(out_weight, by) for by in range(1, quarters))]
    message, rates, read_real, read_imag, cum_real, cum_imag, local_out = call(
        mixer_kernel,
        [
            ((devices, *MESSAGE), BF16),
            ((8, wide), F32),
            ((channels, wide), F32),
            ((channels, wide), F32),
            ((length, wide), F32),
            ((length, wide), F32),
            ((length, channels), F32),
        ],
        *map(
            in_hbm,
            (
                step_shift.T,
                mixer_input,
                log_step[None],
                decay_real,
                freq_imag,
                jnp.swapaxes(in_real, 1, 2),
                jnp.swapaxes(in_imag, 1, 2),
                out_real,
                out_imag,
                skip_gain[None],
            ),
        ),
        flops=10**9,
    )
    got = across_sp(message)
    place, weigh = call(
        route_kernel,
        [((4 * slots, slots), BF16), ((slots, 4 * slots), F32)],
        route_ids.T,
        route_logits.T,
        flops=10**8,
    )
    mixed = call(
        carry_kernel, ((length, channels), BF16),
        got.reshape(-1, MESSAGE[1]), rates, read_real, read_imag, cum_real, cum_imag, local_out,
        flops=10**9,
    )
    tokens = lax.all_to_all(
        mixed.reshape(quarters, rows, channels), "tp", split_axis=0, concat_axis=0, tiled=True
    )
    stream, outgoing = call(
        project_kernel,
        [((rows, width), BF16), ((4 * slots, width // 4), BF16)],
        tokens.reshape(-1, channels),
        *gathered,
        residual,
        post_gain[None],
        pre_gain[None],
        place,
        flops=10**9,
    )
    pieces = (devices, 4 * slots // devices, width // 4)
    arrived = across_sp(outgoing.reshape(pieces))
    summed = run_expert((expert_gate, expert_up, expert_down), arrived.reshape(outgoing.shape))
    results = across_sp(summed.reshape(pieces))
    return call(
        combine_kernel, ((rows, width), BF16),
        results.reshape(outgoing.shape), weigh, stream, final_gain[None], flops=10**9,
    )


def solution(mesh):
    in_specs = (
        P("sp", "tp"),
        P("sp", "tp"),
        P("tp"),
        P("tp", None),
        P("tp", None),
        P("tp", None, None),
        P("tp", None, None),
        P("tp", None, None),
        P("tp", None, None),
        P("tp"),
        P("tp", None),
        P(("sp", "tp"), None),
        P(),
        P(),
        P(),
        P("sp", None),
        P("sp", None),
        P("sp", None, "tp"),
        P("sp", None, "tp"),
        P("sp", "tp", None),
    )
    out_specs = P(("sp", "tp"), None)

    return jax.shard_map(
        on_device, mesh=mesh, in_specs=in_specs, out_specs=out_specs, check_vma=False
    )
```

time: 266 us -> 147 us (0.55)
  waiting for transfers between devices: 84.2 us -> 27.1 us
  blocking collectives: 88.2 us -> 55.2 us
  local copies, waits for them, and re-layouts: 27.9 us -> 1.71 us
  Pallas kernels: 0 us -> 24.6 us
  matrix products: 18.1 us -> 0 us
  other arithmetic: 8.38 us -> 0.37 us
    all_to_all x6 -> x2, waiting for transfers between devices: 84.2 us -> 8.35 us  [the longest x1 8 us: across_sp(): return lax.all_to_all(pieces, 'sp', split_axis=0, concat_axis=0, tiled=True)]
    all_to_all x4 -> x2, blocking collectives: 88.2 us -> 55.2 us  [across_sp(): return lax.all_to_all(pieces, 'sp', split_axis=0, concat_axis=0, tiled=True)]
    pallas_call x0 -> x8, Pallas kernels: none -> 24.6 us  [call(): pl.pallas_call(kernel, out_shape=shapes, in_specs=[left if k in in_place...]
    ppermute x0 -> x15, starting transfers between devices: none -> 20.3 us  [shifted(): return lax.ppermute(part, 'tp', [(i, (i + by) % size) for i in range(size)])]
    all_to_all x6 -> x2, starting transfers between devices: 37.2 us -> 17.2 us  [the longest x1 13 us: across_sp(): return lax.all_to_all(pieces, 'sp', split_axis=0, concat_axis=0, tiled=True)]
    ppermute x0 -> x15, waiting for transfers between devices: none -> 18.8 us  [shifted(): return lax.ppermute(part, 'tp', [(i, (i + by) % size) for i in range(size)])]
    dot_general x8 -> x0, matrix products: 18.1 us -> none  [the longest x1 5.14 us: run_expert(): jnp.dot(flat_rows, expert_gate[0], preferred_element_type=jnp.float32)]
    broadcast_in_dim x6 -> x0, local copies, waits for them, and re-layouts: 5.79 us -> none  [copy_for_each(): copies = jnp.broadcast_to(shard, (lax.axis_size(axis), *shard.shape))]
  transfers between devices with their start and end apart: 6 -> 17, of which waited for: 6 -> 7; matrix products, arithmetic and copies ran while one was open for 1% -> 0% of each run, Pallas kernels for 0% -> 11%
where the time goes in v1:
time: 147 us
  blocking collectives  55.2 us (38%)
  starting transfers between devices  37.4 us (25%)
  waiting for transfers between devices  27.1 us (18%)
  Pallas kernels  24.6 us (17%)
  local copies, waits for them, and re-layouts  1.71 us (1%)
    all_to_all x2, blocking collectives, across_sp(): return lax.all_to_all(pieces, 'sp', split_axis=0, concat_axis=0, tiled=True)  55.2 us
    pallas_call x8, Pallas kernels, call(): pl.pallas_call(kernel, out_shape=shapes, in_specs=[left if k in in_place...  24.6 us
    ppermute x15, starting transfers between devices, shifted(): return lax.ppermute(part, 'tp', [(i, (i + by) % size) for i in range(size)])  20.3 us
    ppermute x15, waiting for transfers between devices, shifted(): return lax.ppermute(part, 'tp', [(i, (i + by) % size) for i in range(size)])  18.8 us
    all_to_all x1, starting transfers between devices, across_sp(): return lax.all_to_all(pieces, 'sp', split_axis=0, concat_axis=0, tiled=True)  13 us
    all_to_all x1, waiting for transfers between devices, across_sp(): return lax.all_to_all(pieces, 'sp', split_axis=0, concat_axis=0, tiled=True)  8 us
    all_to_all x1, starting transfers between devices, on_device(): lax.all_to_all(mixed.reshape(quarters, rows, channels), 'tp', split_axis=...  4.19 us
  transfers between devices with their start and end apart: 17, of which 7 were waited for; matrix products, arithmetic and copies ran while one was open for 0% of the time, Pallas kernels for 11%

profile of v1, /device:TPU:1, one launch (start us, length us, event | category | flops | bytes accessed | tf_op | source)
XLA Modules:
  0.0 146.6 jit_solution(3841672215752098680)
XLA Ops:
  0.0 5.9 %shard_map.190 = (bf16[64,8,256]{2,1,0:T(8,128)(2,1)}, f32[8,512]{1,0:T(8,128)S(1)}, f32[128,512]{1,0:T(8,128)S(1)}, f32[128,512]{1,0:T(8,128)S(1)}, f32[128,512...) custom-call(f32[8,128]{1,0:T(8,128)} %bitcast.32, bf16[128,128]{1,0:T(8,128)(2,1)} %inputs.1, ...), custom_call_target="tpu_custom_call" | custom-call | flops 1000000000 | tf_op jit(solution)/shard_map/pallas_call | solution.py:308
  5.9 0.7 copy-done.7
  6.6 13.0 %all-to-all-start = ((bf16[64,8,256]{2,1,0:T(8,128)(2,1)}), bf16[64,8,256]{2,1,0:T(8,128)(2,1)S(1)}, u32[]{:S(2)}, u32[]{:S(2)}) async-start(bf16[64,8,256]{2,1,0:T(8,128)(2,1)} %get-tuple-element.27), calls=%async_computation | async-start | bytes 524288 | tf_op jit(solution)/shard_map/all_to_all | solution.py:328
  19.6 1.4 collective-permute-start
  21.0 2.6 %collective-permute-start.1 = (bf16[128,2048]{1,0:T(8,128)(2,1)S(1)}, bf16[128,2048]{1,0:T(8,128)(2,1)S(1)}, u32[]{:S(2)}, u32[]{:S(2)}) collective-permute-start(bf16[128,2048]{1,0:T(8,128)(2,1)S(1)} %copy-done), channel_id=1, source_target_pairs={{0,2},{1,3},{2,0},{3,1},{4,6},{5,7},{6,4},{7,5},{8,10},{9,11},{10,... | collective-permute-start | bytes 1572872 | tf_op jit(solution)/shard_map/ppermute | solution.py:333
  23.6 1.1 collective-permute-start.2
  24.7 8.0 %all-to-all-done = bf16[64,8,256]{2,1,0:T(8,128)(2,1)S(1)} async-done(((bf16[64,8,256]{2,1,0:T(8,128)(2,1)}), bf16[64,8,256]{2,1,0:T(8,128)(2,1)S(1)}, u32[]{:S(2)}, u32[]{:S(2)}) %all-to-all-start) | async-done | bytes 262176 | tf_op jit(solution)/shard_map/all_to_all | solution.py:328
  32.7 0.9 copy-done.8
  33.6 2.5 %shard_map.191 = bf16[128,128]{1,0:T(8,128)(2,1)} custom-call(bf16[512,256]{1,0:T(8,128)(2,1)S(1)} %bitcast.23, f32[8,512]{1,0:T(8,128)S(1)} %get-tuple-element.28.rates, f32[128,512]{1,0:T(8,128)S(1)} %get-tuple-element.29.read_real, f32[128,512]{1,0:T(8,128)S(1)} %get-tuple-element.30.read_imag, f32[128,512]{1,0:T(8,128)S(1)} %get-tuple-element.31.cum_real, ...), custom_call_target="tpu_custom_call" | custom-call | flops 1000000000 | tf_op jit(solution)/shard_map/pallas_call | solution.py:308
  36.1 4.2 %all-to-all-start.1 = ((bf16[4,32,128]{2,1,0:T(8,128)(2,1)}), bf16[4,32,128]{2,1,0:T(8,128)(2,1)S(1)}, u32[]{:S(2)}, u32[]{:S(2)}) async-start(bf16[4,32,128]{2,1,0:T(8,128)(2,1)} %bitcast.6), calls=%async_computation.1 | async-start | bytes 65536 | tf_op jit(solution)/shard_map/all_to_all | solution.py:455
  40.3 0.6 shard_map.192
  40.9 0.0 collective-permute-done.weight_1
  40.9 5.5 %collective-permute-done.1.weight_2 = bf16[128,2048]{1,0:T(8,128)(2,1)S(1)} collective-permute-done((bf16[128,2048]{1,0:T(8,128)(2,1)S(1)}, bf16[128,2048]{1,0:T(8,128)(2,1)S(1)}, u32[]{:S(2)}, u32[]{:S(2)}) %collective-permute-start.1) | collective-permute-done | bytes 524320 | tf_op jit(solution)/shard_map/ppermute | solution.py:333
  46.4 0.0 collective-permute-done.2.weight_3
  46.4 0.3 all-to-all-done.1
  46.8 0.9 shard_map.193
  47.7 28.7 %all_to_all.20 = bf16[64,8,512]{2,1,0:T(8,128)(2,1)S(1)} all-to-all(bf16[64,8,512]{2,1,0:T(8,128)(2,1)S(1)} %bitcast.21), channel_id=1, replica_groups=mesh['sp'=64,'tp'=4] {'sp'}, dimensions={0} | all-to-all | bytes 1048576 | tf_op jit(solution)/shard_map/all_to_all | solution.py:328
  76.5 1.7 %collective-permute-start.3 = (bf16[256,512]{1,0:T(8,128)(2,1)S(1)}, bf16[256,512]{1,0:T(8,128)(2,1)S(1)}, u32[]{:S(2)}, u32[]{:S(2)}) collective-permute-start(bf16[256,512]{1,0:T(8,128)(2,1)S(1)} %get-tuple-element.50.first), channel_id=1, source_target_pairs={{0,1},{1,2},{2,3},{3,0},{4,5},{5,6},{6,7},{7,4},{8,9},{9,10},{10,1... | collective-permute-start | bytes 786440 | tf_op jit(solution)/shard_map/ppermute | solution.py:333
  78.2 1.0 collective-permute-start.6
  79.2 6.0 %collective-permute-done.3.refs_0_ = bf16[256,512]{1,0:T(8,128)(2,1)S(1)} collective-permute-done((bf16[256,512]{1,0:T(8,128)(2,1)S(1)}, bf16[256,512]{1,0:T(8,128)(2,1)S(1)}, u32[]{:S(2)}, u32[]{:S(2)}) %collective-permute-start.3) | collective-permute-done | bytes 262176 | tf_op jit(solution)/shard_map/ppermute | solution.py:333
  85.2 0.4 collective-permute-start.7
  85.7 0.0 collective-permute-done.6.refs_3_
  85.7 2.2 %collective-permute-start.8 = (bf16[256,512]{1,0:T(8,128)(2,1)S(1)}, bf16[256,512]{1,0:T(8,128)(2,1)S(1)}, u32[]{:S(2)}, u32[]{:S(2)}) collective-permute-start(bf16[256,512]{1,0:T(8,128)(2,1)S(1)} %collective-permute-done.6.refs_3_), channel_id=1, source_target_pairs={{0,3},{1,0},{2,1},{3,2},{4,7},{5,4},{6,5},{7,6},{8,11},{9,8},{10,9... | collective-permute-start | bytes 786440 | tf_op jit(solution)/shard_map/ppermute | solution.py:333
  87.9 2.7 %collective-permute-start.5 = (bf16[256,512]{1,0:T(8,128)(2,1)S(1)}, bf16[256,512]{1,0:T(8,128)(2,1)S(1)}, u32[]{:S(2)}, u32[]{:S(2)}) collective-permute-start(bf16[256,512]{1,0:T(8,128)(2,1)S(1)} %get-tuple-element.50.first), channel_id=1, source_target_pairs={{0,3},{1,0},{2,1},{3,2},{4,7},{5,4},{6,5},{7,6},{8,11},{9,8},{10,9... | collective-permute-start | bytes 786440 | tf_op jit(solution)/shard_map/ppermute | solution.py:333
  90.6 5.7 %shard_map.194 = (bf16[256,512]{1,0:T(8,128)(2,1)S(1)}, bf16[256,512]{1,0:T(8,128)(2,1)S(1)}, bf16[1,2048,896]{2,1,0:T(8,128)(2,1)S(1)}, bf16[1,2048,896]{2,1,0:T(8,128)(2,1)S(1)}, bf16[1,896,2048]{2,1,0:T(8,128)(2,1)S(1)}) custom-call(bf16[256,512]{1,0:T(8,128)(2,1)S(1)} %get-tuple-element.50.first, bf16[256,512]{1,0:T(8,128)(2,1)S(1)} %get-tuple-element.49.last, ...), custom_call_target="tpu_custom_call" | custom-call | flops 1409286144 | tf_op jit(solution)/shard_map/pallas_call | solution.py:308
  96.3 0.0 collective-permute-done.7.refs_0_
  96.3 2.8 %shard_map.196 = (bf16[256,512]{1,0:T(8,128)(2,1)S(1)}, bf16[256,512]{1,0:T(8,128)(2,1)S(1)}) custom-call(bf16[256,512]{1,0:T(8,128)(2,1)S(1)} %collective-permute-done.7.refs_0_, bf16[256,512]{1,0:T(8,128)(2,1)S(1)} %collective-permute-done.8.refs_1_, bf16[1,2048,896]{2,1,0:T(8,128)(2,1)S(1)} %get-tuple-element.37.refs_4_.refs_2_, ...), custom_call_target="tpu_custom_call" | custom-call | flops 1409286144 | tf_op jit(solution)/shard_map/pallas_call | solution.py:308
  99.1 0.1 collective-permute-start.9
  99.2 2.7 %collective-permute-start.13 = (bf16[256,512]{1,0:T(8,128)(2,1)S(1)}, bf16[256,512]{1,0:T(8,128)(2,1)S(1)}, u32[]{:S(2)}, u32[]{:S(2)}) collective-permute-start(bf16[256,512]{1,0:T(8,128)(2,1)S(1)} %get-tuple-element.46), channel_id=1, source_target_pairs={{0,3},{1,0},{2,1},{3,2},{4,7},{5,4},{6,5},{7,6},{8,11},{9,8},{10,9... | collective-permute-start | bytes 786440 | tf_op jit(solution)/shard_map/ppermute | solution.py:333
  101.9 0.0 collective-permute-done.4.refs_1_
  101.9 0.0 collective-permute-done.5.refs_2_
  101.9 4.8 %shard_map.195 = (bf16[256,512]{1,0:T(8,128)(2,1)S(1)}, bf16[256,512]{1,0:T(8,128)(2,1)S(1)}, bf16[256,512]{1,0:T(8,128)(2,1)S(1)}, bf16[256,512]{1,0:T(8,128)(2,1)S(1)}) custom-call(bf16[256,512]{1,0:T(8,128)(2,1)S(1)} %collective-permute-done.3.refs_0_, bf16[256,512]{1,0:T(8,128)(2,1)S(1)} %collective-permute-done.4.refs_1_, ...), custom_call_target="tpu_custom_call" | custom-call | flops 2818572288 | tf_op jit(solution)/shard_map/pallas_call | solution.py:308
  106.7 0.0 copy-start.4
  106.7 0.1 collective-permute-start.11
  106.8 0.1 add_convert_fusion.3
  106.9 1.5 %collective-permute-start.10 = (bf16[256,512]{1,0:T(8,128)(2,1)S(1)}, bf16[256,512]{1,0:T(8,128)(2,1)S(1)}, u32[]{:S(2)}, u32[]{:S(2)}) collective-permute-start(bf16[256,512]{1,0:T(8,128)(2,1)S(1)} %add_convert_fusion.3), channel_id=1, source_target_pairs={{0,1},{1,2},{2,3},{3,0},{4,5},{5,6},{6,7},{7,4},{8,9},{9,10},{10,1... | collective-permute-start | bytes 786440 | tf_op jit(solution)/shard_map/ppermute | solution.py:333
  108.4 0.1 collective-permute-start.12
  108.5 0.0 collective-permute-done.13
  108.5 0.1 add_convert_fusion.1
  108.6 2.7 %collective-permute-start.14 = (bf16[256,512]{1,0:T(8,128)(2,1)S(1)}, bf16[256,512]{1,0:T(8,128)(2,1)S(1)}, u32[]{:S(2)}, u32[]{:S(2)}) collective-permute-start(bf16[256,512]{1,0:T(8,128)(2,1)S(1)} %add_convert_fusion.1), channel_id=1, source_target_pairs={{0,3},{1,0},{2,1},{3,2},{4,7},{5,4},{6,5},{7,6},{8,11},{9,8},{10,9... | collective-permute-start | bytes 786440 | tf_op jit(solution)/shard_map/ppermute | solution.py:333
  111.2 0.8 collective-permute-done.11
  112.0 1.4 collective-permute-done.10
  113.4 0.1 add_convert_fusion.2
  113.5 5.0 %collective-permute-done.12 = bf16[256,512]{1,0:T(8,128)(2,1)S(1)} collective-permute-done((bf16[256,512]{1,0:T(8,128)(2,1)S(1)}, bf16[256,512]{1,0:T(8,128)(2,1)S(1)}, u32[]{:S(2)}, u32[]{:S(2)}) %collective-permute-start.12) | collective-permute-done | bytes 262176 | tf_op jit(solution)/shard_map/ppermute | solution.py:333
  118.5 0.0 collective-permute-done.14
  118.5 0.1 add_convert_fusion
  118.7 26.5 %all_to_all.21 = bf16[64,8,512]{2,1,0:T(8,128)(2,1)S(1)} all-to-all(bf16[64,8,512]{2,1,0:T(8,128)(2,1)S(1)} %maximum_bitcast_fusion), channel_id=1, replica_groups=mesh['sp'=64,'tp'=4] {'sp'}, dimensions={0} | all-to-all | bytes 1048576 | tf_op jit(solution)/shard_map/all_to_all | solution.py:328
  145.2 1.4 shard_map.197
  (20 shorter events, 0.1 us)
Async XLA Ops:
  0.0 19.6 %copy-start = (bf16[128,2048]{1,0:T(8,128)(2,1)S(1)}, bf16[128,2048]{1,0:T(8,128)(2,1)}, u32[]{:S(2)}) copy-start(bf16[128,2048]{1,0:T(8,128)(2,1)} %weight_0.1) | copy-start | bytes 1572868
  0.0 40.3 %copy-start.5 = (s32[128,2]{0,1:T(2,128)S(1)}, s32[128,2]{0,1:T(2,128)}, u32[]{:S(2)}) copy-start(s32[128,2]{0,1:T(2,128)} %param.35) | copy-start | bytes 3076
  0.0 40.3 %copy-start.6 = (f32[128,2]{0,1:T(2,128)S(1)}, f32[128,2]{0,1:T(2,128)}, u32[]{:S(2)}) copy-start(f32[128,2]{0,1:T(2,128)} %param.36) | copy-start | bytes 3076
  0.0 46.8 %copy-start.1 = (bf16[32,2048]{1,0:T(8,128)(2,1)S(1)}, bf16[32,2048]{1,0:T(8,128)(2,1)}, u32[]{:S(2)}) copy-start(bf16[32,2048]{1,0:T(8,128)(2,1)} %residual.1) | copy-start | bytes 393220
  0.0 46.8 %copy-start.2 = (f32[2048]{0:T(1024)S(1)}, f32[2048]{0:T(1024)}, u32[]{:S(2)}) copy-start(f32[2048]{0:T(1024)} %param.32) | copy-start | bytes 24580
  0.0 46.8 %copy-start.3 = (f32[2048]{0:T(1024)S(1)}, f32[2048]{0:T(1024)}, u32[]{:S(2)}) copy-start(f32[2048]{0:T(1024)} %param.33) | copy-start | bytes 24580
  5.9 0.7 copy-start.7
  6.6 26.1 %all-to-all-start = ((bf16[64,8,256]{2,1,0:T(8,128)(2,1)}), bf16[64,8,256]{2,1,0:T(8,128)(2,1)S(1)}, u32[]{:S(2)}, u32[]{:S(2)}) async-start(bf16[64,8,256]{2,1,0:T(8,128)(2,1)} %get-tuple-element.27), calls=%async_computation | async-start | bytes 524288 | tf_op jit(solution)/shard_map/all_to_all | solution.py:328
  19.6 21.3 %collective-permute-start = (bf16[128,2048]{1,0:T(8,128)(2,1)S(1)}, bf16[128,2048]{1,0:T(8,128)(2,1)S(1)}, u32[]{:S(2)}, u32[]{:S(2)}) collective-permute-start(bf16[128,2048]{1,0:T(8,128)(2,1)S(1)} %copy-done), channel_id=1, source_target_pairs={{0,1},{1,2},{2,3},{3,0},{4,5},{5,6},{6,7},{7,4},{8,9},{9,10},{10,1... | collective-permute-start | bytes 1572872 | tf_op jit(solution)/shard_map/ppermute | solution.py:333
  21.0 25.5 %collective-permute-start.1 = (bf16[128,2048]{1,0:T(8,128)(2,1)S(1)}, bf16[128,2048]{1,0:T(8,128)(2,1)S(1)}, u32[]{:S(2)}, u32[]{:S(2)}) collective-permute-start(bf16[128,2048]{1,0:T(8,128)(2,1)S(1)} %copy-done), channel_id=1, source_target_pairs={{0,2},{1,3},{2,0},{3,1},{4,6},{5,7},{6,4},{7,5},{8,10},{9,11},{10,... | collective-permute-start | bytes 1572872 | tf_op jit(solution)/shard_map/ppermute | solution.py:333
  23.6 22.8 %collective-permute-start.2 = (bf16[128,2048]{1,0:T(8,128)(2,1)S(1)}, bf16[128,2048]{1,0:T(8,128)(2,1)S(1)}, u32[]{:S(2)}, u32[]{:S(2)}) collective-permute-start(bf16[128,2048]{1,0:T(8,128)(2,1)S(1)} %copy-done), channel_id=1, source_target_pairs={{0,3},{1,0},{2,1},{3,2},{4,7},{5,4},{6,5},{7,6},{8,11},{9,8},{10,9... | collective-permute-start | bytes 1572872 | tf_op jit(solution)/shard_map/ppermute | solution.py:333
  32.7 1.0 copy-start.8
  36.1 10.7 %all-to-all-start.1 = ((bf16[4,32,128]{2,1,0:T(8,128)(2,1)}), bf16[4,32,128]{2,1,0:T(8,128)(2,1)S(1)}, u32[]{:S(2)}, u32[]{:S(2)}) async-start(bf16[4,32,128]{2,1,0:T(8,128)(2,1)} %bitcast.6), calls=%async_computation.1 | async-start | bytes 65536 | tf_op jit(solution)/shard_map/all_to_all | solution.py:455
  76.5 8.8 %collective-permute-start.3 = (bf16[256,512]{1,0:T(8,128)(2,1)S(1)}, bf16[256,512]{1,0:T(8,128)(2,1)S(1)}, u32[]{:S(2)}, u32[]{:S(2)}) collective-permute-start(bf16[256,512]{1,0:T(8,128)(2,1)S(1)} %get-tuple-element.50.first), channel_id=1, source_target_pairs={{0,1},{1,2},{2,3},{3,0},{4,5},{5,6},{6,7},{7,4},{8,9},{9,10},{10,1... | collective-permute-start | bytes 786440 | tf_op jit(solution)/shard_map/ppermute | solution.py:333
  78.2 7.5 %collective-permute-start.6 = (bf16[256,512]{1,0:T(8,128)(2,1)S(1)}, bf16[256,512]{1,0:T(8,128)(2,1)S(1)}, u32[]{:S(2)}, u32[]{:S(2)}) collective-permute-start(bf16[256,512]{1,0:T(8,128)(2,1)S(1)} %get-tuple-element.49.last), channel_id=1, source_target_pairs={{0,3},{1,0},{2,1},{3,2},{4,7},{5,4},{6,5},{7,6},{8,11},{9,8},{10,9... | collective-permute-start | bytes 786440 | tf_op jit(solution)/shard_map/ppermute | solution.py:333
  85.2 11.1 %collective-permute-start.7 = (bf16[256,512]{1,0:T(8,128)(2,1)S(1)}, bf16[256,512]{1,0:T(8,128)(2,1)S(1)}, u32[]{:S(2)}, u32[]{:S(2)}) collective-permute-start(bf16[256,512]{1,0:T(8,128)(2,1)S(1)} %collective-permute-done.3.refs_0_), channel_id=1, source_target_pairs={{0,1},{1,2},{2,3},{3,0},{4,5},{5,6},{6,7},{7,4},{8,9},{9,10},{10,1... | collective-permute-start | bytes 786440 | tf_op jit(solution)/shard_map/ppermute | solution.py:333
  85.7 10.6 %collective-permute-start.8 = (bf16[256,512]{1,0:T(8,128)(2,1)S(1)}, bf16[256,512]{1,0:T(8,128)(2,1)S(1)}, u32[]{:S(2)}, u32[]{:S(2)}) collective-permute-start(bf16[256,512]{1,0:T(8,128)(2,1)S(1)} %collective-permute-done.6.refs_3_), channel_id=1, source_target_pairs={{0,3},{1,0},{2,1},{3,2},{4,7},{5,4},{6,5},{7,6},{8,11},{9,8},{10,9... | collective-permute-start | bytes 786440 | tf_op jit(solution)/shard_map/ppermute | solution.py:333
  87.9 14.0 %collective-permute-start.4 = (bf16[256,512]{1,0:T(8,128)(2,1)S(1)}, bf16[256,512]{1,0:T(8,128)(2,1)S(1)}, u32[]{:S(2)}, u32[]{:S(2)}) collective-permute-start(bf16[256,512]{1,0:T(8,128)(2,1)S(1)} %get-tuple-element.49.last), channel_id=1, source_target_pairs={{0,1},{1,2},{2,3},{3,0},{4,5},{5,6},{6,7},{7,4},{8,9},{9,10},{10,1... | collective-permute-start | bytes 786440 | tf_op jit(solution)/shard_map/ppermute | solution.py:333
  87.9 14.0 %collective-permute-start.5 = (bf16[256,512]{1,0:T(8,128)(2,1)S(1)}, bf16[256,512]{1,0:T(8,128)(2,1)S(1)}, u32[]{:S(2)}, u32[]{:S(2)}) collective-permute-start(bf16[256,512]{1,0:T(8,128)(2,1)S(1)} %get-tuple-element.50.first), channel_id=1, source_target_pairs={{0,3},{1,0},{2,1},{3,2},{4,7},{5,4},{6,5},{7,6},{8,11},{9,8},{10,9... | collective-permute-start | bytes 786440 | tf_op jit(solution)/shard_map/ppermute | solution.py:333
  99.1 7.7 %collective-permute-start.9 = (bf16[256,512]{1,0:T(8,128)(2,1)S(1)}, bf16[256,512]{1,0:T(8,128)(2,1)S(1)}, u32[]{:S(2)}, u32[]{:S(2)}) collective-permute-start(bf16[256,512]{1,0:T(8,128)(2,1)S(1)} %get-tuple-element.41), channel_id=1, source_target_pairs={{0,1},{1,2},{2,3},{3,0},{4,5},{5,6},{6,7},{7,4},{8,9},{9,10},{10,1... | collective-permute-start | bytes 786440 | tf_op jit(solution)/shard_map/ppermute | solution.py:333
  99.2 9.3 %collective-permute-start.13 = (bf16[256,512]{1,0:T(8,128)(2,1)S(1)}, bf16[256,512]{1,0:T(8,128)(2,1)S(1)}, u32[]{:S(2)}, u32[]{:S(2)}) collective-permute-start(bf16[256,512]{1,0:T(8,128)(2,1)S(1)} %get-tuple-element.46), channel_id=1, source_target_pairs={{0,3},{1,0},{2,1},{3,2},{4,7},{5,4},{6,5},{7,6},{8,11},{9,8},{10,9... | collective-permute-start | bytes 786440 | tf_op jit(solution)/shard_map/ppermute | solution.py:333
  106.7 38.5 %copy-start.4 = (f32[2048]{0:T(1024)S(1)}, f32[2048]{0:T(1024)}, u32[]{:S(2)}) copy-start(f32[2048]{0:T(1024)} %param.34) | copy-start | bytes 24580
  106.7 5.3 %collective-permute-start.11 = (bf16[256,512]{1,0:T(8,128)(2,1)S(1)}, bf16[256,512]{1,0:T(8,128)(2,1)S(1)}, u32[]{:S(2)}, u32[]{:S(2)}) collective-permute-start(bf16[256,512]{1,0:T(8,128)(2,1)S(1)} %get-tuple-element.42), channel_id=1, source_target_pairs={{0,3},{1,0},{2,1},{3,2},{4,7},{5,4},{6,5},{7,6},{8,11},{9,8},{10,9... | collective-permute-start | bytes 786440 | tf_op jit(solution)/shard_map/ppermute | solution.py:333
  106.9 6.5 %collective-permute-start.10 = (bf16[256,512]{1,0:T(8,128)(2,1)S(1)}, bf16[256,512]{1,0:T(8,128)(2,1)S(1)}, u32[]{:S(2)}, u32[]{:S(2)}) collective-permute-start(bf16[256,512]{1,0:T(8,128)(2,1)S(1)} %add_convert_fusion.3), channel_id=1, source_target_pairs={{0,1},{1,2},{2,3},{3,0},{4,5},{5,6},{6,7},{7,4},{8,9},{9,10},{10,1... | collective-permute-start | bytes 786440 | tf_op jit(solution)/shard_map/ppermute | solution.py:333
  108.4 10.1 %collective-permute-start.12 = (bf16[256,512]{1,0:T(8,128)(2,1)S(1)}, bf16[256,512]{1,0:T(8,128)(2,1)S(1)}, u32[]{:S(2)}, u32[]{:S(2)}) collective-permute-start(bf16[256,512]{1,0:T(8,128)(2,1)S(1)} %get-tuple-element.44), channel_id=1, source_target_pairs={{0,1},{1,2},{2,3},{3,0},{4,5},{5,6},{6,7},{7,4},{8,9},{9,10},{10,1... | collective-permute-start | bytes 786440 | tf_op jit(solution)/shard_map/ppermute | solution.py:333
  108.6 10.0 %collective-permute-start.14 = (bf16[256,512]{1,0:T(8,128)(2,1)S(1)}, bf16[256,512]{1,0:T(8,128)(2,1)S(1)}, u32[]{:S(2)}, u32[]{:S(2)}) collective-permute-start(bf16[256,512]{1,0:T(8,128)(2,1)S(1)} %add_convert_fusion.1), channel_id=1, source_target_pairs={{0,3},{1,0},{2,1},{3,2},{4,7},{5,4},{6,5},{7,6},{8,11},{9,8},{10,9... | collective-permute-start | bytes 786440 | tf_op jit(solution)/shard_map/ppermute | solution.py:333

commit v2 on v1

--- a/solution.py
+++ b/solution.py
@@ -8,15 +8,14 @@
 
 F32 = jnp.float32
 BF16 = jnp.bfloat16
-EXACT = lax.Precision.HIGHEST
 EPS = 1e-06
 STEP_LIMIT = 300.0
 MESSAGE = (8, 256)
 
 
-def dot(first, second, over=(1, 0), precision=None):
+def dot(first, second, over=(1, 0)):
     dims = (((over[0],), (over[1],)), ((), ()))
-    return lax.dot_general(first, second, dims, precision=precision, preferred_element_type=F32)
+    return lax.dot_general(first, second, dims, preferred_element_type=F32)
 
 
 def iota(shape, dim):
@@ -59,39 +58,70 @@
     return jnp.where(iota(values.shape, 0) >= by, pltpu.roll(values, by, 0), fill)
 
 
+def split(values, count):
+    found = []
+    for _ in range(count):
+        found.append(values.astype(BF16))
+        values = values - found[-1].astype(F32)
+    return found
+
+
+def repeated(values, width):
+    pair = jnp.concatenate([values, values], axis=1)
+    return jnp.concatenate([pair] * (width // pair.shape[1]), axis=1)
+
+
+def read_out(state_real, state_imag, read):
+    high, low = split(jnp.concatenate([state_real, state_imag], axis=1), 2)
+    both = dot(jnp.concatenate([high, low], axis=0), read[...])
+    rows, cut = (state_real.shape[0], both.shape[1] // 2)
+    return (both[:rows, :cut] + both[:rows, cut:]) + (both[rows:, :cut] + both[rows:, cut:])
+
+
 def mixer_kernel(
     shift, inputs, log_step, decay_real, freq_imag, in_real, in_imag, out_real, out_imag, skip,
-    message, rates, read_real, read_imag, cum_real, cum_imag, local_out,
+    message, rates, read, cum_real, cum_imag, local_out,
 ):
     groups, length = shift.shape
     states = decay_real.shape[1]
     channels = in_real.shape[1]
     width = groups * states
-    own = ones_where(iota((groups, width), 1) // states == iota((groups, width), 0))
-    repeat = ones_where(iota((states, width), 1) % states == iota((states, width), 0))
+    own = iota((groups, width), 1) // states == iota((groups, width), 0)
     square = (groups, groups)
     log_column = jnp.sum(
         jnp.where(iota(square, 0) == iota(square, 1), log_step[...], 0.0), axis=1, keepdims=True
     )
     small_step = jnp.minimum(jnp.exp(log_column + shift[...]), STEP_LIMIT)
-    step = dot(small_step.T, own, precision=EXACT)
-    decay = jnp.sum(dot(decay_real[...], repeat, precision=EXACT) * own, axis=0, keepdims=True)
-    freq = jnp.sum(dot(freq_imag[...], repeat, precision=EXACT) * own, axis=0, keepdims=True)
+    step = dot(jnp.concatenate(split(small_step.T, 3), axis=0), ones_where(own, BF16))
+    step = (step[:length] + step[length : 2 * length]) + step[2 * length :]
+
+    def row(ref):
+        return jnp.sum(jnp.where(own, repeated(ref[...], width), 0.0), axis=0, keepdims=True)
+
+    decay, freq = (row(decay_real), row(freq_imag))
     rates[...] = jnp.concatenate([decay, freq, jnp.zeros((6, width), F32)], axis=0)
     wide = (groups * channels, width)
-    block = ones_where(iota(wide, 0) // channels == iota(wide, 1) // states)
-
-    def spread(ref):
-        return dot(ref[...].reshape(wide[0], states), repeat, precision=EXACT) * block
-
-    values = inputs[...].astype(F32)
-    into_real = dot(values, spread(in_real), precision=EXACT)
-    into_imag = dot(values, spread(in_imag), precision=EXACT)
-    read_real[...] = spread(out_real)
-    read_imag[...] = spread(out_imag)
+    block = iota(wide, 0) // channels == iota(wide, 1) // states
+    values = inputs[...]
+    doubled = jnp.concatenate([values, values], axis=1)
+
+    def driven(ref):
+        spread = jnp.where(block, repeated(ref[...].reshape(wide[0], states), width), 0.0)
+        return dot(doubled, jnp.concatenate(split(spread, 2), axis=0))
+
+    into_real, into_imag = (driven(in_real), driven(in_imag))
+    tall = (width, wide[0])
+    block = iota(tall, 0) // states == iota(tall, 1) // channels
+
+    def reading(ref):
+        turned = ref[...].reshape(wide[0], states).T
+        return jnp.where(block, jnp.concatenate([turned] * groups, axis=0), 0.0)
+
+    read[...] = jnp.concatenate(
+        split(jnp.concatenate([reading(out_real), -reading(out_imag)], axis=0), 2), axis=1
+    )
     inverse = 1.0 / (decay * decay + freq * freq)
-    last_real, last_imag = ([], [])
-    result = skip[...] * values
+    states_real, states_imag = ([], [])
     for start in range(0, width, 128):
         cut = slice(start, start + 128)
         a_real, a_imag = rotation(decay[:, cut], freq[:, cut], step[:, cut])
@@ -112,26 +142,24 @@
             by *= 2
         cum_real[:, cut] = a_real
         cum_imag[:, cut] = a_imag
-        last_real.append(s_real[length - 1 :])
-        last_imag.append(s_imag[length - 1 :])
-        result = result + dot(s_real, read_real[:, cut], (1, 1), EXACT)
-        result = result - dot(s_imag, read_imag[:, cut], (1, 1), EXACT)
-    local_out[...] = result
+        states_real.append(s_real)
+        states_imag.append(s_imag)
+    local_out[...] = skip[...] * values.astype(F32) + read_out(
+        jnp.concatenate(states_real, axis=1), jnp.concatenate(states_imag, axis=1), read
+    )
     rows, lanes = MESSAGE
     pick = (width, lanes)
     compress = ones_where(
-        (iota(pick, 0) == (iota(pick, 1) % groups) * states) & (iota(pick, 1) < 3 * groups)
-    )
-    total = dot(jnp.sum(step, axis=0, keepdims=True), compress, precision=EXACT)
-    first = total.astype(BF16).astype(F32)
-    second = (total - first).astype(BF16).astype(F32)
-    third = total - first - second
-    lane = iota(total.shape, 1)
+        (iota(pick, 0) == (iota(pick, 1) % groups) * states) & (iota(pick, 1) < 3 * groups), BF16
+    )
+    total = jnp.concatenate(split(jnp.sum(step, axis=0, keepdims=True), 3), axis=0)
+    first, second, third = [part[None] for part in dot(total, compress)]
+    lane = iota(first.shape, 1)
     total = jnp.where(lane < groups, first, jnp.where(lane < 2 * groups, second, third))
     per = lanes // 128
     lines = [
-        jnp.concatenate(part[k : k + per], axis=1)
-        for part in (last_real, last_imag)
+        jnp.concatenate([s[length - 1 :] for s in part[k : k + per]], axis=1)
+        for part in (states_real, states_imag)
         for k in range(0, len(part), per)
     ]
     lines.append(total)
@@ -140,7 +168,7 @@
     message[...] = jnp.broadcast_to(sent[None], message.shape)
 
 
-def carry_kernel(got, rates, read_real, read_imag, cum_real, cum_imag, local_out, mixed):
+def carry_kernel(got, rates, read, cum_real, cum_imag, local_out, mixed):
     rows, lanes = MESSAGE
     devices = got.shape[0] // rows
     width = rates.shape[1]
@@ -148,23 +176,25 @@
     states = width // groups
     mine = lax.axis_index("sp")
     decay, freq = (rates[0:1, :], rates[1:2, :])
-    pick = (devices, devices * rows)
-    everything = got[...]
-
-    def line(k):
-        return dot(ones_where(iota(pick, 1) == iota(pick, 0) * rows + k, BF16), everything)
-
     per = width // lanes
-    got_real = jnp.concatenate([line(k) for k in range(per)], axis=1)
-    got_imag = jnp.concatenate([line(per + k) for k in range(per)], axis=1)
+    used = 2 * per + 1
+    pick = (used * devices, devices * rows)
+    line, column = (iota(pick, 0), iota(pick, 1))
+    chosen = ones_where(column == (line % devices) * rows + line // devices, BF16)
+    lines = dot(chosen, got[...])
+    lines = [lines[k * devices : (k + 1) * devices] for k in range(used)]
+    got_real = jnp.concatenate(lines[:per], axis=1)
+    got_imag = jnp.concatenate(lines[per : 2 * per], axis=1)
+    square = (devices, devices)
+    between = (iota(square, 0) < iota(square, 1)) & (iota(square, 1) < mine)
+    sums = dot(ones_where(between, BF16), lines[2 * per].astype(BF16))
     wide = (lanes, width)
     spread = ones_where(
         (iota(wide, 0) < 3 * groups) & (iota(wide, 0) % groups == iota(wide, 1) // states), BF16
     )
-    steps = dot(line(2 * per).astype(BF16), spread)
-    square = (devices, devices)
-    between = ones_where((iota(square, 0) < iota(square, 1)) & (iota(square, 1) < mine))
-    elapsed = jnp.minimum(dot(between, steps, precision=EXACT), STEP_LIMIT)
+    elapsed = dot(jnp.concatenate(split(sums, 3), axis=0), spread)
+    elapsed = (elapsed[:devices] + elapsed[devices : 2 * devices]) + elapsed[2 * devices :]
+    elapsed = jnp.minimum(elapsed, STEP_LIMIT)
     weight_real, weight_imag = rotation(decay, freq, elapsed)
     earlier = iota((devices, width), 0) < mine
     weight_real = jnp.where(earlier, weight_real, 0.0)
@@ -172,14 +202,14 @@
     carry_real = jnp.sum(weight_real * got_real - weight_imag * got_imag, axis=0, keepdims=True)
     carry_imag = jnp.sum(weight_real * got_imag + weight_imag * got_real, axis=0, keepdims=True)
     c_real, c_imag = (cum_real[...], cum_imag[...])
-    result = local_out[...]
-    result = result + dot(c_real * carry_real - c_imag * carry_imag, read_real[...], (1, 1), EXACT)
-    result = result - dot(c_real * carry_imag + c_imag * carry_real, read_imag[...], (1, 1), EXACT)
+    result = local_out[...] + read_out(
+        c_real * carry_real - c_imag * carry_imag, c_real * carry_imag + c_imag * carry_real, read
+    )
     mixed[...] = jax.nn.gelu(result).astype(BF16)
 
 
 def route_kernel(ids, logits, place, weigh):
-    slots = weigh.shape[1] // 4
+    slots = ids.shape[1]
     tall = (slots, slots)
     rows = slots // 4
     member, lane = (iota(tall, 0) % rows, iota(tall, 1))
@@ -202,9 +232,10 @@
     place[...] = jnp.where(iota(long, 0) % 4 == iota(long, 1) // rows, put, 0.0).astype(BF16)
     weight = (is_first * first + is_second * (1.0 - first)) * kept
     back = (slots, slots * 4)
-    repeat = ones_where(iota(back, 1) // 4 == iota(back, 0))
-    took = dot(weight, repeat, precision=EXACT)
-    weigh[...] = jnp.where(iota(back, 1) % 4 == iota(back, 0) // rows, took, 0.0)
+    repeat = ones_where(iota(back, 1) // 4 == iota(back, 0), BF16)
+    took = dot(jnp.concatenate(split(weight, 3), axis=0), repeat)
+    fits = iota(took.shape, 1) % 4 == (iota(took.shape, 0) % slots) // rows
+    weigh[...] = jnp.where(fits, took, 0.0).astype(BF16)
 
 
 def normalized(values, gain):
@@ -230,38 +261,46 @@
     outgoing[...] = dot(place[...], stacked).astype(BF16)
 
 
-def expert_kernel(halves, weights, results, arrived=lambda which, q: None):
+def expert_kernel(halves, weights, results, arrived=None):
     gate, up, down = weights
     count = len(halves) // 2
     lines, cut = (2 * halves[0].shape[0], halves[0].shape[1])
     slots = lines // 4
-    whole = [
-        jnp.concatenate([halves[2 * k][...], halves[2 * k + 1][...]], axis=0) for k in range(count)
-    ]
-    pick = (slots, lines)
-    gate_hidden = up_hidden = None
-    for q in range(4):
-        chosen = ones_where(iota(pick, 1) == iota(pick, 0) * 4 + q, BF16)
-        part = jnp.concatenate([dot(chosen, rows).astype(BF16) for rows in whole], axis=0)
-        span = slice(q * cut, (q + 1) * cut)
-        arrived(0, q)
-        gate_part = dot(part, gate[0, span, :])
-        arrived(1, q)
-        up_part = dot(part, up[0, span, :])
-        gate_hidden = gate_part if q == 0 else gate_hidden + gate_part
-        up_hidden = up_part if q == 0 else up_hidden + up_part
+    square = (lines, lines)
+    by_quarter = ones_where(
+        iota(square, 1) == (iota(square, 0) % slots) * 4 + iota(square, 0) // slots, BF16
+    )
+    parts = []
+    for k in range(count):
+        rows = jnp.concatenate([halves[2 * k][...], halves[2 * k + 1][...]], axis=0)
+        rows = dot(by_quarter, rows).astype(BF16)
+        parts.append([rows[q * slots : (q + 1) * slots] for q in range(4)])
+    parts = [jnp.concatenate(part, axis=0) for part in zip(*parts)]
+    if arrived is None:
+        whole = jnp.concatenate(parts, axis=1)
+        gate_hidden, up_hidden = (dot(whole, gate[0]), dot(whole, up[0]))
+    else:
+        gate_hidden = up_hidden = 0.0
+        for q, part in enumerate(parts):
+            span = slice(q * cut, (q + 1) * cut)
+            arrived(0, q)
+            gate_hidden = gate_hidden + dot(part, gate[0, span, :])
+            arrived(1, q)
+            up_hidden = up_hidden + dot(part, up[0, span, :])
     active = (jax.nn.silu(gate_hidden) * up_hidden).astype(BF16)
     made = []
     for q in range(4):
-        arrived(2, q)
+        if arrived is not None:
+            arrived(2, q)
         made.append(dot(active, down[0, :, q * cut : (q + 1) * cut]).astype(BF16))
-    half = (lines // 2, lines)
+    in_lines = ones_where(
+        iota(square, 1) == (iota(square, 0) % 4) * slots + iota(square, 0) // 4, BF16
+    )
     for k in range(count):
         stacked = jnp.concatenate([m[k * slots : (k + 1) * slots] for m in made], axis=0)
-        for side in range(2):
-            line = iota(half, 0) + side * (lines // 2)
-            order = ones_where(iota(half, 1) == (line % 4) * slots + line // 4, BF16)
-            results[2 * k + side][...] = dot(order, stacked).astype(BF16)
+        product = dot(in_lines, stacked).astype(BF16)
+        results[2 * k][...] = product[: lines // 2]
+        results[2 * k + 1][...] = product[lines // 2 :]
 
 
 def own_rows_kernel(first, last, gate, up, down, made_first, made_last, *held):
@@ -290,9 +329,19 @@
     expert_kernel(refs[:count], refs[count : count + 3], refs[count + 3 : 2 * count + 3])
 
 
+def total_kernel(*refs):
+    *parts, out = refs
+    half = out.shape[0] // 2
+    for side in range(2):
+        chosen = parts[3 * side : 3 * side + 3]
+        out[side * half : (side + 1) * half, :] = sum(p[...].astype(F32) for p in chosen).astype(BF16)
+
+
 def combine_kernel(results, weigh, stream, final_gain, out):
     rows = stream.shape[0]
-    mixture = dot(weigh[...], results[...].astype(F32), precision=EXACT)
+    mixture = dot(weigh[...], results[...])
+    height = mixture.shape[0] // 3
+    mixture = (mixture[:height] + mixture[height : 2 * height]) + mixture[2 * height :]
     mixture = jnp.concatenate([mixture[q * rows : (q + 1) * rows] for q in range(4)], axis=1)
     out[...] = (stream[...].astype(F32) + normalized(mixture, final_gain[...])).astype(BF16)
 
@@ -372,14 +421,11 @@
     to_left_last = added(to_left_last, shifted(far_last, -1))
     from_left_first, from_right_last = (shifted(to_right_first, 1), shifted(to_left_last, -1))
 
-    def total(*parts):
-        return sum(part.astype(F32) for part in parts).astype(BF16)
-
-    return jnp.concatenate(
-        [
-            total(own_first, from_left_first, from_right_first),
-            total(own_last, from_left_last, from_right_last),
-        ]
+    return call(
+        total_kernel, (own.shape, BF16),
+        own_first, from_left_first, from_right_first,
+        own_last, from_left_last, from_right_last,
+        flops=10**6,
     )
 
 
@@ -411,13 +457,12 @@
     channels = mixer_input.shape[1]
     slots = 2 * devices
     gathered = [out_weight, *(shifted(out_weight, by) for by in range(1, quarters))]
-    message, rates, read_real, read_imag, cum_real, cum_imag, local_out = call(
+    message, rates, read, cum_real, cum_imag, local_out = call(
         mixer_kernel,
         [
             ((devices, *MESSAGE), BF16),
             ((8, wide), F32),
-            ((channels, wide), F32),
-            ((channels, wide), F32),
+            ((2 * wide, 2 * channels), BF16),
             ((length, wide), F32),
             ((length, wide), F32),
             ((length, channels), F32),
@@ -442,14 +487,14 @@
     got = across_sp(message)
     place, weigh = call(
         route_kernel,
-        [((4 * slots, slots), BF16), ((slots, 4 * slots), F32)],
+        [((4 * slots, slots), BF16), ((3 * slots, 4 * slots), BF16)],
         route_ids.T,
         route_logits.T,
         flops=10**8,
     )
     mixed = call(
         carry_kernel, ((length, channels), BF16),
-        got.reshape(-1, MESSAGE[1]), rates, read_real, read_imag, cum_real, cum_imag, local_out,
+        got.reshape(-1, MESSAGE[1]), rates, read, cum_real, cum_imag, local_out,
         flops=10**9,
     )
     tokens = lax.all_to_all(

time: 147 us -> 144 us (0.980)
  Pallas kernels: 24.6 us -> 21.1 us
    pallas_call x8 -> x9, Pallas kernels: 24.6 us -> 21.1 us  [call(): pl.pallas_call(kernel, out_shape=shapes, in_specs=[left if k in in_place...]
  transfers between devices with their start and end apart: 17 -> 17, of which waited for: 7 -> 8; matrix products, arithmetic and copies ran while one was open for 0% -> 0% of each run, Pallas kernels for 11% -> 10%
where the time goes in v2:
time: 144 us
  blocking collectives  56.4 us (39%)
  starting transfers between devices  36.1 us (25%)
  waiting for transfers between devices  28.2 us (20%)
  Pallas kernels  21.1 us (15%)
  local copies, waits for them, and re-layouts  1.71 us (1%)
    all_to_all x2, blocking collectives, across_sp(): return lax.all_to_all(pieces, 'sp', split_axis=0, concat_axis=0, tiled=True)  56.4 us
    pallas_call x9, Pallas kernels, call(): pl.pallas_call(kernel, out_shape=shapes, in_specs=[left if k in in_place...  21.1 us
    ppermute x15, waiting for transfers between devices, shifted(): return lax.ppermute(part, 'tp', [(i, (i + by) % size) for i in range(size)])  19.8 us
    ppermute x15, starting transfers between devices, shifted(): return lax.ppermute(part, 'tp', [(i, (i + by) % size) for i in range(size)])  18.9 us
    all_to_all x1, starting transfers between devices, across_sp(): return lax.all_to_all(pieces, 'sp', split_axis=0, concat_axis=0, tiled=True)  13 us
    all_to_all x1, waiting for transfers between devices, across_sp(): return lax.all_to_all(pieces, 'sp', split_axis=0, concat_axis=0, tiled=True)  8 us
    all_to_all x1, starting transfers between devices, on_device(): lax.all_to_all(mixed.reshape(quarters, rows, channels), 'tp', split_axis=...  4.18 us
  transfers between devices with their start and end apart: 17, of which 8 were waited for; matrix products, arithmetic and copies ran while one was open for 0% of the time, Pallas kernels for 10%

profile of v2, /device:TPU:1, one launch (start us, length us, event | category | flops | bytes accessed | tf_op | source)
XLA Modules:
  0.0 143.7 jit_solution(16534533679434389140)
XLA Ops:
  0.0 4.1 %shard_map.190 = (bf16[64,8,256]{2,1,0:T(8,128)(2,1)}, f32[8,512]{1,0:T(8,128)S(1)}, bf16[1024,256]{1,0:T(8,128)(2,1)S(1)}, f32[128,512]{1,0:T(8,128)S(1)}, f32[...) custom-call(f32[8,128]{1,0:T(8,128)} %bitcast.32, bf16[128,128]{1,0:T(8,128)(2,1)} %inputs.1, f32[1,8]{1,0:T(1,128)} %bitcast.33, ...), custom_call_target="tpu_custom_call" | custom-call | flops 1000000000 | tf_op jit(solution)/shard_map/pallas_call | solution.py:357
  4.1 0.7 copy-done.7
  4.8 13.0 %all-to-all-start = ((bf16[64,8,256]{2,1,0:T(8,128)(2,1)}), bf16[64,8,256]{2,1,0:T(8,128)(2,1)S(1)}, u32[]{:S(2)}, u32[]{:S(2)}) async-start(bf16[64,8,256]{2,1,0:T(8,128)(2,1)} %get-tuple-element.26), calls=%async_computation | async-start | bytes 524288 | tf_op jit(solution)/shard_map/all_to_all | solution.py:377
  17.8 1.4 collective-permute-start
  19.2 2.6 %collective-permute-start.1 = (bf16[128,2048]{1,0:T(8,128)(2,1)S(1)}, bf16[128,2048]{1,0:T(8,128)(2,1)S(1)}, u32[]{:S(2)}, u32[]{:S(2)}) collective-permute-start(bf16[128,2048]{1,0:T(8,128)(2,1)S(1)} %copy-done), channel_id=1, source_target_pairs={{0,2},{1,3},{2,0},{3,1},{4,6},{5,7},{6,4},{7,5},{8,10},{9,11},{10,... | collective-permute-start | bytes 1572872 | tf_op jit(solution)/shard_map/ppermute | solution.py:382
  21.8 1.1 collective-permute-start.2
  22.9 8.0 %all-to-all-done = bf16[64,8,256]{2,1,0:T(8,128)(2,1)S(1)} async-done(((bf16[64,8,256]{2,1,0:T(8,128)(2,1)}), bf16[64,8,256]{2,1,0:T(8,128)(2,1)S(1)}, u32[]{:S(2)}, u32[]{:S(2)}) %all-to-all-start) | async-done | bytes 262176 | tf_op jit(solution)/shard_map/all_to_all | solution.py:377
  30.9 0.9 copy-done.8
  31.8 1.8 %shard_map.191 = bf16[128,128]{1,0:T(8,128)(2,1)} custom-call(bf16[512,256]{1,0:T(8,128)(2,1)S(1)} %bitcast.23, f32[8,512]{1,0:T(8,128)S(1)} %get-tuple-element.27.rates, bf16[1024,256]{1,0:T(8,128)(2,1)S(1)} %get-tuple-element.28.read, f32[128,512]{1,0:T(8,128)S(1)} %get-tuple-element.29.cum_real, f32[128,512]{1,0:T(8,128)S(1)} %copy-done.8, ...), custom_call_target="tpu_custom_call" | custom-call | flops 1000000000 | tf_op jit(solution)/shard_map/pallas_call | solution.py:357
  33.6 4.2 %all-to-all-start.1 = ((bf16[4,32,128]{2,1,0:T(8,128)(2,1)}), bf16[4,32,128]{2,1,0:T(8,128)(2,1)S(1)}, u32[]{:S(2)}, u32[]{:S(2)}) async-start(bf16[4,32,128]{2,1,0:T(8,128)(2,1)} %bitcast.6), calls=%async_computation.1 | async-start | bytes 65536 | tf_op jit(solution)/shard_map/all_to_all | solution.py:500
  37.8 0.5 shard_map.192
  38.4 0.0 collective-permute-done.weight_1
  38.4 6.3 %collective-permute-done.1.weight_2 = bf16[128,2048]{1,0:T(8,128)(2,1)S(1)} collective-permute-done((bf16[128,2048]{1,0:T(8,128)(2,1)S(1)}, bf16[128,2048]{1,0:T(8,128)(2,1)S(1)}, u32[]{:S(2)}, u32[]{:S(2)}) %collective-permute-start.1) | collective-permute-done | bytes 524320 | tf_op jit(solution)/shard_map/ppermute | solution.py:382
  44.7 0.0 collective-permute-done.2.weight_3
  44.7 0.3 all-to-all-done.1
  45.0 0.9 shard_map.193
  45.9 28.7 %all_to_all.20 = bf16[64,8,512]{2,1,0:T(8,128)(2,1)S(1)} all-to-all(bf16[64,8,512]{2,1,0:T(8,128)(2,1)S(1)} %bitcast.21), channel_id=1, replica_groups=mesh['sp'=64,'tp'=4] {'sp'}, dimensions={0} | all-to-all | bytes 1048576 | tf_op jit(solution)/shard_map/all_to_all | solution.py:377
  74.7 1.7 %collective-permute-start.3 = (bf16[256,512]{1,0:T(8,128)(2,1)S(1)}, bf16[256,512]{1,0:T(8,128)(2,1)S(1)}, u32[]{:S(2)}, u32[]{:S(2)}) collective-permute-start(bf16[256,512]{1,0:T(8,128)(2,1)S(1)} %get-tuple-element.48.first), channel_id=1, source_target_pairs={{0,1},{1,2},{2,3},{3,0},{4,5},{5,6},{6,7},{7,4},{8,9},{9,10},{10,1... | collective-permute-start | bytes 786440 | tf_op jit(solution)/shard_map/ppermute | solution.py:382
  76.4 1.0 collective-permute-start.6
  77.4 6.0 %collective-permute-done.3.refs_0_ = bf16[256,512]{1,0:T(8,128)(2,1)S(1)} collective-permute-done((bf16[256,512]{1,0:T(8,128)(2,1)S(1)}, bf16[256,512]{1,0:T(8,128)(2,1)S(1)}, u32[]{:S(2)}, u32[]{:S(2)}) %collective-permute-start.3) | collective-permute-done | bytes 262176 | tf_op jit(solution)/shard_map/ppermute | solution.py:382
  83.4 0.4 collective-permute-start.7
  83.9 0.0 collective-permute-done.6.refs_3_
  83.9 2.2 %collective-permute-start.8 = (bf16[256,512]{1,0:T(8,128)(2,1)S(1)}, bf16[256,512]{1,0:T(8,128)(2,1)S(1)}, u32[]{:S(2)}, u32[]{:S(2)}) collective-permute-start(bf16[256,512]{1,0:T(8,128)(2,1)S(1)} %collective-permute-done.6.refs_3_), channel_id=1, source_target_pairs={{0,3},{1,0},{2,1},{3,2},{4,7},{5,4},{6,5},{7,6},{8,11},{9,8},{10,9... | collective-permute-start | bytes 786440 | tf_op jit(solution)/shard_map/ppermute | solution.py:382
  86.1 0.0 collective-permute-start.4
  86.1 2.7 %collective-permute-start.5 = (bf16[256,512]{1,0:T(8,128)(2,1)S(1)}, bf16[256,512]{1,0:T(8,128)(2,1)S(1)}, u32[]{:S(2)}, u32[]{:S(2)}) collective-permute-start(bf16[256,512]{1,0:T(8,128)(2,1)S(1)} %get-tuple-element.48.first), channel_id=1, source_target_pairs={{0,3},{1,0},{2,1},{3,2},{4,7},{5,4},{6,5},{7,6},{8,11},{9,8},{10,9... | collective-permute-start | bytes 786440 | tf_op jit(solution)/shard_map/ppermute | solution.py:382
  88.8 5.5 %shard_map.194 = (bf16[256,512]{1,0:T(8,128)(2,1)S(1)}, bf16[256,512]{1,0:T(8,128)(2,1)S(1)}, bf16[1,2048,896]{2,1,0:T(8,128)(2,1)S(1)}, bf16[1,2048,896]{2,1,0:T(8,128)(2,1)S(1)}, bf16[1,896,2048]{2,1,0:T(8,128)(2,1)S(1)}) custom-call(bf16[256,512]{1,0:T(8,128)(2,1)S(1)} %get-tuple-element.48.first, bf16[256,512]{1,0:T(8,128)(2,1)S(1)} %get-tuple-element.47.last, ...), custom_call_target="tpu_custom_call" | custom-call | flops 1409286144 | tf_op jit(solution)/shard_map/pallas_call | solution.py:357
  94.3 0.0 collective-permute-done.7.refs_0_
  94.3 0.0 collective-permute-done.8.refs_1_
  94.3 2.4 %shard_map.196 = (bf16[256,512]{1,0:T(8,128)(2,1)S(1)}, bf16[256,512]{1,0:T(8,128)(2,1)S(1)}) custom-call(bf16[256,512]{1,0:T(8,128)(2,1)S(1)} %collective-permute-done.7.refs_0_, bf16[256,512]{1,0:T(8,128)(2,1)S(1)} %collective-permute-done.8.refs_1_, bf16[1,2048,896]{2,1,0:T(8,128)(2,1)S(1)} %get-tuple-element.35.refs_4_.refs_2_, ...), custom_call_target="tpu_custom_call" | custom-call | flops 1409286144 | tf_op jit(solution)/shard_map/pallas_call | solution.py:357
  96.7 0.1 collective-permute-start.13
  96.8 1.5 %collective-permute-start.9 = (bf16[256,512]{1,0:T(8,128)(2,1)S(1)}, bf16[256,512]{1,0:T(8,128)(2,1)S(1)}, u32[]{:S(2)}, u32[]{:S(2)}) collective-permute-start(bf16[256,512]{1,0:T(8,128)(2,1)S(1)} %get-tuple-element.39), channel_id=1, source_target_pairs={{0,1},{1,2},{2,3},{3,0},{4,5},{5,6},{6,7},{7,4},{8,9},{9,10},{10,1... | collective-permute-start | bytes 786440 | tf_op jit(solution)/shard_map/ppermute | solution.py:382
  98.2 0.0 collective-permute-done.5.refs_2_
  98.2 4.5 %shard_map.195 = (bf16[256,512]{1,0:T(8,128)(2,1)S(1)}, bf16[256,512]{1,0:T(8,128)(2,1)S(1)}, bf16[256,512]{1,0:T(8,128)(2,1)S(1)}, bf16[256,512]{1,0:T(8,128)(2,1)S(1)}) custom-call(bf16[256,512]{1,0:T(8,128)(2,1)S(1)} %collective-permute-done.3.refs_0_, bf16[256,512]{1,0:T(8,128)(2,1)S(1)} %collective-permute-done.4.refs_1_, ...), custom_call_target="tpu_custom_call" | custom-call | flops 2818572288 | tf_op jit(solution)/shard_map/pallas_call | solution.py:357
  102.8 0.0 copy-start.4
  102.8 1.4 collective-permute-start.11
  104.2 0.2 collective-permute-start.12
  104.3 0.1 add_convert_fusion
  104.4 2.6 %collective-permute-start.14 = (bf16[256,512]{1,0:T(8,128)(2,1)S(1)}, bf16[256,512]{1,0:T(8,128)(2,1)S(1)}, u32[]{:S(2)}, u32[]{:S(2)}) collective-permute-start(bf16[256,512]{1,0:T(8,128)(2,1)S(1)} %add_convert_fusion), channel_id=1, source_target_pairs={{0,3},{1,0},{2,1},{3,2},{4,7},{5,4},{6,5},{7,6},{8,11},{9,8},{10,9... | collective-permute-start | bytes 786440 | tf_op jit(solution)/shard_map/ppermute | solution.py:382
  107.0 0.0 collective-permute-done.9
  107.0 0.1 add_convert_fusion.1
  107.1 0.1 collective-permute-start.10
  107.2 0.9 collective-permute-done.11.refs_2_
  108.1 2.5 %collective-permute-done.12.refs_4_ = bf16[256,512]{1,0:T(8,128)(2,1)S(1)} collective-permute-done((bf16[256,512]{1,0:T(8,128)(2,1)S(1)}, bf16[256,512]{1,0:T(8,128)(2,1)S(1)}, u32[]{:S(2)}, u32[]{:S(2)}) %collective-permute-start.12) | collective-permute-done | bytes 262176 | tf_op jit(solution)/shard_map/ppermute | solution.py:382
  110.6 2.8 %collective-permute-done.14.refs_5_ = bf16[256,512]{1,0:T(8,128)(2,1)S(1)} collective-permute-done((bf16[256,512]{1,0:T(8,128)(2,1)S(1)}, bf16[256,512]{1,0:T(8,128)(2,1)S(1)}, u32[]{:S(2)}, u32[]{:S(2)}) %collective-permute-start.14) | collective-permute-done | bytes 262176 | tf_op jit(solution)/shard_map/ppermute | solution.py:382
  113.4 1.3 collective-permute-done.10.refs_1_
  114.7 0.2 shard_map.197
  114.9 27.7 %all_to_all.21 = bf16[64,8,512]{2,1,0:T(8,128)(2,1)S(1)} all-to-all(bf16[64,8,512]{2,1,0:T(8,128)(2,1)S(1)} %bitcast.20), channel_id=1, replica_groups=mesh['sp'=64,'tp'=4] {'sp'}, dimensions={0} | all-to-all | bytes 1048576 | tf_op jit(solution)/shard_map/all_to_all | solution.py:377
  142.6 1.2 shard_map.198
  (18 shorter events, 0.1 us)
Async XLA Ops:
  0.0 17.8 %copy-start = (bf16[128,2048]{1,0:T(8,128)(2,1)S(1)}, bf16[128,2048]{1,0:T(8,128)(2,1)}, u32[]{:S(2)}) copy-start(bf16[128,2048]{1,0:T(8,128)(2,1)} %weight_0.1) | copy-start | bytes 1572868
  0.0 37.8 %copy-start.5 = (s32[128,2]{0,1:T(2,128)S(1)}, s32[128,2]{0,1:T(2,128)}, u32[]{:S(2)}) copy-start(s32[128,2]{0,1:T(2,128)} %param.35) | copy-start | bytes 3076
  0.0 37.8 %copy-start.6 = (f32[128,2]{0,1:T(2,128)S(1)}, f32[128,2]{0,1:T(2,128)}, u32[]{:S(2)}) copy-start(f32[128,2]{0,1:T(2,128)} %param.36) | copy-start | bytes 3076
  0.0 45.0 %copy-start.1 = (bf16[32,2048]{1,0:T(8,128)(2,1)S(1)}, bf16[32,2048]{1,0:T(8,128)(2,1)}, u32[]{:S(2)}) copy-start(bf16[32,2048]{1,0:T(8,128)(2,1)} %residual.1) | copy-start | bytes 393220
  0.0 45.0 %copy-start.2 = (f32[2048]{0:T(1024)S(1)}, f32[2048]{0:T(1024)}, u32[]{:S(2)}) copy-start(f32[2048]{0:T(1024)} %param.32) | copy-start | bytes 24580
  0.0 45.0 %copy-start.3 = (f32[2048]{0:T(1024)S(1)}, f32[2048]{0:T(1024)}, u32[]{:S(2)}) copy-start(f32[2048]{0:T(1024)} %param.33) | copy-start | bytes 24580
  4.1 0.7 copy-start.7
  4.8 26.1 %all-to-all-start = ((bf16[64,8,256]{2,1,0:T(8,128)(2,1)}), bf16[64,8,256]{2,1,0:T(8,128)(2,1)S(1)}, u32[]{:S(2)}, u32[]{:S(2)}) async-start(bf16[64,8,256]{2,1,0:T(8,128)(2,1)} %get-tuple-element.26), calls=%async_computation | async-start | bytes 524288 | tf_op jit(solution)/shard_map/all_to_all | solution.py:377
  17.8 20.5 %collective-permute-start = (bf16[128,2048]{1,0:T(8,128)(2,1)S(1)}, bf16[128,2048]{1,0:T(8,128)(2,1)S(1)}, u32[]{:S(2)}, u32[]{:S(2)}) collective-permute-start(bf16[128,2048]{1,0:T(8,128)(2,1)S(1)} %copy-done), channel_id=1, source_target_pairs={{0,1},{1,2},{2,3},{3,0},{4,5},{5,6},{6,7},{7,4},{8,9},{9,10},{10,1... | collective-permute-start | bytes 1572872 | tf_op jit(solution)/shard_map/ppermute | solution.py:382
  19.2 25.5 %collective-permute-start.1 = (bf16[128,2048]{1,0:T(8,128)(2,1)S(1)}, bf16[128,2048]{1,0:T(8,128)(2,1)S(1)}, u32[]{:S(2)}, u32[]{:S(2)}) collective-permute-start(bf16[128,2048]{1,0:T(8,128)(2,1)S(1)} %copy-done), channel_id=1, source_target_pairs={{0,2},{1,3},{2,0},{3,1},{4,6},{5,7},{6,4},{7,5},{8,10},{9,11},{10,... | collective-permute-start | bytes 1572872 | tf_op jit(solution)/shard_map/ppermute | solution.py:382
  21.8 22.8 %collective-permute-start.2 = (bf16[128,2048]{1,0:T(8,128)(2,1)S(1)}, bf16[128,2048]{1,0:T(8,128)(2,1)S(1)}, u32[]{:S(2)}, u32[]{:S(2)}) collective-permute-start(bf16[128,2048]{1,0:T(8,128)(2,1)S(1)} %copy-done), channel_id=1, source_target_pairs={{0,3},{1,0},{2,1},{3,2},{4,7},{5,4},{6,5},{7,6},{8,11},{9,8},{10,9... | collective-permute-start | bytes 1572872 | tf_op jit(solution)/shard_map/ppermute | solution.py:382
  30.9 1.0 copy-start.8
  33.6 11.4 %all-to-all-start.1 = ((bf16[4,32,128]{2,1,0:T(8,128)(2,1)}), bf16[4,32,128]{2,1,0:T(8,128)(2,1)S(1)}, u32[]{:S(2)}, u32[]{:S(2)}) async-start(bf16[4,32,128]{2,1,0:T(8,128)(2,1)} %bitcast.6), calls=%async_computation.1 | async-start | bytes 65536 | tf_op jit(solution)/shard_map/all_to_all | solution.py:500
  74.7 8.8 %collective-permute-start.3 = (bf16[256,512]{1,0:T(8,128)(2,1)S(1)}, bf16[256,512]{1,0:T(8,128)(2,1)S(1)}, u32[]{:S(2)}, u32[]{:S(2)}) collective-permute-start(bf16[256,512]{1,0:T(8,128)(2,1)S(1)} %get-tuple-element.48.first), channel_id=1, source_target_pairs={{0,1},{1,2},{2,3},{3,0},{4,5},{5,6},{6,7},{7,4},{8,9},{9,10},{10,1... | collective-permute-start | bytes 786440 | tf_op jit(solution)/shard_map/ppermute | solution.py:382
  76.4 7.5 %collective-permute-start.6 = (bf16[256,512]{1,0:T(8,128)(2,1)S(1)}, bf16[256,512]{1,0:T(8,128)(2,1)S(1)}, u32[]{:S(2)}, u32[]{:S(2)}) collective-permute-start(bf16[256,512]{1,0:T(8,128)(2,1)S(1)} %get-tuple-element.47.last), channel_id=1, source_target_pairs={{0,3},{1,0},{2,1},{3,2},{4,7},{5,4},{6,5},{7,6},{8,11},{9,8},{10,9... | collective-permute-start | bytes 786440 | tf_op jit(solution)/shard_map/ppermute | solution.py:382
  83.4 10.8 %collective-permute-start.7 = (bf16[256,512]{1,0:T(8,128)(2,1)S(1)}, bf16[256,512]{1,0:T(8,128)(2,1)S(1)}, u32[]{:S(2)}, u32[]{:S(2)}) collective-permute-start(bf16[256,512]{1,0:T(8,128)(2,1)S(1)} %collective-permute-done.3.refs_0_), channel_id=1, source_target_pairs={{0,1},{1,2},{2,3},{3,0},{4,5},{5,6},{6,7},{7,4},{8,9},{9,10},{10,1... | collective-permute-start | bytes 786440 | tf_op jit(solution)/shard_map/ppermute | solution.py:382
  83.9 10.4 %collective-permute-start.8 = (bf16[256,512]{1,0:T(8,128)(2,1)S(1)}, bf16[256,512]{1,0:T(8,128)(2,1)S(1)}, u32[]{:S(2)}, u32[]{:S(2)}) collective-permute-start(bf16[256,512]{1,0:T(8,128)(2,1)S(1)} %collective-permute-done.6.refs_3_), channel_id=1, source_target_pairs={{0,3},{1,0},{2,1},{3,2},{4,7},{5,4},{6,5},{7,6},{8,11},{9,8},{10,9... | collective-permute-start | bytes 786440 | tf_op jit(solution)/shard_map/ppermute | solution.py:382
  86.1 12.1 %collective-permute-start.4 = (bf16[256,512]{1,0:T(8,128)(2,1)S(1)}, bf16[256,512]{1,0:T(8,128)(2,1)S(1)}, u32[]{:S(2)}, u32[]{:S(2)}) collective-permute-start(bf16[256,512]{1,0:T(8,128)(2,1)S(1)} %get-tuple-element.47.last), channel_id=1, source_target_pairs={{0,1},{1,2},{2,3},{3,0},{4,5},{5,6},{6,7},{7,4},{8,9},{9,10},{10,1... | collective-permute-start | bytes 786440 | tf_op jit(solution)/shard_map/ppermute | solution.py:382
  86.1 12.1 %collective-permute-start.5 = (bf16[256,512]{1,0:T(8,128)(2,1)S(1)}, bf16[256,512]{1,0:T(8,128)(2,1)S(1)}, u32[]{:S(2)}, u32[]{:S(2)}) collective-permute-start(bf16[256,512]{1,0:T(8,128)(2,1)S(1)} %get-tuple-element.48.first), channel_id=1, source_target_pairs={{0,3},{1,0},{2,1},{3,2},{4,7},{5,4},{6,5},{7,6},{8,11},{9,8},{10,9... | collective-permute-start | bytes 786440 | tf_op jit(solution)/shard_map/ppermute | solution.py:382
  96.7 7.6 %collective-permute-start.13 = (bf16[256,512]{1,0:T(8,128)(2,1)S(1)}, bf16[256,512]{1,0:T(8,128)(2,1)S(1)}, u32[]{:S(2)}, u32[]{:S(2)}) collective-permute-start(bf16[256,512]{1,0:T(8,128)(2,1)S(1)} %get-tuple-element.44), channel_id=1, source_target_pairs={{0,3},{1,0},{2,1},{3,2},{4,7},{5,4},{6,5},{7,6},{8,11},{9,8},{10,9... | collective-permute-start | bytes 786440 | tf_op jit(solution)/shard_map/ppermute | solution.py:382
  96.8 10.2 %collective-permute-start.9 = (bf16[256,512]{1,0:T(8,128)(2,1)S(1)}, bf16[256,512]{1,0:T(8,128)(2,1)S(1)}, u32[]{:S(2)}, u32[]{:S(2)}) collective-permute-start(bf16[256,512]{1,0:T(8,128)(2,1)S(1)} %get-tuple-element.39), channel_id=1, source_target_pairs={{0,1},{1,2},{2,3},{3,0},{4,5},{5,6},{6,7},{7,4},{8,9},{9,10},{10,1... | collective-permute-start | bytes 786440 | tf_op jit(solution)/shard_map/ppermute | solution.py:382
  102.8 39.8 %copy-start.4 = (f32[2048]{0:T(1024)S(1)}, f32[2048]{0:T(1024)}, u32[]{:S(2)}) copy-start(f32[2048]{0:T(1024)} %param.34) | copy-start | bytes 24580
  102.8 5.3 %collective-permute-start.11 = (bf16[256,512]{1,0:T(8,128)(2,1)S(1)}, bf16[256,512]{1,0:T(8,128)(2,1)S(1)}, u32[]{:S(2)}, u32[]{:S(2)}) collective-permute-start(bf16[256,512]{1,0:T(8,128)(2,1)S(1)} %get-tuple-element.40), channel_id=1, source_target_pairs={{0,3},{1,0},{2,1},{3,2},{4,7},{5,4},{6,5},{7,6},{8,11},{9,8},{10,9... | collective-permute-start | bytes 786440 | tf_op jit(solution)/shard_map/ppermute | solution.py:382
  104.2 6.4 %collective-permute-start.12 = (bf16[256,512]{1,0:T(8,128)(2,1)S(1)}, bf16[256,512]{1,0:T(8,128)(2,1)S(1)}, u32[]{:S(2)}, u32[]{:S(2)}) collective-permute-start(bf16[256,512]{1,0:T(8,128)(2,1)S(1)} %get-tuple-element.42), channel_id=1, source_target_pairs={{0,1},{1,2},{2,3},{3,0},{4,5},{5,6},{6,7},{7,4},{8,9},{9,10},{10,1... | collective-permute-start | bytes 786440 | tf_op jit(solution)/shard_map/ppermute | solution.py:382
  104.4 9.0 %collective-permute-start.14 = (bf16[256,512]{1,0:T(8,128)(2,1)S(1)}, bf16[256,512]{1,0:T(8,128)(2,1)S(1)}, u32[]{:S(2)}, u32[]{:S(2)}) collective-permute-start(bf16[256,512]{1,0:T(8,128)(2,1)S(1)} %add_convert_fusion), channel_id=1, source_target_pairs={{0,3},{1,0},{2,1},{3,2},{4,7},{5,4},{6,5},{7,6},{8,11},{9,8},{10,9... | collective-permute-start | bytes 786440 | tf_op jit(solution)/shard_map/ppermute | solution.py:382
  107.1 7.6 %collective-permute-start.10 = (bf16[256,512]{1,0:T(8,128)(2,1)S(1)}, bf16[256,512]{1,0:T(8,128)(2,1)S(1)}, u32[]{:S(2)}, u32[]{:S(2)}) collective-permute-start(bf16[256,512]{1,0:T(8,128)(2,1)S(1)} %add_convert_fusion.1), channel_id=1, source_target_pairs={{0,1},{1,2},{2,3},{3,0},{4,5},{5,6},{6,7},{7,4},{8,9},{9,10},{10,1... | collective-permute-start | bytes 786440 | tf_op jit(solution)/shard_map/ppermute | solution.py:382

commit v3 on v2

--- a/solution.py
+++ b/solution.py
@@ -168,7 +168,8 @@
     message[...] = jnp.broadcast_to(sent[None], message.shape)
 
 
-def carry_kernel(got, rates, read, cum_real, cum_imag, local_out, mixed):
+def carry_kernel(got, rates, read, cum_real, cum_imag, local_out, routed, mixed):
+    del routed
     rows, lanes = MESSAGE
     devices = got.shape[0] // rows
     width = rates.shape[1]
@@ -242,17 +243,19 @@
     return values * lax.rsqrt(jnp.mean(values * values, axis=-1, keepdims=True) + EPS) * gain
 
 
-def project_kernel(
-    tokens, weight_0, weight_1, weight_2, weight_3, residual, post_gain, pre_gain, place,
-    stream, outgoing,
-):
+def project_kernel(tokens, weight, *refs):
+    *halves, residual, post_gain, pre_gain, place, stream, outgoing = refs
     rows, width = residual.shape
     quarter = lax.axis_index("tp")
-    projected = jnp.zeros((rows, width), F32)
-    for by, weight in enumerate((weight_0, weight_1, weight_2, weight_3)):
+    projected = None
+    for by in range(4):
         source = lax.rem(quarter + 4 - by, 4)
         part = tokens[pl.ds(pl.multiple_of(source * rows, rows), rows), :]
-        projected = projected + dot(part, weight[...])
+        if by == 0:
+            projected = dot(part, weight[...])
+        else:
+            whole = jnp.concatenate([half[...] for half in halves[2 * by - 2 : 2 * by]], axis=0)
+            projected = projected + dot(part, whole)
     own = (residual[...].astype(F32) + normalized(projected, post_gain[...])).astype(BF16)
     stream[...] = own
     normed = normalized(own.astype(F32), pre_gain[...]).astype(BF16)
@@ -371,6 +374,10 @@
 
 def in_hbm(value):
     return pltpu.with_memory_space_constraint(value, pltpu.HBM)
+
+
+def in_vmem(value):
+    return pltpu.with_memory_space_constraint(value, pltpu.VMEM)
 
 
 def across_sp(pieces):
@@ -456,7 +463,15 @@
     length, wide = (mixer_input.shape[0], decay_real.size)
     channels = mixer_input.shape[1]
     slots = 2 * devices
-    gathered = [out_weight, *(shifted(out_weight, by) for by in range(1, quarters))]
+    half = channels // 2
+    first, last = (out_weight[:half], out_weight[half:])
+    behind_first, ahead_last = (shifted(first, 1), shifted(last, -1))
+    behind_last, ahead_first = (shifted(last, 1), shifted(first, -1))
+    across_first, across_last = (shifted(behind_first, 1), shifted(ahead_last, -1))
+    gathered = (
+        in_hbm(out_weight),
+        behind_first, behind_last, across_first, across_last, ahead_first, ahead_last,
+    )
     message, rates, read, cum_real, cum_imag, local_out = call(
         mixer_kernel,
         [
@@ -494,8 +509,8 @@
     )
     mixed = call(
         carry_kernel, ((length, channels), BF16),
-        got.reshape(-1, MESSAGE[1]), rates, read, cum_real, cum_imag, local_out,
-        flops=10**9,
+        got.reshape(-1, MESSAGE[1]), *map(in_vmem, (rates, read, cum_real, cum_imag, local_out)), place,
+        flops=10**9, in_place=(6,),
     )
     tokens = lax.all_to_all(
         mixed.reshape(quarters, rows, channels), "tp", split_axis=0, concat_axis=0, tiled=True

time: 144 us -> 143 us (level)
  waiting for transfers between devices: 28.2 us -> 21.7 us
  starting transfers between devices: 36.1 us -> 39.5 us
    all_to_all x1, waiting for transfers between devices: 8 us -> 0.04 us  [across_sp(): return lax.all_to_all(pieces, 'sp', split_axis=0, concat_axis=0, tiled=True)]
    ppermute x15 -> x18, starting transfers between devices: 18.9 us -> 22.2 us  [shifted(): return lax.ppermute(part, 'tp', [(i, (i + by) % size) for i in range(size)])]
    all_to_all x1, waiting for transfers between devices: 0.35 us -> 3.27 us  [on_device(): lax.all_to_all(mixed.reshape(quarters, rows, channels), 'tp', split_axis=...]
    ppermute x15 -> x18, waiting for transfers between devices: 19.8 us -> 18.3 us  [shifted(): return lax.ppermute(part, 'tp', [(i, (i + by) % size) for i in range(size)])]
  transfers between devices with their start and end apart: 17 -> 20, of which waited for: 8 -> 8; matrix products, arithmetic and copies ran while one was open for 0% -> 1% of each run, Pallas kernels for 10% -> 10%
where the time goes in v3:
time: 143 us
  blocking collectives  57.6 us (40%)
  starting transfers between devices  39.5 us (28%)
  Pallas kernels  22.1 us (15%)
  waiting for transfers between devices  21.7 us (15%)
  local copies, waits for them, and re-layouts  1.86 us (1%)
    all_to_all x2, blocking collectives, across_sp(): return lax.all_to_all(pieces, 'sp', split_axis=0, concat_axis=0, tiled=True)  57.6 us
    ppermute x18, starting transfers between devices, shifted(): return lax.ppermute(part, 'tp', [(i, (i + by) % size) for i in range(size)])  22.2 us
    pallas_call x9, Pallas kernels, call(): pl.pallas_call(kernel, out_shape=shapes, in_specs=[left if k in in_place...  22.1 us
    ppermute x18, waiting for transfers between devices, shifted(): return lax.ppermute(part, 'tp', [(i, (i + by) % size) for i in range(size)])  18.3 us
    all_to_all x1, starting transfers between devices, across_sp(): return lax.all_to_all(pieces, 'sp', split_axis=0, concat_axis=0, tiled=True)  13.1 us
    all_to_all x1, starting transfers between devices, on_device(): lax.all_to_all(mixed.reshape(quarters, rows, channels), 'tp', split_axis=...  4.18 us
    all_to_all x1, waiting for transfers between devices, on_device(): lax.all_to_all(mixed.reshape(quarters, rows, channels), 'tp', split_axis=...  3.27 us
  transfers between devices with their start and end apart: 20, of which 8 were waited for; matrix products, arithmetic and copies ran while one was open for 1% of the time, Pallas kernels for 10%

profile of v3, /device:TPU:1, one launch (start us, length us, event | category | flops | bytes accessed | tf_op | source)
XLA Modules:
  0.0 143.0 jit_solution(6459885788394120621)
XLA Ops:
  0.0 4.1 %shard_map.190 = (bf16[64,8,256]{2,1,0:T(8,128)(2,1)}, f32[8,512]{1,0:T(8,128)S(1)}, bf16[1024,256]{1,0:T(8,128)(2,1)S(1)}, f32[128,512]{1,0:T(8,128)S(1)}, f32[...) custom-call(f32[8,128]{1,0:T(8,128)} %bitcast.32, bf16[128,128]{1,0:T(8,128)(2,1)} %inputs.1, f32[1,8]{1,0:T(1,128)} %bitcast.33, ...), custom_call_target="tpu_custom_call" | custom-call | flops 1000000000 | tf_op jit(solution)/shard_map/pallas_call | solution.py:360
  4.1 0.0 copy-start.2
  4.1 13.1 %all-to-all-start = ((bf16[64,8,256]{2,1,0:T(8,128)(2,1)}), bf16[64,8,256]{2,1,0:T(8,128)(2,1)S(1)}, u32[]{:S(2)}, u32[]{:S(2)}) async-start(bf16[64,8,256]{2,1,0:T(8,128)(2,1)} %get-tuple-element.26), calls=%async_computation | async-start | bytes 524288 | tf_op jit(solution)/shard_map/all_to_all | solution.py:384
  17.3 0.8 fusion
  18.1 1.3 collective-permute-start
  19.4 1.4 %collective-permute-start.3 = (bf16[64,2048]{1,0:T(8,128)(2,1)}, bf16[64,2048]{1,0:T(8,128)(2,1)S(1)}, u32[]{:S(2)}, u32[]{:S(2)}) collective-permute-start(bf16[64,2048]{1,0:T(8,128)(2,1)} %get-tuple-element.49), channel_id=1, source_target_pairs={{0,3},{1,0},{2,1},{3,2},{4,7},{5,4},{6,5},{7,6},{8,11},{9,8},{10,9... | collective-permute-start | bytes 786440 | tf_op jit(solution)/shard_map/ppermute | solution.py:389
  20.9 0.0 collective-permute-start.1
  20.9 2.7 %collective-permute-start.5 = (bf16[64,2048]{1,0:T(8,128)(2,1)}, bf16[64,2048]{1,0:T(8,128)(2,1)S(1)}, u32[]{:S(2)}, u32[]{:S(2)}) collective-permute-start(bf16[64,2048]{1,0:T(8,128)(2,1)} %get-tuple-element.50), channel_id=1, source_target_pairs={{0,3},{1,0},{2,1},{3,2},{4,7},{5,4},{6,5},{7,6},{8,11},{9,8},{10,9... | collective-permute-start | bytes 786440 | tf_op jit(solution)/shard_map/ppermute | solution.py:389
  23.5 3.5 %collective-permute-done.refs_0_ = bf16[64,2048]{1,0:T(8,128)(2,1)S(1)} collective-permute-done((bf16[64,2048]{1,0:T(8,128)(2,1)}, bf16[64,2048]{1,0:T(8,128)(2,1)S(1)}, u32[]{:S(2)}, u32[]{:S(2)}) %collective-permute-start) | collective-permute-done | bytes 262176 | tf_op jit(solution)/shard_map/ppermute | solution.py:389
  27.1 0.0 collective-permute-start.2
  27.1 0.0 collective-permute-done.3.refs_5_
  27.1 2.7 %collective-permute-start.4 = (bf16[64,2048]{1,0:T(8,128)(2,1)S(1)}, bf16[64,2048]{1,0:T(8,128)(2,1)S(1)}, u32[]{:S(2)}, u32[]{:S(2)}) collective-permute-start(bf16[64,2048]{1,0:T(8,128)(2,1)S(1)} %collective-permute-done.3.refs_5_), channel_id=1, source_target_pairs={{0,3},{1,0},{2,1},{3,2},{4,7},{5,4},{6,5},{7,6},{8,11},{9,8},{10,9... | collective-permute-start | bytes 786440 | tf_op jit(solution)/shard_map/ppermute | solution.py:389
  29.8 0.5 shard_map.191
  30.3 0.0 all-to-all-done
  30.3 0.9 copy-done.7
  31.3 1.8 %shard_map.192 = bf16[128,128]{1,0:T(8,128)(2,1)} custom-call(bf16[512,256]{1,0:T(8,128)(2,1)S(1)} %bitcast.23, f32[8,512]{1,0:T(8,128)S(1)} %get-tuple-element.27.rates, bf16[1024,256]{1,0:T(8,128)(2,1)S(1)} %get-tuple-element.28.read, f32[128,512]{1,0:T(8,128)S(1)} %get-tuple-element.29.cum_real, f32[128,512]{1,0:T(8,128)S(1)} %copy-done.7, ...), custom_call_target="tpu_custom_call" | custom-call | flops 1000000000 | tf_op jit(solution)/shard_map/pallas_call | solution.py:360
  33.1 4.2 %all-to-all-start.1 = ((bf16[4,32,128]{2,1,0:T(8,128)(2,1)}), bf16[4,32,128]{2,1,0:T(8,128)(2,1)S(1)}, u32[]{:S(2)}, u32[]{:S(2)}) async-start(bf16[4,32,128]{2,1,0:T(8,128)(2,1)} %bitcast.8), calls=%async_computation.1 | async-start | bytes 65536 | tf_op jit(solution)/shard_map/all_to_all | solution.py:515
  37.3 1.0 collective-permute-done.2.refs_2_
  38.3 3.3 %all-to-all-done.1 = bf16[4,32,128]{2,1,0:T(8,128)(2,1)S(1)} async-done(((bf16[4,32,128]{2,1,0:T(8,128)(2,1)}), bf16[4,32,128]{2,1,0:T(8,128)(2,1)S(1)}, u32[]{:S(2)}, u32[]{:S(2)}) %all-to-all-start.1) | async-done | bytes 32800 | tf_op jit(solution)/shard_map/all_to_all | solution.py:515
  41.6 2.0 %shard_map.193 = (bf16[32,2048]{1,0:T(8,128)(2,1)S(1)}, bf16[512,512]{1,0:T(8,128)(2,1)S(1)}) custom-call(bf16[128,128]{1,0:T(8,128)(2,1)S(1)} %bitcast.24, bf16[128,2048]{1,0:T(8,128)(2,1)} %weight.1, bf16[64,2048]{1,0:T(8,128)(2,1)S(1)} %collective-permute-done.refs_0_, bf16[64,2048]{1,0:T(8,128)(2,1)S(1)} %collective-permute-done.1.refs_1_, ...), custom_call_target="tpu_custom_call" | custom-call | flops 1000000000 | tf_op jit(solution)/shard_map/pallas_call | solution.py:360
  43.6 30.2 %all_to_all.20 = bf16[64,8,512]{2,1,0:T(8,128)(2,1)S(1)} all-to-all(bf16[64,8,512]{2,1,0:T(8,128)(2,1)S(1)} %bitcast.21), channel_id=1, replica_groups=mesh['sp'=64,'tp'=4] {'sp'}, dimensions={0} | all-to-all | bytes 1048576 | tf_op jit(solution)/shard_map/all_to_all | solution.py:384
  73.8 0.4 collective-permute-start.6
  74.1 2.4 %collective-permute-start.9 = (bf16[256,512]{1,0:T(8,128)(2,1)S(1)}, bf16[256,512]{1,0:T(8,128)(2,1)S(1)}, u32[]{:S(2)}, u32[]{:S(2)}) collective-permute-start(bf16[256,512]{1,0:T(8,128)(2,1)S(1)} %get-tuple-element.47.last), channel_id=1, source_target_pairs={{0,3},{1,0},{2,1},{3,2},{4,7},{5,4},{6,5},{7,6},{8,11},{9,8},{10,9... | collective-permute-start | bytes 786440 | tf_op jit(solution)/shard_map/ppermute | solution.py:389
  76.5 6.0 %collective-permute-done.6.refs_0_ = bf16[256,512]{1,0:T(8,128)(2,1)S(1)} collective-permute-done((bf16[256,512]{1,0:T(8,128)(2,1)S(1)}, bf16[256,512]{1,0:T(8,128)(2,1)S(1)}, u32[]{:S(2)}, u32[]{:S(2)}) %collective-permute-start.6) | collective-permute-done | bytes 262176 | tf_op jit(solution)/shard_map/ppermute | solution.py:389
  82.5 0.0 collective-permute-done.9.refs_3_
  82.5 2.7 %collective-permute-start.11 = (bf16[256,512]{1,0:T(8,128)(2,1)S(1)}, bf16[256,512]{1,0:T(8,128)(2,1)S(1)}, u32[]{:S(2)}, u32[]{:S(2)}) collective-permute-start(bf16[256,512]{1,0:T(8,128)(2,1)S(1)} %collective-permute-done.9.refs_3_), channel_id=1, source_target_pairs={{0,3},{1,0},{2,1},{3,2},{4,7},{5,4},{6,5},{7,6},{8,11},{9,8},{10,9... | collective-permute-start | bytes 786440 | tf_op jit(solution)/shard_map/ppermute | solution.py:389
  85.2 0.0 collective-permute-start.7
  85.2 2.7 %collective-permute-start.8 = (bf16[256,512]{1,0:T(8,128)(2,1)S(1)}, bf16[256,512]{1,0:T(8,128)(2,1)S(1)}, u32[]{:S(2)}, u32[]{:S(2)}) collective-permute-start(bf16[256,512]{1,0:T(8,128)(2,1)S(1)} %get-tuple-element.48.first), channel_id=1, source_target_pairs={{0,3},{1,0},{2,1},{3,2},{4,7},{5,4},{6,5},{7,6},{8,11},{9,8},{10,9... | collective-permute-start | bytes 786440 | tf_op jit(solution)/shard_map/ppermute | solution.py:389
  87.9 5.4 %shard_map.194 = (bf16[256,512]{1,0:T(8,128)(2,1)S(1)}, bf16[256,512]{1,0:T(8,128)(2,1)S(1)}, bf16[1,2048,896]{2,1,0:T(8,128)(2,1)S(1)}, bf16[1,2048,896]{2,1,0:T(8,128)(2,1)S(1)}, bf16[1,896,2048]{2,1,0:T(8,128)(2,1)S(1)}) custom-call(bf16[256,512]{1,0:T(8,128)(2,1)S(1)} %get-tuple-element.48.first, bf16[256,512]{1,0:T(8,128)(2,1)S(1)} %get-tuple-element.47.last, ...), custom_call_target="tpu_custom_call" | custom-call | flops 1409286144 | tf_op jit(solution)/shard_map/pallas_call | solution.py:360
  93.3 0.0 collective-permute-done.11.refs_1_
  93.3 2.4 %shard_map.196 = (bf16[256,512]{1,0:T(8,128)(2,1)S(1)}, bf16[256,512]{1,0:T(8,128)(2,1)S(1)}) custom-call(bf16[256,512]{1,0:T(8,128)(2,1)S(1)} %collective-permute-done.10.refs_0_, bf16[256,512]{1,0:T(8,128)(2,1)S(1)} %collective-permute-done.11.refs_1_, bf16[1,2048,896]{2,1,0:T(8,128)(2,1)S(1)} %get-tuple-element.35.refs_4_.refs_2_, ...), custom_call_target="tpu_custom_call" | custom-call | flops 1409286144 | tf_op jit(solution)/shard_map/pallas_call | solution.py:360
  95.8 0.1 collective-permute-start.16
  95.9 1.5 %collective-permute-start.12 = (bf16[256,512]{1,0:T(8,128)(2,1)S(1)}, bf16[256,512]{1,0:T(8,128)(2,1)S(1)}, u32[]{:S(2)}, u32[]{:S(2)}) collective-permute-start(bf16[256,512]{1,0:T(8,128)(2,1)S(1)} %get-tuple-element.39), channel_id=1, source_target_pairs={{0,1},{1,2},{2,3},{3,0},{4,5},{5,6},{6,7},{7,4},{8,9},{9,10},{10,1... | collective-permute-start | bytes 786440 | tf_op jit(solution)/shard_map/ppermute | solution.py:389
  97.3 0.0 collective-permute-done.7.refs_1_
  97.3 4.5 %shard_map.195 = (bf16[256,512]{1,0:T(8,128)(2,1)S(1)}, bf16[256,512]{1,0:T(8,128)(2,1)S(1)}, bf16[256,512]{1,0:T(8,128)(2,1)S(1)}, bf16[256,512]{1,0:T(8,128)(2,1)S(1)}) custom-call(bf16[256,512]{1,0:T(8,128)(2,1)S(1)} %collective-permute-done.6.refs_0_, bf16[256,512]{1,0:T(8,128)(2,1)S(1)} %collective-permute-done.7.refs_1_, ...), custom_call_target="tpu_custom_call" | custom-call | flops 2818572288 | tf_op jit(solution)/shard_map/pallas_call | solution.py:360
  101.8 0.0 copy-start.3
  101.9 1.6 %collective-permute-start.14 = (bf16[256,512]{1,0:T(8,128)(2,1)S(1)}, bf16[256,512]{1,0:T(8,128)(2,1)S(1)}, u32[]{:S(2)}, u32[]{:S(2)}) collective-permute-start(bf16[256,512]{1,0:T(8,128)(2,1)S(1)} %get-tuple-element.40), channel_id=1, source_target_pairs={{0,3},{1,0},{2,1},{3,2},{4,7},{5,4},{6,5},{7,6},{8,11},{9,8},{10,9... | collective-permute-start | bytes 786440 | tf_op jit(solution)/shard_map/ppermute | solution.py:389
  103.5 0.1 add_convert_fusion
  103.5 2.8 %collective-permute-start.17 = (bf16[256,512]{1,0:T(8,128)(2,1)S(1)}, bf16[256,512]{1,0:T(8,128)(2,1)S(1)}, u32[]{:S(2)}, u32[]{:S(2)}) collective-permute-start(bf16[256,512]{1,0:T(8,128)(2,1)S(1)} %add_convert_fusion), channel_id=1, source_target_pairs={{0,3},{1,0},{2,1},{3,2},{4,7},{5,4},{6,5},{7,6},{8,11},{9,8},{10,9... | collective-permute-start | bytes 786440 | tf_op jit(solution)/shard_map/ppermute | solution.py:389
  106.3 0.1 add_convert_fusion.1
  106.4 0.1 collective-permute-start.13
  106.5 0.7 collective-permute-done.14.refs_2_
  107.2 2.7 %collective-permute-done.15.refs_4_ = bf16[256,512]{1,0:T(8,128)(2,1)S(1)} collective-permute-done((bf16[256,512]{1,0:T(8,128)(2,1)S(1)}, bf16[256,512]{1,0:T(8,128)(2,1)S(1)}, u32[]{:S(2)}, u32[]{:S(2)}) %collective-permute-start.15) | collective-permute-done | bytes 262176 | tf_op jit(solution)/shard_map/ppermute | solution.py:389
  109.9 2.6 %collective-permute-done.17.refs_5_ = bf16[256,512]{1,0:T(8,128)(2,1)S(1)} collective-permute-done((bf16[256,512]{1,0:T(8,128)(2,1)S(1)}, bf16[256,512]{1,0:T(8,128)(2,1)S(1)}, u32[]{:S(2)}, u32[]{:S(2)}) %collective-permute-start.17) | collective-permute-done | bytes 262176 | tf_op jit(solution)/shard_map/ppermute | solution.py:389
  112.5 1.7 %collective-permute-done.13.refs_1_ = bf16[256,512]{1,0:T(8,128)(2,1)S(1)} collective-permute-done((bf16[256,512]{1,0:T(8,128)(2,1)S(1)}, bf16[256,512]{1,0:T(8,128)(2,1)S(1)}, u32[]{:S(2)}, u32[]{:S(2)}) %collective-permute-start.13) | collective-permute-done | bytes 262176 | tf_op jit(solution)/shard_map/ppermute | solution.py:389
  114.2 0.2 shard_map.197
  114.4 27.5 %all_to_all.21 = bf16[64,8,512]{2,1,0:T(8,128)(2,1)S(1)} all-to-all(bf16[64,8,512]{2,1,0:T(8,128)(2,1)S(1)} %bitcast.20), channel_id=1, replica_groups=mesh['sp'=64,'tp'=4] {'sp'}, dimensions={0} | all-to-all | bytes 1048576 | tf_op jit(solution)/shard_map/all_to_all | solution.py:384
  141.9 1.2 shard_map.198
  (25 shorter events, 0.1 us)
Async XLA Ops:
  0.0 17.3 %copy-start.8 = (bf16[128,2048]{1,0:T(8,128)(2,1)S(1)}, bf16[128,2048]{1,0:T(8,128)(2,1)}, u32[]{:S(2)}) copy-start(bf16[128,2048]{1,0:T(8,128)(2,1)} %weight.1) | copy-start | bytes 1572868
  0.0 29.8 %copy-start.4 = (s32[128,2]{0,1:T(2,128)S(1)}, s32[128,2]{0,1:T(2,128)}, u32[]{:S(2)}) copy-start(s32[128,2]{0,1:T(2,128)} %param.35) | copy-start | bytes 3076
  0.0 29.8 %copy-start.5 = (f32[128,2]{0,1:T(2,128)S(1)}, f32[128,2]{0,1:T(2,128)}, u32[]{:S(2)}) copy-start(f32[128,2]{0,1:T(2,128)} %param.36) | copy-start | bytes 3076
  4.1 25.6 %copy-start.6 = (f32[128,512]{1,0:T(8,128)}, f32[128,512]{1,0:T(8,128)S(1)}, u32[]{:S(2)}) copy-start(f32[128,512]{1,0:T(8,128)S(1)} %get-tuple-element.30.cum_imag) | copy-start | bytes 786436
  4.1 37.5 %copy-start = (bf16[32,2048]{1,0:T(8,128)(2,1)S(1)}, bf16[32,2048]{1,0:T(8,128)(2,1)}, u32[]{:S(2)}) copy-start(bf16[32,2048]{1,0:T(8,128)(2,1)} %refs_6_.1) | copy-start | bytes 393220
  4.1 37.5 %copy-start.1 = (f32[2048]{0:T(1024)S(1)}, f32[2048]{0:T(1024)}, u32[]{:S(2)}) copy-start(f32[2048]{0:T(1024)} %param.32) | copy-start | bytes 24580
  4.1 37.5 %copy-start.2 = (f32[2048]{0:T(1024)S(1)}, f32[2048]{0:T(1024)}, u32[]{:S(2)}) copy-start(f32[2048]{0:T(1024)} %param.33) | copy-start | bytes 24580
  4.1 26.2 %all-to-all-start = ((bf16[64,8,256]{2,1,0:T(8,128)(2,1)}), bf16[64,8,256]{2,1,0:T(8,128)(2,1)S(1)}, u32[]{:S(2)}, u32[]{:S(2)}) async-start(bf16[64,8,256]{2,1,0:T(8,128)(2,1)} %get-tuple-element.26), calls=%async_computation | async-start | bytes 524288 | tf_op jit(solution)/shard_map/all_to_all | solution.py:384
  18.1 9.0 %collective-permute-start = (bf16[64,2048]{1,0:T(8,128)(2,1)}, bf16[64,2048]{1,0:T(8,128)(2,1)S(1)}, u32[]{:S(2)}, u32[]{:S(2)}) collective-permute-start(bf16[64,2048]{1,0:T(8,128)(2,1)} %get-tuple-element.50), channel_id=1, source_target_pairs={{0,1},{1,2},{2,3},{3,0},{4,5},{5,6},{6,7},{7,4},{8,9},{9,10},{10,1... | collective-permute-start | bytes 786440 | tf_op jit(solution)/shard_map/ppermute | solution.py:389
  19.4 7.7 %collective-permute-start.3 = (bf16[64,2048]{1,0:T(8,128)(2,1)}, bf16[64,2048]{1,0:T(8,128)(2,1)S(1)}, u32[]{:S(2)}, u32[]{:S(2)}) collective-permute-start(bf16[64,2048]{1,0:T(8,128)(2,1)} %get-tuple-element.49), channel_id=1, source_target_pairs={{0,3},{1,0},{2,1},{3,2},{4,7},{5,4},{6,5},{7,6},{8,11},{9,8},{10,9... | collective-permute-start | bytes 786440 | tf_op jit(solution)/shard_map/ppermute | solution.py:389
  20.9 16.4 %collective-permute-start.1 = (bf16[64,2048]{1,0:T(8,128)(2,1)}, bf16[64,2048]{1,0:T(8,128)(2,1)S(1)}, u32[]{:S(2)}, u32[]{:S(2)}) collective-permute-start(bf16[64,2048]{1,0:T(8,128)(2,1)} %get-tuple-element.49), channel_id=1, source_target_pairs={{0,1},{1,2},{2,3},{3,0},{4,5},{5,6},{6,7},{7,4},{8,9},{9,10},{10,1... | collective-permute-start | bytes 786440 | tf_op jit(solution)/shard_map/ppermute | solution.py:389
  20.9 16.4 %collective-permute-start.5 = (bf16[64,2048]{1,0:T(8,128)(2,1)}, bf16[64,2048]{1,0:T(8,128)(2,1)S(1)}, u32[]{:S(2)}, u32[]{:S(2)}) collective-permute-start(bf16[64,2048]{1,0:T(8,128)(2,1)} %get-tuple-element.50), channel_id=1, source_target_pairs={{0,3},{1,0},{2,1},{3,2},{4,7},{5,4},{6,5},{7,6},{8,11},{9,8},{10,9... | collective-permute-start | bytes 786440 | tf_op jit(solution)/shard_map/ppermute | solution.py:389
  27.1 11.2 %collective-permute-start.2 = (bf16[64,2048]{1,0:T(8,128)(2,1)S(1)}, bf16[64,2048]{1,0:T(8,128)(2,1)S(1)}, u32[]{:S(2)}, u32[]{:S(2)}) collective-permute-start(bf16[64,2048]{1,0:T(8,128)(2,1)S(1)} %collective-permute-done.refs_0_), channel_id=1, source_target_pairs={{0,1},{1,2},{2,3},{3,0},{4,5},{5,6},{6,7},{7,4},{8,9},{9,10},{10,1... | collective-permute-start | bytes 786440 | tf_op jit(solution)/shard_map/ppermute | solution.py:389
  27.1 11.2 %collective-permute-start.4 = (bf16[64,2048]{1,0:T(8,128)(2,1)S(1)}, bf16[64,2048]{1,0:T(8,128)(2,1)S(1)}, u32[]{:S(2)}, u32[]{:S(2)}) collective-permute-start(bf16[64,2048]{1,0:T(8,128)(2,1)S(1)} %collective-permute-done.3.refs_5_), channel_id=1, source_target_pairs={{0,3},{1,0},{2,1},{3,2},{4,7},{5,4},{6,5},{7,6},{8,11},{9,8},{10,9... | collective-permute-start | bytes 786440 | tf_op jit(solution)/shard_map/ppermute | solution.py:389
  30.3 1.0 copy-start.7
  33.1 8.5 %all-to-all-start.1 = ((bf16[4,32,128]{2,1,0:T(8,128)(2,1)}), bf16[4,32,128]{2,1,0:T(8,128)(2,1)S(1)}, u32[]{:S(2)}, u32[]{:S(2)}) async-start(bf16[4,32,128]{2,1,0:T(8,128)(2,1)} %bitcast.8), calls=%async_computation.1 | async-start | bytes 65536 | tf_op jit(solution)/shard_map/all_to_all | solution.py:515
  73.8 8.8 %collective-permute-start.6 = (bf16[256,512]{1,0:T(8,128)(2,1)S(1)}, bf16[256,512]{1,0:T(8,128)(2,1)S(1)}, u32[]{:S(2)}, u32[]{:S(2)}) collective-permute-start(bf16[256,512]{1,0:T(8,128)(2,1)S(1)} %get-tuple-element.48.first), channel_id=1, source_target_pairs={{0,1},{1,2},{2,3},{3,0},{4,5},{5,6},{6,7},{7,4},{8,9},{9,10},{10,1... | collective-permute-start | bytes 786440 | tf_op jit(solution)/shard_map/ppermute | solution.py:389
  74.1 8.4 %collective-permute-start.9 = (bf16[256,512]{1,0:T(8,128)(2,1)S(1)}, bf16[256,512]{1,0:T(8,128)(2,1)S(1)}, u32[]{:S(2)}, u32[]{:S(2)}) collective-permute-start(bf16[256,512]{1,0:T(8,128)(2,1)S(1)} %get-tuple-element.47.last), channel_id=1, source_target_pairs={{0,3},{1,0},{2,1},{3,2},{4,7},{5,4},{6,5},{7,6},{8,11},{9,8},{10,9... | collective-permute-start | bytes 786440 | tf_op jit(solution)/shard_map/ppermute | solution.py:389
  82.5 10.8 %collective-permute-start.10 = (bf16[256,512]{1,0:T(8,128)(2,1)S(1)}, bf16[256,512]{1,0:T(8,128)(2,1)S(1)}, u32[]{:S(2)}, u32[]{:S(2)}) collective-permute-start(bf16[256,512]{1,0:T(8,128)(2,1)S(1)} %collective-permute-done.6.refs_0_), channel_id=1, source_target_pairs={{0,1},{1,2},{2,3},{3,0},{4,5},{5,6},{6,7},{7,4},{8,9},{9,10},{10,1... | collective-permute-start | bytes 786440 | tf_op jit(solution)/shard_map/ppermute | solution.py:389
  82.5 10.8 %collective-permute-start.11 = (bf16[256,512]{1,0:T(8,128)(2,1)S(1)}, bf16[256,512]{1,0:T(8,128)(2,1)S(1)}, u32[]{:S(2)}, u32[]{:S(2)}) collective-permute-start(bf16[256,512]{1,0:T(8,128)(2,1)S(1)} %collective-permute-done.9.refs_3_), channel_id=1, source_target_pairs={{0,3},{1,0},{2,1},{3,2},{4,7},{5,4},{6,5},{7,6},{8,11},{9,8},{10,9... | collective-permute-start | bytes 786440 | tf_op jit(solution)/shard_map/ppermute | solution.py:389
  85.2 12.1 %collective-permute-start.7 = (bf16[256,512]{1,0:T(8,128)(2,1)S(1)}, bf16[256,512]{1,0:T(8,128)(2,1)S(1)}, u32[]{:S(2)}, u32[]{:S(2)}) collective-permute-start(bf16[256,512]{1,0:T(8,128)(2,1)S(1)} %get-tuple-element.47.last), channel_id=1, source_target_pairs={{0,1},{1,2},{2,3},{3,0},{4,5},{5,6},{6,7},{7,4},{8,9},{9,10},{10,1... | collective-permute-start | bytes 786440 | tf_op jit(solution)/shard_map/ppermute | solution.py:389
  85.2 12.1 %collective-permute-start.8 = (bf16[256,512]{1,0:T(8,128)(2,1)S(1)}, bf16[256,512]{1,0:T(8,128)(2,1)S(1)}, u32[]{:S(2)}, u32[]{:S(2)}) collective-permute-start(bf16[256,512]{1,0:T(8,128)(2,1)S(1)} %get-tuple-element.48.first), channel_id=1, source_target_pairs={{0,3},{1,0},{2,1},{3,2},{4,7},{5,4},{6,5},{7,6},{8,11},{9,8},{10,9... | collective-permute-start | bytes 786440 | tf_op jit(solution)/shard_map/ppermute | solution.py:389
  95.8 7.7 %collective-permute-start.16 = (bf16[256,512]{1,0:T(8,128)(2,1)S(1)}, bf16[256,512]{1,0:T(8,128)(2,1)S(1)}, u32[]{:S(2)}, u32[]{:S(2)}) collective-permute-start(bf16[256,512]{1,0:T(8,128)(2,1)S(1)} %get-tuple-element.44), channel_id=1, source_target_pairs={{0,3},{1,0},{2,1},{3,2},{4,7},{5,4},{6,5},{7,6},{8,11},{9,8},{10,9... | collective-permute-start | bytes 786440 | tf_op jit(solution)/shard_map/ppermute | solution.py:389
  95.9 10.4 %collective-permute-start.12 = (bf16[256,512]{1,0:T(8,128)(2,1)S(1)}, bf16[256,512]{1,0:T(8,128)(2,1)S(1)}, u32[]{:S(2)}, u32[]{:S(2)}) collective-permute-start(bf16[256,512]{1,0:T(8,128)(2,1)S(1)} %get-tuple-element.39), channel_id=1, source_target_pairs={{0,1},{1,2},{2,3},{3,0},{4,5},{5,6},{6,7},{7,4},{8,9},{9,10},{10,1... | collective-permute-start | bytes 786440 | tf_op jit(solution)/shard_map/ppermute | solution.py:389
  101.8 40.0 %copy-start.3 = (f32[2048]{0:T(1024)S(1)}, f32[2048]{0:T(1024)}, u32[]{:S(2)}) copy-start(f32[2048]{0:T(1024)} %param.34) | copy-start | bytes 24580
  101.9 5.3 %collective-permute-start.14 = (bf16[256,512]{1,0:T(8,128)(2,1)S(1)}, bf16[256,512]{1,0:T(8,128)(2,1)S(1)}, u32[]{:S(2)}, u32[]{:S(2)}) collective-permute-start(bf16[256,512]{1,0:T(8,128)(2,1)S(1)} %get-tuple-element.40), channel_id=1, source_target_pairs={{0,3},{1,0},{2,1},{3,2},{4,7},{5,4},{6,5},{7,6},{8,11},{9,8},{10,9... | collective-permute-start | bytes 786440 | tf_op jit(solution)/shard_map/ppermute | solution.py:389
  103.5 6.4 %collective-permute-start.15 = (bf16[256,512]{1,0:T(8,128)(2,1)S(1)}, bf16[256,512]{1,0:T(8,128)(2,1)S(1)}, u32[]{:S(2)}, u32[]{:S(2)}) collective-permute-start(bf16[256,512]{1,0:T(8,128)(2,1)S(1)} %get-tuple-element.42), channel_id=1, source_target_pairs={{0,1},{1,2},{2,3},{3,0},{4,5},{5,6},{6,7},{7,4},{8,9},{9,10},{10,1... | collective-permute-start | bytes 786440 | tf_op jit(solution)/shard_map/ppermute | solution.py:389
  103.5 8.9 %collective-permute-start.17 = (bf16[256,512]{1,0:T(8,128)(2,1)S(1)}, bf16[256,512]{1,0:T(8,128)(2,1)S(1)}, u32[]{:S(2)}, u32[]{:S(2)}) collective-permute-start(bf16[256,512]{1,0:T(8,128)(2,1)S(1)} %add_convert_fusion), channel_id=1, source_target_pairs={{0,3},{1,0},{2,1},{3,2},{4,7},{5,4},{6,5},{7,6},{8,11},{9,8},{10,9... | collective-permute-start | bytes 786440 | tf_op jit(solution)/shard_map/ppermute | solution.py:389
  106.4 7.9 %collective-permute-start.13 = (bf16[256,512]{1,0:T(8,128)(2,1)S(1)}, bf16[256,512]{1,0:T(8,128)(2,1)S(1)}, u32[]{:S(2)}, u32[]{:S(2)}) collective-permute-start(bf16[256,512]{1,0:T(8,128)(2,1)S(1)} %add_convert_fusion.1), channel_id=1, source_target_pairs={{0,1},{1,2},{2,3},{3,0},{4,5},{5,6},{6,7},{7,4},{8,9},{9,10},{10,1... | collective-permute-start | bytes 786440 | tf_op jit(solution)/shard_map/ppermute | solution.py:389

commit v4 on v2

--- a/solution.py
+++ b/solution.py
@@ -168,7 +168,10 @@
     message[...] = jnp.broadcast_to(sent[None], message.shape)
 
 
-def carry_kernel(got, rates, read, cum_real, cum_imag, local_out, mixed):
+def carry_kernel(
+    got, rates, read, cum_real, cum_imag, local_out, ids, logits, mixed, place, weigh
+):
+    routing(ids, logits, place, weigh)
     rows, lanes = MESSAGE
     devices = got.shape[0] // rows
     width = rates.shape[1]
@@ -208,7 +211,7 @@
     mixed[...] = jax.nn.gelu(result).astype(BF16)
 
 
-def route_kernel(ids, logits, place, weigh):
+def routing(ids, logits, place, weigh):
     slots = ids.shape[1]
     tall = (slots, slots)
     rows = slots // 4
@@ -412,10 +415,9 @@
             *halves, *held, flops=work * count // 2,
         )
 
-    to_left_first, to_left_last, to_right_first, to_right_last = part(
-        left_first, left_last, right_first, right_last
-    )
+    to_left_first, to_right_last = part(left_first, right_last)
     from_left_last, from_right_first = (shifted(to_right_last, 1), shifted(to_left_first, -1))
+    to_left_last, to_right_first = part(left_last, right_first)
     far_first, far_last = part(across_first, across_last)
     to_right_first = added(to_right_first, shifted(far_first, 1))
     to_left_last = added(to_left_last, shifted(far_last, -1))
@@ -485,16 +487,16 @@
         flops=10**9,
     )
     got = across_sp(message)
-    place, weigh = call(
-        route_kernel,
-        [((4 * slots, slots), BF16), ((3 * slots, 4 * slots), BF16)],
+    mixed, place, weigh = call(
+        carry_kernel,
+        [
+            ((length, channels), BF16),
+            ((4 * slots, slots), BF16),
+            ((3 * slots, 4 * slots), BF16),
+        ],
+        got.reshape(-1, MESSAGE[1]), rates, read, cum_real, cum_imag, local_out,
         route_ids.T,
         route_logits.T,
-        flops=10**8,
-    )
-    mixed = call(
-        carry_kernel, ((length, channels), BF16),
-        got.reshape(-1, MESSAGE[1]), rates, read, cum_real, cum_imag, local_out,
         flops=10**9,
     )
     tokens = lax.all_to_all(

time: 144 us -> 145 us (level)
  starting transfers between devices: 36.1 us -> 40.6 us
  waiting for transfers between devices: 28.2 us -> 24.1 us
    ppermute x15, starting transfers between devices: 18.9 us -> 23.4 us  [shifted(): return lax.ppermute(part, 'tp', [(i, (i + by) % size) for i in range(size)])]
    ppermute x15, waiting for transfers between devices: 19.8 us -> 16.6 us  [shifted(): return lax.ppermute(part, 'tp', [(i, (i + by) % size) for i in range(size)])]
  transfers between devices with their start and end apart: 17 -> 17, of which waited for: 8 -> 7; matrix products, arithmetic and copies ran while one was open for 0% -> 0% of each run, Pallas kernels for 10% -> 10%
where the time goes in v4:
time: 145 us
  blocking collectives  56.4 us (39%)
  starting transfers between devices  40.6 us (28%)
  waiting for transfers between devices  24.1 us (17%)
  Pallas kernels  21.2 us (15%)
  local copies, waits for them, and re-layouts  2.47 us (2%)
    all_to_all x2, blocking collectives, across_sp(): return lax.all_to_all(pieces, 'sp', split_axis=0, concat_axis=0, tiled=True)  56.4 us
    ppermute x15, starting transfers between devices, shifted(): return lax.ppermute(part, 'tp', [(i, (i + by) % size) for i in range(size)])  23.4 us
    pallas_call x9, Pallas kernels, call(): pl.pallas_call(kernel, out_shape=shapes, in_specs=[left if k in in_place...  21.2 us
    ppermute x15, waiting for transfers between devices, shifted(): return lax.ppermute(part, 'tp', [(i, (i + by) % size) for i in range(size)])  16.6 us
    all_to_all x1, starting transfers between devices, across_sp(): return lax.all_to_all(pieces, 'sp', split_axis=0, concat_axis=0, tiled=True)  13 us
    all_to_all x1, waiting for transfers between devices, across_sp(): return lax.all_to_all(pieces, 'sp', split_axis=0, concat_axis=0, tiled=True)  7.39 us
    all_to_all x1, starting transfers between devices, on_device(): lax.all_to_all(mixed.reshape(quarters, rows, channels), 'tp', split_axis=...  4.18 us
  transfers between devices with their start and end apart: 17, of which 7 were waited for; matrix products, arithmetic and copies ran while one was open for 0% of the time, Pallas kernels for 10%

profile of v4, /device:TPU:1, one launch (start us, length us, event | category | flops | bytes accessed | tf_op | source)
XLA Modules:
  0.0 145.1 jit_solution(3154363325144575859)
XLA Ops:
  0.0 4.1 %shard_map.190 = (bf16[64,8,256]{2,1,0:T(8,128)(2,1)}, f32[8,512]{1,0:T(8,128)S(1)}, bf16[1024,256]{1,0:T(8,128)(2,1)S(1)}, f32[128,512]{1,0:T(8,128)S(1)}, f32[...) custom-call(f32[8,128]{1,0:T(8,128)} %bitcast.32, bf16[128,128]{1,0:T(8,128)(2,1)} %inputs.1, f32[1,8]{1,0:T(1,128)} %bitcast.33, ...), custom_call_target="tpu_custom_call" | custom-call | flops 1000000000 | tf_op jit(solution)/shard_map/pallas_call | solution.py:360
  4.1 0.7 copy-done.9
  4.8 13.0 %all-to-all-start = ((bf16[64,8,256]{2,1,0:T(8,128)(2,1)}), bf16[64,8,256]{2,1,0:T(8,128)(2,1)S(1)}, u32[]{:S(2)}, u32[]{:S(2)}) async-start(bf16[64,8,256]{2,1,0:T(8,128)(2,1)} %get-tuple-element.27), calls=%async_computation | async-start | bytes 524288 | tf_op jit(solution)/shard_map/all_to_all | solution.py:380
  17.8 3.0 %collective-permute-start.1 = (bf16[128,2048]{1,0:T(8,128)(2,1)S(1)}, bf16[128,2048]{1,0:T(8,128)(2,1)S(1)}, u32[]{:S(2)}, u32[]{:S(2)}) collective-permute-start(bf16[128,2048]{1,0:T(8,128)(2,1)S(1)} %copy-done), channel_id=1, source_target_pairs={{0,2},{1,3},{2,0},{3,1},{4,6},{5,7},{6,4},{7,5},{8,10},{9,11},{10,... | collective-permute-start | bytes 1572872 | tf_op jit(solution)/shard_map/ppermute | solution.py:385
  20.8 0.4 collective-permute-start
  21.2 2.3 %collective-permute-start.2 = (bf16[128,2048]{1,0:T(8,128)(2,1)S(1)}, bf16[128,2048]{1,0:T(8,128)(2,1)S(1)}, u32[]{:S(2)}, u32[]{:S(2)}) collective-permute-start(bf16[128,2048]{1,0:T(8,128)(2,1)S(1)} %copy-done), channel_id=1, source_target_pairs={{0,3},{1,0},{2,1},{3,2},{4,7},{5,4},{6,5},{7,6},{8,11},{9,8},{10,9... | collective-permute-start | bytes 1572872 | tf_op jit(solution)/shard_map/ppermute | solution.py:385
  23.5 7.4 %all-to-all-done = bf16[64,8,256]{2,1,0:T(8,128)(2,1)S(1)} async-done(((bf16[64,8,256]{2,1,0:T(8,128)(2,1)}), bf16[64,8,256]{2,1,0:T(8,128)(2,1)S(1)}, u32[]{:S(2)}, u32[]{:S(2)}) %all-to-all-start) | async-done | bytes 262176 | tf_op jit(solution)/shard_map/all_to_all | solution.py:380
  30.9 0.9 copy-done.10
  31.8 2.2 %shard_map.191 = (bf16[128,128]{1,0:T(8,128)(2,1)}, bf16[512,128]{1,0:T(8,128)(2,1)S(1)}, bf16[384,512]{1,0:T(8,128)(2,1)S(1)}) custom-call(bf16[512,256]{1,0:T(8,128)(2,1)S(1)} %bitcast.23, f32[8,512]{1,0:T(8,128)S(1)} %get-tuple-element.28.rates, bf16[1024,256]{1,0:T(8,128)(2,1)S(1)} %get-tuple-element.29.read, f32[128,512]{1,0:T(8,128)S(1)} %get-tuple-element.30.cum_real, ...), custom_call_target="tpu_custom_call" | custom-call | flops 1000000000 | tf_op jit(solution)/shard_map/pallas_call | solution.py:360
  34.1 0.7 copy-done.7
  34.8 4.2 %all-to-all-start.1 = ((bf16[4,32,128]{2,1,0:T(8,128)(2,1)}), bf16[4,32,128]{2,1,0:T(8,128)(2,1)S(1)}, u32[]{:S(2)}, u32[]{:S(2)}) async-start(bf16[4,32,128]{2,1,0:T(8,128)(2,1)} %bitcast.8), calls=%async_computation.1 | async-start | bytes 65536 | tf_op jit(solution)/shard_map/all_to_all | solution.py:502
  39.0 0.0 collective-permute-done.1.weight_2
  39.0 5.6 %collective-permute-done.weight_1 = bf16[128,2048]{1,0:T(8,128)(2,1)S(1)} collective-permute-done((bf16[128,2048]{1,0:T(8,128)(2,1)S(1)}, bf16[128,2048]{1,0:T(8,128)(2,1)S(1)}, u32[]{:S(2)}, u32[]{:S(2)}) %collective-permute-start) | collective-permute-done | bytes 524320 | tf_op jit(solution)/shard_map/ppermute | solution.py:385
  44.6 0.0 collective-permute-done.2.weight_3
  44.6 0.2 all-to-all-done.1
  44.8 0.9 shard_map.192
  45.7 28.3 %all_to_all.20 = bf16[64,8,512]{2,1,0:T(8,128)(2,1)S(1)} all-to-all(bf16[64,8,512]{2,1,0:T(8,128)(2,1)S(1)} %bitcast.21), channel_id=1, replica_groups=mesh['sp'=64,'tp'=4] {'sp'}, dimensions={0} | all-to-all | bytes 1048576 | tf_op jit(solution)/shard_map/all_to_all | solution.py:380
  74.0 2.6 %collective-permute-start.7 = (bf16[256,512]{1,0:T(8,128)(2,1)S(1)}, bf16[256,512]{1,0:T(8,128)(2,1)S(1)}, u32[]{:S(2)}, u32[]{:S(2)}) collective-permute-start(bf16[256,512]{1,0:T(8,128)(2,1)S(1)} %get-tuple-element.49.last), channel_id=1, source_target_pairs={{0,3},{1,0},{2,1},{3,2},{4,7},{5,4},{6,5},{7,6},{8,11},{9,8},{10,9... | collective-permute-start | bytes 786440 | tf_op jit(solution)/shard_map/ppermute | solution.py:385
  76.6 0.0 collective-permute-start.5
  76.6 5.3 %collective-permute-done.7.refs_1_ = bf16[256,512]{1,0:T(8,128)(2,1)S(1)} collective-permute-done((bf16[256,512]{1,0:T(8,128)(2,1)S(1)}, bf16[256,512]{1,0:T(8,128)(2,1)S(1)}, u32[]{:S(2)}, u32[]{:S(2)}) %collective-permute-start.7) | collective-permute-done | bytes 262176 | tf_op jit(solution)/shard_map/ppermute | solution.py:385
  81.8 3.4 %collective-permute-start.8 = (bf16[256,512]{1,0:T(8,128)(2,1)S(1)}, bf16[256,512]{1,0:T(8,128)(2,1)S(1)}, u32[]{:S(2)}, u32[]{:S(2)}) collective-permute-start(bf16[256,512]{1,0:T(8,128)(2,1)S(1)} %collective-permute-done.7.refs_1_), channel_id=1, source_target_pairs={{0,3},{1,0},{2,1},{3,2},{4,7},{5,4},{6,5},{7,6},{8,11},{9,8},{10,9... | collective-permute-start | bytes 786440 | tf_op jit(solution)/shard_map/ppermute | solution.py:385
  85.2 0.0 collective-permute-done.5.refs_0_
  85.2 0.0 collective-permute-start.6
  85.2 0.0 collective-permute-start.3
  85.3 2.7 %collective-permute-start.4 = (bf16[256,512]{1,0:T(8,128)(2,1)S(1)}, bf16[256,512]{1,0:T(8,128)(2,1)S(1)}, u32[]{:S(2)}, u32[]{:S(2)}) collective-permute-start(bf16[256,512]{1,0:T(8,128)(2,1)S(1)} %get-tuple-element.50.first), channel_id=1, source_target_pairs={{0,3},{1,0},{2,1},{3,2},{4,7},{5,4},{6,5},{7,6},{8,11},{9,8},{10,9... | collective-permute-start | bytes 786440 | tf_op jit(solution)/shard_map/ppermute | solution.py:385
  87.9 5.4 %shard_map.193 = (bf16[256,512]{1,0:T(8,128)(2,1)S(1)}, bf16[256,512]{1,0:T(8,128)(2,1)S(1)}, bf16[1,2048,896]{2,1,0:T(8,128)(2,1)S(1)}, bf16[1,2048,896]{2,1,0:T(8,128)(2,1)S(1)}, bf16[1,896,2048]{2,1,0:T(8,128)(2,1)S(1)}) custom-call(bf16[256,512]{1,0:T(8,128)(2,1)S(1)} %get-tuple-element.50.first, bf16[256,512]{1,0:T(8,128)(2,1)S(1)} %get-tuple-element.49.last, ...), custom_call_target="tpu_custom_call" | custom-call | flops 1409286144 | tf_op jit(solution)/shard_map/pallas_call | solution.py:360
  93.4 0.0 collective-permute-done.8.refs_1_
  93.4 0.0 collective-permute-done.6.refs_0_
  93.4 2.4 %shard_map.195 = (bf16[256,512]{1,0:T(8,128)(2,1)S(1)}, bf16[256,512]{1,0:T(8,128)(2,1)S(1)}) custom-call(bf16[256,512]{1,0:T(8,128)(2,1)S(1)} %collective-permute-done.6.refs_0_, bf16[256,512]{1,0:T(8,128)(2,1)S(1)} %collective-permute-done.8.refs_1_, bf16[1,2048,896]{2,1,0:T(8,128)(2,1)S(1)} %get-tuple-element.37.refs_2_, ...), custom_call_target="tpu_custom_call" | custom-call | flops 1409286144 | tf_op jit(solution)/shard_map/pallas_call | solution.py:360
  95.8 0.1 collective-permute-start.9
  95.9 2.4 %shard_map.196 = (bf16[256,512]{1,0:T(8,128)(2,1)S(1)}, bf16[256,512]{1,0:T(8,128)(2,1)S(1)}) custom-call(bf16[256,512]{1,0:T(8,128)(2,1)S(1)} %collective-permute-done.5.refs_0_, bf16[256,512]{1,0:T(8,128)(2,1)S(1)} %collective-permute-done.7.refs_1_, bf16[1,2048,896]{2,1,0:T(8,128)(2,1)S(1)} %get-tuple-element.37.refs_2_, ...), custom_call_target="tpu_custom_call" | custom-call | flops 1409286144 | tf_op jit(solution)/shard_map/pallas_call | solution.py:360
  98.3 2.7 %collective-permute-start.11 = (bf16[256,512]{1,0:T(8,128)(2,1)S(1)}, bf16[256,512]{1,0:T(8,128)(2,1)S(1)}, u32[]{:S(2)}, u32[]{:S(2)}) collective-permute-start(bf16[256,512]{1,0:T(8,128)(2,1)S(1)} %get-tuple-element.42), channel_id=1, source_target_pairs={{0,3},{1,0},{2,1},{3,2},{4,7},{5,4},{6,5},{7,6},{8,11},{9,8},{10,9... | collective-permute-start | bytes 786440 | tf_op jit(solution)/shard_map/ppermute | solution.py:385
  101.1 2.7 %collective-permute-start.13 = (bf16[256,512]{1,0:T(8,128)(2,1)S(1)}, bf16[256,512]{1,0:T(8,128)(2,1)S(1)}, u32[]{:S(2)}, u32[]{:S(2)}) collective-permute-start(bf16[256,512]{1,0:T(8,128)(2,1)S(1)} %get-tuple-element.46), channel_id=1, source_target_pairs={{0,3},{1,0},{2,1},{3,2},{4,7},{5,4},{6,5},{7,6},{8,11},{9,8},{10,9... | collective-permute-start | bytes 786440 | tf_op jit(solution)/shard_map/ppermute | solution.py:385
  103.8 2.4 %shard_map.194 = (bf16[256,512]{1,0:T(8,128)(2,1)S(1)}, bf16[256,512]{1,0:T(8,128)(2,1)S(1)}) custom-call(bf16[256,512]{1,0:T(8,128)(2,1)S(1)} %collective-permute-done.3.refs_0_, bf16[256,512]{1,0:T(8,128)(2,1)S(1)} %collective-permute-done.4.refs_1_, bf16[1,2048,896]{2,1,0:T(8,128)(2,1)S(1)} %get-tuple-element.37.refs_2_, ...), custom_call_target="tpu_custom_call" | custom-call | flops 1409286144 | tf_op jit(solution)/shard_map/pallas_call | solution.py:360
  106.2 0.0 copy-start.4
  106.2 0.0 collective-permute-done.9
  106.2 0.1 add_convert_fusion.1
  106.3 0.1 collective-permute-start.10
  106.4 2.0 %collective-permute-done.13 = bf16[256,512]{1,0:T(8,128)(2,1)S(1)} collective-permute-done((bf16[256,512]{1,0:T(8,128)(2,1)S(1)}, bf16[256,512]{1,0:T(8,128)(2,1)S(1)}, u32[]{:S(2)}, u32[]{:S(2)}) %collective-permute-start.13) | collective-permute-done | bytes 262176 | tf_op jit(solution)/shard_map/ppermute | solution.py:385
  108.3 0.1 add_convert_fusion
  108.4 3.5 %collective-permute-start.14 = (bf16[256,512]{1,0:T(8,128)(2,1)S(1)}, bf16[256,512]{1,0:T(8,128)(2,1)S(1)}, u32[]{:S(2)}, u32[]{:S(2)}) collective-permute-start(bf16[256,512]{1,0:T(8,128)(2,1)S(1)} %add_convert_fusion), channel_id=1, source_target_pairs={{0,3},{1,0},{2,1},{3,2},{4,7},{5,4},{6,5},{7,6},{8,11},{9,8},{10,9... | collective-permute-start | bytes 786440 | tf_op jit(solution)/shard_map/ppermute | solution.py:385
  111.9 0.0 collective-permute-done.11.refs_2_
  111.9 0.0 collective-permute-done.12.refs_4_
  111.9 3.2 %collective-permute-done.10.refs_1_ = bf16[256,512]{1,0:T(8,128)(2,1)S(1)} collective-permute-done((bf16[256,512]{1,0:T(8,128)(2,1)S(1)}, bf16[256,512]{1,0:T(8,128)(2,1)S(1)}, u32[]{:S(2)}, u32[]{:S(2)}) %collective-permute-start.10) | collective-permute-done | bytes 262176 | tf_op jit(solution)/shard_map/ppermute | solution.py:385
  115.1 0.5 collective-permute-done.14.refs_5_
  115.6 0.2 shard_map.197
  115.8 28.2 %all_to_all.21 = bf16[64,8,512]{2,1,0:T(8,128)(2,1)S(1)} all-to-all(bf16[64,8,512]{2,1,0:T(8,128)(2,1)S(1)} %bitcast.20), channel_id=1, replica_groups=mesh['sp'=64,'tp'=4] {'sp'}, dimensions={0} | all-to-all | bytes 1048576 | tf_op jit(solution)/shard_map/all_to_all | solution.py:380
  144.0 1.2 shard_map.198
  (22 shorter events, 0.1 us)
Async XLA Ops:
  0.0 17.8 %copy-start = (bf16[128,2048]{1,0:T(8,128)(2,1)S(1)}, bf16[128,2048]{1,0:T(8,128)(2,1)}, u32[]{:S(2)}) copy-start(bf16[128,2048]{1,0:T(8,128)(2,1)} %weight_0.1) | copy-start | bytes 1572868
  0.0 30.9 %copy-start.6 = (f32[128,2]{0,1:T(2,128)S(1)}, f32[128,2]{0,1:T(2,128)}, u32[]{:S(2)}) copy-start(f32[128,2]{0,1:T(2,128)} %param.36) | copy-start | bytes 3076
  0.0 30.9 %copy-start.5 = (s32[128,2]{0,1:T(2,128)S(1)}, s32[128,2]{0,1:T(2,128)}, u32[]{:S(2)}) copy-start(s32[128,2]{0,1:T(2,128)} %param.35) | copy-start | bytes 3076
  0.0 44.7 %copy-start.1 = (bf16[32,2048]{1,0:T(8,128)(2,1)S(1)}, bf16[32,2048]{1,0:T(8,128)(2,1)}, u32[]{:S(2)}) copy-start(bf16[32,2048]{1,0:T(8,128)(2,1)} %residual.1) | copy-start | bytes 393220
  0.0 44.7 %copy-start.2 = (f32[2048]{0:T(1024)S(1)}, f32[2048]{0:T(1024)}, u32[]{:S(2)}) copy-start(f32[2048]{0:T(1024)} %param.32) | copy-start | bytes 24580
  0.0 44.7 %copy-start.3 = (f32[2048]{0:T(1024)S(1)}, f32[2048]{0:T(1024)}, u32[]{:S(2)}) copy-start(f32[2048]{0:T(1024)} %param.33) | copy-start | bytes 24580
  4.1 0.7 copy-start.9
  4.8 26.1 %all-to-all-start = ((bf16[64,8,256]{2,1,0:T(8,128)(2,1)}), bf16[64,8,256]{2,1,0:T(8,128)(2,1)S(1)}, u32[]{:S(2)}, u32[]{:S(2)}) async-start(bf16[64,8,256]{2,1,0:T(8,128)(2,1)} %get-tuple-element.27), calls=%async_computation | async-start | bytes 524288 | tf_op jit(solution)/shard_map/all_to_all | solution.py:380
  17.8 21.2 %collective-permute-start.1 = (bf16[128,2048]{1,0:T(8,128)(2,1)S(1)}, bf16[128,2048]{1,0:T(8,128)(2,1)S(1)}, u32[]{:S(2)}, u32[]{:S(2)}) collective-permute-start(bf16[128,2048]{1,0:T(8,128)(2,1)S(1)} %copy-done), channel_id=1, source_target_pairs={{0,2},{1,3},{2,0},{3,1},{4,6},{5,7},{6,4},{7,5},{8,10},{9,11},{10,... | collective-permute-start | bytes 1572872 | tf_op jit(solution)/shard_map/ppermute | solution.py:385
  20.8 23.8 %collective-permute-start = (bf16[128,2048]{1,0:T(8,128)(2,1)S(1)}, bf16[128,2048]{1,0:T(8,128)(2,1)S(1)}, u32[]{:S(2)}, u32[]{:S(2)}) collective-permute-start(bf16[128,2048]{1,0:T(8,128)(2,1)S(1)} %copy-done), channel_id=1, source_target_pairs={{0,1},{1,2},{2,3},{3,0},{4,5},{5,6},{6,7},{7,4},{8,9},{9,10},{10,1... | collective-permute-start | bytes 1572872 | tf_op jit(solution)/shard_map/ppermute | solution.py:385
  21.2 23.4 %collective-permute-start.2 = (bf16[128,2048]{1,0:T(8,128)(2,1)S(1)}, bf16[128,2048]{1,0:T(8,128)(2,1)S(1)}, u32[]{:S(2)}, u32[]{:S(2)}) collective-permute-start(bf16[128,2048]{1,0:T(8,128)(2,1)S(1)} %copy-done), channel_id=1, source_target_pairs={{0,3},{1,0},{2,1},{3,2},{4,7},{5,4},{6,5},{7,6},{8,11},{9,8},{10,9... | collective-permute-start | bytes 1572872 | tf_op jit(solution)/shard_map/ppermute | solution.py:385
  30.9 1.0 copy-start.10
  34.1 0.7 copy-start.7
  34.8 9.9 %all-to-all-start.1 = ((bf16[4,32,128]{2,1,0:T(8,128)(2,1)}), bf16[4,32,128]{2,1,0:T(8,128)(2,1)S(1)}, u32[]{:S(2)}, u32[]{:S(2)}) async-start(bf16[4,32,128]{2,1,0:T(8,128)(2,1)} %bitcast.8), calls=%async_computation.1 | async-start | bytes 65536 | tf_op jit(solution)/shard_map/all_to_all | solution.py:502
  74.0 7.8 %collective-permute-start.7 = (bf16[256,512]{1,0:T(8,128)(2,1)S(1)}, bf16[256,512]{1,0:T(8,128)(2,1)S(1)}, u32[]{:S(2)}, u32[]{:S(2)}) collective-permute-start(bf16[256,512]{1,0:T(8,128)(2,1)S(1)} %get-tuple-element.49.last), channel_id=1, source_target_pairs={{0,3},{1,0},{2,1},{3,2},{4,7},{5,4},{6,5},{7,6},{8,11},{9,8},{10,9... | collective-permute-start | bytes 786440 | tf_op jit(solution)/shard_map/ppermute | solution.py:385
  76.6 8.7 %collective-permute-start.5 = (bf16[256,512]{1,0:T(8,128)(2,1)S(1)}, bf16[256,512]{1,0:T(8,128)(2,1)S(1)}, u32[]{:S(2)}, u32[]{:S(2)}) collective-permute-start(bf16[256,512]{1,0:T(8,128)(2,1)S(1)} %get-tuple-element.50.first), channel_id=1, source_target_pairs={{0,1},{1,2},{2,3},{3,0},{4,5},{5,6},{6,7},{7,4},{8,9},{9,10},{10,1... | collective-permute-start | bytes 786440 | tf_op jit(solution)/shard_map/ppermute | solution.py:385
  81.8 11.6 %collective-permute-start.8 = (bf16[256,512]{1,0:T(8,128)(2,1)S(1)}, bf16[256,512]{1,0:T(8,128)(2,1)S(1)}, u32[]{:S(2)}, u32[]{:S(2)}) collective-permute-start(bf16[256,512]{1,0:T(8,128)(2,1)S(1)} %collective-permute-done.7.refs_1_), channel_id=1, source_target_pairs={{0,3},{1,0},{2,1},{3,2},{4,7},{5,4},{6,5},{7,6},{8,11},{9,8},{10,9... | collective-permute-start | bytes 786440 | tf_op jit(solution)/shard_map/ppermute | solution.py:385
  85.2 8.2 %collective-permute-start.6 = (bf16[256,512]{1,0:T(8,128)(2,1)S(1)}, bf16[256,512]{1,0:T(8,128)(2,1)S(1)}, u32[]{:S(2)}, u32[]{:S(2)}) collective-permute-start(bf16[256,512]{1,0:T(8,128)(2,1)S(1)} %collective-permute-done.5.refs_0_), channel_id=1, source_target_pairs={{0,1},{1,2},{2,3},{3,0},{4,5},{5,6},{6,7},{7,4},{8,9},{9,10},{10,1... | collective-permute-start | bytes 786440 | tf_op jit(solution)/shard_map/ppermute | solution.py:385
  85.2 15.8 %collective-permute-start.3 = (bf16[256,512]{1,0:T(8,128)(2,1)S(1)}, bf16[256,512]{1,0:T(8,128)(2,1)S(1)}, u32[]{:S(2)}, u32[]{:S(2)}) collective-permute-start(bf16[256,512]{1,0:T(8,128)(2,1)S(1)} %get-tuple-element.49.last), channel_id=1, source_target_pairs={{0,1},{1,2},{2,3},{3,0},{4,5},{5,6},{6,7},{7,4},{8,9},{9,10},{10,1... | collective-permute-start | bytes 786440 | tf_op jit(solution)/shard_map/ppermute | solution.py:385
  85.3 18.5 %collective-permute-start.4 = (bf16[256,512]{1,0:T(8,128)(2,1)S(1)}, bf16[256,512]{1,0:T(8,128)(2,1)S(1)}, u32[]{:S(2)}, u32[]{:S(2)}) collective-permute-start(bf16[256,512]{1,0:T(8,128)(2,1)S(1)} %get-tuple-element.50.first), channel_id=1, source_target_pairs={{0,3},{1,0},{2,1},{3,2},{4,7},{5,4},{6,5},{7,6},{8,11},{9,8},{10,9... | collective-permute-start | bytes 786440 | tf_op jit(solution)/shard_map/ppermute | solution.py:385
  95.8 10.4 %collective-permute-start.9 = (bf16[256,512]{1,0:T(8,128)(2,1)S(1)}, bf16[256,512]{1,0:T(8,128)(2,1)S(1)}, u32[]{:S(2)}, u32[]{:S(2)}) collective-permute-start(bf16[256,512]{1,0:T(8,128)(2,1)S(1)} %get-tuple-element.41), channel_id=1, source_target_pairs={{0,1},{1,2},{2,3},{3,0},{4,5},{5,6},{6,7},{7,4},{8,9},{9,10},{10,1... | collective-permute-start | bytes 786440 | tf_op jit(solution)/shard_map/ppermute | solution.py:385
  98.3 13.6 %collective-permute-start.11 = (bf16[256,512]{1,0:T(8,128)(2,1)S(1)}, bf16[256,512]{1,0:T(8,128)(2,1)S(1)}, u32[]{:S(2)}, u32[]{:S(2)}) collective-permute-start(bf16[256,512]{1,0:T(8,128)(2,1)S(1)} %get-tuple-element.42), channel_id=1, source_target_pairs={{0,3},{1,0},{2,1},{3,2},{4,7},{5,4},{6,5},{7,6},{8,11},{9,8},{10,9... | collective-permute-start | bytes 786440 | tf_op jit(solution)/shard_map/ppermute | solution.py:385
  101.1 10.8 %collective-permute-start.12 = (bf16[256,512]{1,0:T(8,128)(2,1)S(1)}, bf16[256,512]{1,0:T(8,128)(2,1)S(1)}, u32[]{:S(2)}, u32[]{:S(2)}) collective-permute-start(bf16[256,512]{1,0:T(8,128)(2,1)S(1)} %get-tuple-element.44), channel_id=1, source_target_pairs={{0,1},{1,2},{2,3},{3,0},{4,5},{5,6},{6,7},{7,4},{8,9},{9,10},{10,1... | collective-permute-start | bytes 786440 | tf_op jit(solution)/shard_map/ppermute | solution.py:385
  101.1 7.2 %collective-permute-start.13 = (bf16[256,512]{1,0:T(8,128)(2,1)S(1)}, bf16[256,512]{1,0:T(8,128)(2,1)S(1)}, u32[]{:S(2)}, u32[]{:S(2)}) collective-permute-start(bf16[256,512]{1,0:T(8,128)(2,1)S(1)} %get-tuple-element.46), channel_id=1, source_target_pairs={{0,3},{1,0},{2,1},{3,2},{4,7},{5,4},{6,5},{7,6},{8,11},{9,8},{10,9... | collective-permute-start | bytes 786440 | tf_op jit(solution)/shard_map/ppermute | solution.py:385
  106.2 37.8 %copy-start.4 = (f32[2048]{0:T(1024)S(1)}, f32[2048]{0:T(1024)}, u32[]{:S(2)}) copy-start(f32[2048]{0:T(1024)} %param.34) | copy-start | bytes 24580
  106.2 37.8 %copy-start.8 = (bf16[384,512]{1,0:T(8,128)(2,1)S(1)}, bf16[384,512]{1,0:T(8,128)(2,1)}, u32[]{:S(2)}) copy-start(bf16[384,512]{1,0:T(8,128)(2,1)} %copy-done.7) | copy-start | bytes 1179652
  106.3 8.8 %collective-permute-start.10 = (bf16[256,512]{1,0:T(8,128)(2,1)S(1)}, bf16[256,512]{1,0:T(8,128)(2,1)S(1)}, u32[]{:S(2)}, u32[]{:S(2)}) collective-permute-start(bf16[256,512]{1,0:T(8,128)(2,1)S(1)} %add_convert_fusion.1), channel_id=1, source_target_pairs={{0,1},{1,2},{2,3},{3,0},{4,5},{5,6},{6,7},{7,4},{8,9},{9,10},{10,1... | collective-permute-start | bytes 786440 | tf_op jit(solution)/shard_map/ppermute | solution.py:385
  108.4 7.2 %collective-permute-start.14 = (bf16[256,512]{1,0:T(8,128)(2,1)S(1)}, bf16[256,512]{1,0:T(8,128)(2,1)S(1)}, u32[]{:S(2)}, u32[]{:S(2)}) collective-permute-start(bf16[256,512]{1,0:T(8,128)(2,1)S(1)} %add_convert_fusion), channel_id=1, source_target_pairs={{0,3},{1,0},{2,1},{3,2},{4,7},{5,4},{6,5},{7,6},{8,11},{9,8},{10,9... | collective-permute-start | bytes 786440 | tf_op jit(solution)/shard_map/ppermute | solution.py:385

commit v5 on v4

--- a/solution.py
+++ b/solution.py
@@ -10,7 +10,7 @@
 BF16 = jnp.bfloat16
 EPS = 1e-06
 STEP_LIMIT = 300.0
-MESSAGE = (8, 256)
+MESSAGE = (2, 640)
 
 
 def dot(first, second, over=(1, 0)):
@@ -147,7 +147,7 @@
     local_out[...] = skip[...] * values.astype(F32) + read_out(
         jnp.concatenate(states_real, axis=1), jnp.concatenate(states_imag, axis=1), read
     )
-    rows, lanes = MESSAGE
+    lanes = MESSAGE[1] - width
     pick = (width, lanes)
     compress = ones_where(
         (iota(pick, 0) == (iota(pick, 1) % groups) * states) & (iota(pick, 1) < 3 * groups), BF16
@@ -156,41 +156,32 @@
     first, second, third = [part[None] for part in dot(total, compress)]
     lane = iota(first.shape, 1)
     total = jnp.where(lane < groups, first, jnp.where(lane < 2 * groups, second, third))
-    per = lanes // 128
     lines = [
-        jnp.concatenate([s[length - 1 :] for s in part[k : k + per]], axis=1)
-        for part in (states_real, states_imag)
-        for k in range(0, len(part), per)
+        jnp.concatenate([s[length - 1 :] for s in part] + [last], axis=1)
+        for part, last in ((states_real, total), (states_imag, jnp.zeros_like(total)))
     ]
-    lines.append(total)
-    lines.append(jnp.zeros((rows - len(lines), lanes), F32))
-    sent = jnp.concatenate(lines, axis=0).astype(BF16)
-    message[...] = jnp.broadcast_to(sent[None], message.shape)
+    sent = jnp.concatenate(lines, axis=0)
+    message[...] = jnp.broadcast_to(sent[None], message.shape).astype(BF16)
 
 
 def carry_kernel(
-    got, rates, read, cum_real, cum_imag, local_out, ids, logits, mixed, place, weigh
+    got, rates, read, cum_real, cum_imag, local_out, out_weight, ids, logits,
+    partial, place, weigh,
 ):
     routing(ids, logits, place, weigh)
-    rows, lanes = MESSAGE
-    devices = got.shape[0] // rows
+    devices = got.shape[0]
     width = rates.shape[1]
+    lanes = MESSAGE[1] - width
     groups = 8
     states = width // groups
     mine = lax.axis_index("sp")
     decay, freq = (rates[0:1, :], rates[1:2, :])
-    per = width // lanes
-    used = 2 * per + 1
-    pick = (used * devices, devices * rows)
-    line, column = (iota(pick, 0), iota(pick, 1))
-    chosen = ones_where(column == (line % devices) * rows + line // devices, BF16)
-    lines = dot(chosen, got[...])
-    lines = [lines[k * devices : (k + 1) * devices] for k in range(used)]
-    got_real = jnp.concatenate(lines[:per], axis=1)
-    got_imag = jnp.concatenate(lines[per : 2 * per], axis=1)
+    everything = got[...].astype(F32)
+    got_real, got_imag = (everything[:, 0, :width], everything[:, 1, :width])
+    totals = everything[:, 0, width:]
     square = (devices, devices)
     between = (iota(square, 0) < iota(square, 1)) & (iota(square, 1) < mine)
-    sums = dot(ones_where(between, BF16), lines[2 * per].astype(BF16))
+    sums = dot(ones_where(between, BF16), totals.astype(BF16))
     wide = (lanes, width)
     spread = ones_where(
         (iota(wide, 0) < 3 * groups) & (iota(wide, 0) % groups == iota(wide, 1) // states), BF16
@@ -208,7 +199,8 @@
     result = local_out[...] + read_out(
         c_real * carry_real - c_imag * carry_imag, c_real * carry_imag + c_imag * carry_real, read
     )
-    mixed[...] = jax.nn.gelu(result).astype(BF16)
+    mixed = jax.nn.gelu(result).astype(BF16)
+    partial[...] = dot(mixed, out_weight[...]).astype(BF16)
 
 
 def routing(ids, logits, place, weigh):
@@ -245,17 +237,9 @@
     return values * lax.rsqrt(jnp.mean(values * values, axis=-1, keepdims=True) + EPS) * gain
 
 
-def project_kernel(
-    tokens, weight_0, weight_1, weight_2, weight_3, residual, post_gain, pre_gain, place,
-    stream, outgoing,
-):
+def project_kernel(parts, residual, post_gain, pre_gain, place, stream, outgoing):
     rows, width = residual.shape
-    quarter = lax.axis_index("tp")
-    projected = jnp.zeros((rows, width), F32)
-    for by, weight in enumerate((weight_0, weight_1, weight_2, weight_3)):
-        source = lax.rem(quarter + 4 - by, 4)
-        part = tokens[pl.ds(pl.multiple_of(source * rows, rows), rows), :]
-        projected = projected + dot(part, weight[...])
+    projected = sum(parts[k * rows : (k + 1) * rows, :].astype(F32) for k in range(4))
     own = (residual[...].astype(F32) + normalized(projected, post_gain[...])).astype(BF16)
     stream[...] = own
     normed = normalized(own.astype(F32), pre_gain[...]).astype(BF16)
@@ -458,7 +442,6 @@
     length, wide = (mixer_input.shape[0], decay_real.size)
     channels = mixer_input.shape[1]
     slots = 2 * devices
-    gathered = [out_weight, *(shifted(out_weight, by) for by in range(1, quarters))]
     message, rates, read, cum_real, cum_imag, local_out = call(
         mixer_kernel,
         [
@@ -487,26 +470,26 @@
         flops=10**9,
     )
     got = across_sp(message)
-    mixed, place, weigh = call(
+    partial, place, weigh = call(
         carry_kernel,
         [
-            ((length, channels), BF16),
+            ((length, width), BF16),
             ((4 * slots, slots), BF16),
             ((3 * slots, 4 * slots), BF16),
         ],
-        got.reshape(-1, MESSAGE[1]), rates, read, cum_real, cum_imag, local_out,
+        got, rates, read, cum_real, cum_imag, local_out,
+        out_weight,
         route_ids.T,
         route_logits.T,
         flops=10**9,
     )
-    tokens = lax.all_to_all(
-        mixed.reshape(quarters, rows, channels), "tp", split_axis=0, concat_axis=0, tiled=True
+    parts = lax.all_to_all(
+        partial.reshape(quarters, rows, width), "tp", split_axis=0, concat_axis=0, tiled=True
     )
     stream, outgoing = call(
         project_kernel,
         [((rows, width), BF16), ((4 * slots, width // 4), BF16)],
-        tokens.reshape(-1, channels),
-        *gathered,
+        parts.reshape(-1, width),
         residual,
         post_gain[None],
         pre_gain[None],

time: 145 us -> 136 us (0.938)
  blocking collectives: 56.4 us -> 88.1 us
  starting transfers between devices: 40.6 us -> 15.4 us
  waiting for transfers between devices: 24.1 us -> 11.7 us
  local copies, waits for them, and re-layouts: 2.47 us -> 0.06 us
  Pallas kernels: 21.2 us -> 19.7 us
    all_to_all x2 -> x3, blocking collectives: 56.4 us -> 75.5 us  [across_sp(): return lax.all_to_all(pieces, 'sp', split_axis=0, concat_axis=0, tiled=True)]
    all_to_all x2 -> x0, starting transfers between devices: 17.2 us -> none  [the longest x1 13 us: across_sp(): return lax.all_to_all(pieces, 'sp', split_axis=0, concat_axis=0, tiled=True)]
    all_to_all x0 -> x1, blocking collectives: none -> 12.6 us  [on_device(): lax.all_to_all(partial.reshape(quarters, rows, width), 'tp', split_axis=0...]
    ppermute x15 -> x12, starting transfers between devices: 23.4 us -> 15.4 us  [shifted(): return lax.ppermute(part, 'tp', [(i, (i + by) % size) for i in range(size)])]
    all_to_all x2 -> x0, waiting for transfers between devices: 7.56 us -> none  [the longest x1 7.39 us: across_sp(): return lax.all_to_all(pieces, 'sp', split_axis=0, concat_axis=0, tiled=True)]
    ppermute x15 -> x12, waiting for transfers between devices: 16.6 us -> 11.7 us  [shifted(): return lax.ppermute(part, 'tp', [(i, (i + by) % size) for i in range(size)])]
    unnamed x22 -> x14, local copies, waits for them, and re-layouts: 2.43 us -> 0.03 us
    pallas_call x9, Pallas kernels: 21.2 us -> 19.7 us  [call(): pl.pallas_call(kernel, out_shape=shapes, in_specs=[left if k in in_place...]
  transfers between devices with their start and end apart: 17 -> 12, of which waited for: 7 -> 4; matrix products, arithmetic and copies ran while one was open for 0% -> 0% of each run, Pallas kernels for 10% -> 9%
where the time goes in v5:
time: 136 us; the launch traced here: 135 us
  blocking collectives  88.1 us (65%)
  Pallas kernels  19.7 us (14%)
  starting transfers between devices  15.4 us (11%)
  waiting for transfers between devices  11.7 us (9%)
    all_to_all x3, blocking collectives, across_sp(): return lax.all_to_all(pieces, 'sp', split_axis=0, concat_axis=0, tiled=True)  75.5 us
    pallas_call x9, Pallas kernels, call(): pl.pallas_call(kernel, out_shape=shapes, in_specs=[left if k in in_place...  19.7 us
    ppermute x12, starting transfers between devices, shifted(): return lax.ppermute(part, 'tp', [(i, (i + by) % size) for i in range(size)])  15.4 us
    all_to_all x1, blocking collectives, on_device(): lax.all_to_all(partial.reshape(quarters, rows, width), 'tp', split_axis=0...  12.6 us
    ppermute x12, waiting for transfers between devices, shifted(): return lax.ppermute(part, 'tp', [(i, (i + by) % size) for i in range(size)])  11.7 us
  transfers between devices with their start and end apart: 12, of which 4 were waited for; matrix products, arithmetic and copies ran while one was open for 0% of the time, Pallas kernels for 9%

profile of v5, /device:TPU:1, one launch (start us, length us, event | category | flops | bytes accessed | tf_op | source)
XLA Modules:
  0.0 135.4 jit_solution(14495503582985498258)
XLA Ops:
  0.0 0.0 copy-start.1
  0.0 0.0 copy-start.2
  0.0 0.0 copy-start.3
  0.0 3.5 %shard_map.190 = (bf16[64,2,640]{2,1,0:T(2,128)(2,1)S(1)}, f32[8,512]{1,0:T(8,128)S(1)}, bf16[1024,256]{1,0:T(8,128)(2,1)S(1)}, f32[128,512]{1,0:T(8,128)S(1)}, ...) custom-call(f32[8,128]{1,0:T(8,128)} %bitcast.31, bf16[128,128]{1,0:T(8,128)(2,1)} %inputs.1, f32[1,8]{1,0:T(1,128)} %bitcast.32, ...), custom_call_target="tpu_custom_call" | custom-call | flops 1000000000 | tf_op jit(solution)/shard_map/pallas_call | solution.py:344
  3.5 24.4 %all_to_all.20.got = bf16[64,2,640]{2,1,0:T(2,128)(2,1)S(1)} all-to-all(bf16[64,2,640]{2,1,0:T(2,128)(2,1)S(1)} %get-tuple-element.27), channel_id=1, replica_groups=mesh['sp'=64,'tp'=4] {'sp'}, dimensions={0} | all-to-all | bytes 327680 | tf_op jit(solution)/shard_map/all_to_all | solution.py:364
  28.0 0.0 copy-done.6
  28.0 0.0 copy-done.5
  28.0 0.0 copy-done
  28.0 1.7 %shard_map.191 = (bf16[128,2048]{1,0:T(8,128)(2,1)S(1)}, bf16[512,128]{1,0:T(8,128)(2,1)S(1)}, bf16[384,512]{1,0:T(8,128)(2,1)S(1)}) custom-call(bf16[64,2,640]{2,1,0:T(2,128)(2,1)S(1)} %all_to_all.20.got, f32[8,512]{1,0:T(8,128)S(1)} %get-tuple-element.28.rates, bf16[1024,256]{1,0:T(8,128)(2,1)S(1)} %get-tuple-element.29.read, ...), custom_call_target="tpu_custom_call" | custom-call | flops 1000000000 | tf_op jit(solution)/shard_map/pallas_call | solution.py:344
  29.6 12.6 %all_to_all.21 = bf16[4,32,2048]{2,1,0:T(8,128)(2,1)S(1)} all-to-all(bf16[4,32,2048]{2,1,0:T(8,128)(2,1)S(1)} %bitcast.20), channel_id=1, replica_groups=mesh['sp'=64,'tp'=4] {'tp'}, dimensions={0} | all-to-all | bytes 1048576 | tf_op jit(solution)/shard_map/all_to_all | solution.py:486
  42.2 0.0 copy-done.1
  42.2 0.6 shard_map.192
  42.8 22.9 %all_to_all.22 = bf16[64,8,512]{2,1,0:T(8,128)(2,1)S(1)} all-to-all(bf16[64,8,512]{2,1,0:T(8,128)(2,1)S(1)} %bitcast.23), channel_id=1, replica_groups=mesh['sp'=64,'tp'=4] {'sp'}, dimensions={0} | all-to-all | bytes 1048576 | tf_op jit(solution)/shard_map/all_to_all | solution.py:364
  65.8 1.0 collective-permute-start.4
  66.8 0.6 collective-permute-start.2
  67.4 6.0 %collective-permute-done.4.refs_1_ = bf16[256,512]{1,0:T(8,128)(2,1)S(1)} collective-permute-done((bf16[256,512]{1,0:T(8,128)(2,1)S(1)}, bf16[256,512]{1,0:T(8,128)(2,1)S(1)}, u32[]{:S(2)}, u32[]{:S(2)}) %collective-permute-start.4) | collective-permute-done | bytes 262176 | tf_op jit(solution)/shard_map/ppermute | solution.py:369
  73.4 2.1 %collective-permute-start.5 = (bf16[256,512]{1,0:T(8,128)(2,1)S(1)}, bf16[256,512]{1,0:T(8,128)(2,1)S(1)}, u32[]{:S(2)}, u32[]{:S(2)}) collective-permute-start(bf16[256,512]{1,0:T(8,128)(2,1)S(1)} %collective-permute-done.4.refs_1_), channel_id=1, source_target_pairs={{0,3},{1,0},{2,1},{3,2},{4,7},{5,4},{6,5},{7,6},{8,11},{9,8},{10,9... | collective-permute-start | bytes 786440 | tf_op jit(solution)/shard_map/ppermute | solution.py:369
  75.5 0.0 collective-permute-done.2.refs_0_
  75.5 0.0 collective-permute-start.3
  75.5 0.0 collective-permute-start
  75.5 2.7 %collective-permute-start.1 = (bf16[256,512]{1,0:T(8,128)(2,1)S(1)}, bf16[256,512]{1,0:T(8,128)(2,1)S(1)}, u32[]{:S(2)}, u32[]{:S(2)}) collective-permute-start(bf16[256,512]{1,0:T(8,128)(2,1)S(1)} %get-tuple-element.50.first), channel_id=1, source_target_pairs={{0,3},{1,0},{2,1},{3,2},{4,7},{5,4},{6,5},{7,6},{8,11},{9,8},{10,9... | collective-permute-start | bytes 786440 | tf_op jit(solution)/shard_map/ppermute | solution.py:369
  78.2 5.5 %shard_map.193 = (bf16[256,512]{1,0:T(8,128)(2,1)S(1)}, bf16[256,512]{1,0:T(8,128)(2,1)S(1)}, bf16[1,2048,896]{2,1,0:T(8,128)(2,1)S(1)}, bf16[1,2048,896]{2,1,0:T(8,128)(2,1)S(1)}, bf16[1,896,2048]{2,1,0:T(8,128)(2,1)S(1)}) custom-call(bf16[256,512]{1,0:T(8,128)(2,1)S(1)} %get-tuple-element.50.first, bf16[256,512]{1,0:T(8,128)(2,1)S(1)} %get-tuple-element.49.last, ...), custom_call_target="tpu_custom_call" | custom-call | flops 1409286144 | tf_op jit(solution)/shard_map/pallas_call | solution.py:344
  83.6 0.0 collective-permute-done.5.refs_1_
  83.6 0.0 collective-permute-done.3.refs_0_
  83.6 2.4 %shard_map.195 = (bf16[256,512]{1,0:T(8,128)(2,1)S(1)}, bf16[256,512]{1,0:T(8,128)(2,1)S(1)}) custom-call(bf16[256,512]{1,0:T(8,128)(2,1)S(1)} %collective-permute-done.3.refs_0_, bf16[256,512]{1,0:T(8,128)(2,1)S(1)} %collective-permute-done.5.refs_1_, bf16[1,2048,896]{2,1,0:T(8,128)(2,1)S(1)} %get-tuple-element.37.refs_2_, ...), custom_call_target="tpu_custom_call" | custom-call | flops 1409286144 | tf_op jit(solution)/shard_map/pallas_call | solution.py:344
  86.1 0.1 collective-permute-start.6
  86.1 2.4 %shard_map.196 = (bf16[256,512]{1,0:T(8,128)(2,1)S(1)}, bf16[256,512]{1,0:T(8,128)(2,1)S(1)}) custom-call(bf16[256,512]{1,0:T(8,128)(2,1)S(1)} %collective-permute-done.2.refs_0_, bf16[256,512]{1,0:T(8,128)(2,1)S(1)} %collective-permute-done.4.refs_1_, bf16[1,2048,896]{2,1,0:T(8,128)(2,1)S(1)} %get-tuple-element.37.refs_2_, ...), custom_call_target="tpu_custom_call" | custom-call | flops 1409286144 | tf_op jit(solution)/shard_map/pallas_call | solution.py:344
  88.6 2.7 %collective-permute-start.8 = (bf16[256,512]{1,0:T(8,128)(2,1)S(1)}, bf16[256,512]{1,0:T(8,128)(2,1)S(1)}, u32[]{:S(2)}, u32[]{:S(2)}) collective-permute-start(bf16[256,512]{1,0:T(8,128)(2,1)S(1)} %get-tuple-element.42), channel_id=1, source_target_pairs={{0,3},{1,0},{2,1},{3,2},{4,7},{5,4},{6,5},{7,6},{8,11},{9,8},{10,9... | collective-permute-start | bytes 786440 | tf_op jit(solution)/shard_map/ppermute | solution.py:369
  91.3 0.0 collective-permute-start.9
  91.3 0.0 collective-permute-done.refs_0_
  91.3 2.7 %collective-permute-start.10 = (bf16[256,512]{1,0:T(8,128)(2,1)S(1)}, bf16[256,512]{1,0:T(8,128)(2,1)S(1)}, u32[]{:S(2)}, u32[]{:S(2)}) collective-permute-start(bf16[256,512]{1,0:T(8,128)(2,1)S(1)} %get-tuple-element.46), channel_id=1, source_target_pairs={{0,3},{1,0},{2,1},{3,2},{4,7},{5,4},{6,5},{7,6},{8,11},{9,8},{10,9... | collective-permute-start | bytes 786440 | tf_op jit(solution)/shard_map/ppermute | solution.py:369
  94.0 0.0 collective-permute-done.1.refs_1_
  94.0 2.4 %shard_map.194 = (bf16[256,512]{1,0:T(8,128)(2,1)S(1)}, bf16[256,512]{1,0:T(8,128)(2,1)S(1)}) custom-call(bf16[256,512]{1,0:T(8,128)(2,1)S(1)} %collective-permute-done.refs_0_, bf16[256,512]{1,0:T(8,128)(2,1)S(1)} %collective-permute-done.1.refs_1_, bf16[1,2048,896]{2,1,0:T(8,128)(2,1)S(1)} %get-tuple-element.37.refs_2_, ...), custom_call_target="tpu_custom_call" | custom-call | flops 1409286144 | tf_op jit(solution)/shard_map/pallas_call | solution.py:344
  96.4 0.0 copy-start.4
  96.4 0.0 collective-permute-done.6
  96.4 0.1 add_convert_fusion.1
  96.5 0.1 collective-permute-start.7
  96.6 2.0 %collective-permute-done.10 = bf16[256,512]{1,0:T(8,128)(2,1)S(1)} collective-permute-done((bf16[256,512]{1,0:T(8,128)(2,1)S(1)}, bf16[256,512]{1,0:T(8,128)(2,1)S(1)}, u32[]{:S(2)}, u32[]{:S(2)}) %collective-permute-start.10) | collective-permute-done | bytes 262176 | tf_op jit(solution)/shard_map/ppermute | solution.py:369
  98.6 0.1 add_convert_fusion
  98.6 3.5 %collective-permute-start.11 = (bf16[256,512]{1,0:T(8,128)(2,1)S(1)}, bf16[256,512]{1,0:T(8,128)(2,1)S(1)}, u32[]{:S(2)}, u32[]{:S(2)}) collective-permute-start(bf16[256,512]{1,0:T(8,128)(2,1)S(1)} %add_convert_fusion), channel_id=1, source_target_pairs={{0,3},{1,0},{2,1},{3,2},{4,7},{5,4},{6,5},{7,6},{8,11},{9,8},{10,9... | collective-permute-start | bytes 786440 | tf_op jit(solution)/shard_map/ppermute | solution.py:369
  102.1 0.0 collective-permute-done.8.refs_2_
  102.1 0.0 collective-permute-done.9.refs_4_
  102.1 3.1 %collective-permute-done.7.refs_1_ = bf16[256,512]{1,0:T(8,128)(2,1)S(1)} collective-permute-done((bf16[256,512]{1,0:T(8,128)(2,1)S(1)}, bf16[256,512]{1,0:T(8,128)(2,1)S(1)}, u32[]{:S(2)}, u32[]{:S(2)}) %collective-permute-start.7) | collective-permute-done | bytes 262176 | tf_op jit(solution)/shard_map/ppermute | solution.py:369
  105.3 0.6 collective-permute-done.11.refs_5_
  105.8 0.2 shard_map.197
  106.0 28.1 %all_to_all.23 = bf16[64,8,512]{2,1,0:T(8,128)(2,1)S(1)} all-to-all(bf16[64,8,512]{2,1,0:T(8,128)(2,1)S(1)} %bitcast.19), channel_id=1, replica_groups=mesh['sp'=64,'tp'=4] {'sp'}, dimensions={0} | all-to-all | bytes 1048576 | tf_op jit(solution)/shard_map/all_to_all | solution.py:364
  134.2 0.0 copy-done.4
  134.2 1.2 shard_map.198
  (6 shorter events, 0.0 us)
Async XLA Ops:
  0.0 28.0 %copy-start.6 = (f32[128,2]{0,1:T(2,128)S(1)}, f32[128,2]{0,1:T(2,128)}, u32[]{:S(2)}) copy-start(f32[128,2]{0,1:T(2,128)} %param.36) | copy-start | bytes 3076
  0.0 28.0 %copy-start.5 = (s32[128,2]{0,1:T(2,128)S(1)}, s32[128,2]{0,1:T(2,128)}, u32[]{:S(2)}) copy-start(s32[128,2]{0,1:T(2,128)} %param.35) | copy-start | bytes 3076
  0.0 28.0 %copy-start = (bf16[128,2048]{1,0:T(8,128)(2,1)S(1)}, bf16[128,2048]{1,0:T(8,128)(2,1)}, u32[]{:S(2)}) copy-start(bf16[128,2048]{1,0:T(8,128)(2,1)} %out_weight.1) | copy-start | bytes 1572868
  0.0 42.2 %copy-start.1 = (bf16[32,2048]{1,0:T(8,128)(2,1)S(1)}, bf16[32,2048]{1,0:T(8,128)(2,1)}, u32[]{:S(2)}) copy-start(bf16[32,2048]{1,0:T(8,128)(2,1)} %residual.1) | copy-start | bytes 393220
  0.0 42.2 %copy-start.2 = (f32[2048]{0:T(1024)S(1)}, f32[2048]{0:T(1024)}, u32[]{:S(2)}) copy-start(f32[2048]{0:T(1024)} %param.32) | copy-start | bytes 24580
  0.0 42.2 %copy-start.3 = (f32[2048]{0:T(1024)S(1)}, f32[2048]{0:T(1024)}, u32[]{:S(2)}) copy-start(f32[2048]{0:T(1024)} %param.33) | copy-start | bytes 24580
  65.8 7.5 %collective-permute-start.4 = (bf16[256,512]{1,0:T(8,128)(2,1)S(1)}, bf16[256,512]{1,0:T(8,128)(2,1)S(1)}, u32[]{:S(2)}, u32[]{:S(2)}) collective-permute-start(bf16[256,512]{1,0:T(8,128)(2,1)S(1)} %get-tuple-element.49.last), channel_id=1, source_target_pairs={{0,3},{1,0},{2,1},{3,2},{4,7},{5,4},{6,5},{7,6},{8,11},{9,8},{10,9... | collective-permute-start | bytes 786440 | tf_op jit(solution)/shard_map/ppermute | solution.py:369
  66.8 8.7 %collective-permute-start.2 = (bf16[256,512]{1,0:T(8,128)(2,1)S(1)}, bf16[256,512]{1,0:T(8,128)(2,1)S(1)}, u32[]{:S(2)}, u32[]{:S(2)}) collective-permute-start(bf16[256,512]{1,0:T(8,128)(2,1)S(1)} %get-tuple-element.50.first), channel_id=1, source_target_pairs={{0,1},{1,2},{2,3},{3,0},{4,5},{5,6},{6,7},{7,4},{8,9},{9,10},{10,1... | collective-permute-start | bytes 786440 | tf_op jit(solution)/shard_map/ppermute | solution.py:369
  73.4 10.3 %collective-permute-start.5 = (bf16[256,512]{1,0:T(8,128)(2,1)S(1)}, bf16[256,512]{1,0:T(8,128)(2,1)S(1)}, u32[]{:S(2)}, u32[]{:S(2)}) collective-permute-start(bf16[256,512]{1,0:T(8,128)(2,1)S(1)} %collective-permute-done.4.refs_1_), channel_id=1, source_target_pairs={{0,3},{1,0},{2,1},{3,2},{4,7},{5,4},{6,5},{7,6},{8,11},{9,8},{10,9... | collective-permute-start | bytes 786440 | tf_op jit(solution)/shard_map/ppermute | solution.py:369
  75.5 8.2 %collective-permute-start.3 = (bf16[256,512]{1,0:T(8,128)(2,1)S(1)}, bf16[256,512]{1,0:T(8,128)(2,1)S(1)}, u32[]{:S(2)}, u32[]{:S(2)}) collective-permute-start(bf16[256,512]{1,0:T(8,128)(2,1)S(1)} %collective-permute-done.2.refs_0_), channel_id=1, source_target_pairs={{0,1},{1,2},{2,3},{3,0},{4,5},{5,6},{6,7},{7,4},{8,9},{9,10},{10,1... | collective-permute-start | bytes 786440 | tf_op jit(solution)/shard_map/ppermute | solution.py:369
  75.5 15.8 %collective-permute-start = (bf16[256,512]{1,0:T(8,128)(2,1)S(1)}, bf16[256,512]{1,0:T(8,128)(2,1)S(1)}, u32[]{:S(2)}, u32[]{:S(2)}) collective-permute-start(bf16[256,512]{1,0:T(8,128)(2,1)S(1)} %get-tuple-element.49.last), channel_id=1, source_target_pairs={{0,1},{1,2},{2,3},{3,0},{4,5},{5,6},{6,7},{7,4},{8,9},{9,10},{10,1... | collective-permute-start | bytes 786440 | tf_op jit(solution)/shard_map/ppermute | solution.py:369
  75.5 18.5 %collective-permute-start.1 = (bf16[256,512]{1,0:T(8,128)(2,1)S(1)}, bf16[256,512]{1,0:T(8,128)(2,1)S(1)}, u32[]{:S(2)}, u32[]{:S(2)}) collective-permute-start(bf16[256,512]{1,0:T(8,128)(2,1)S(1)} %get-tuple-element.50.first), channel_id=1, source_target_pairs={{0,3},{1,0},{2,1},{3,2},{4,7},{5,4},{6,5},{7,6},{8,11},{9,8},{10,9... | collective-permute-start | bytes 786440 | tf_op jit(solution)/shard_map/ppermute | solution.py:369
  86.1 10.4 %collective-permute-start.6 = (bf16[256,512]{1,0:T(8,128)(2,1)S(1)}, bf16[256,512]{1,0:T(8,128)(2,1)S(1)}, u32[]{:S(2)}, u32[]{:S(2)}) collective-permute-start(bf16[256,512]{1,0:T(8,128)(2,1)S(1)} %get-tuple-element.41), channel_id=1, source_target_pairs={{0,1},{1,2},{2,3},{3,0},{4,5},{5,6},{6,7},{7,4},{8,9},{9,10},{10,1... | collective-permute-start | bytes 786440 | tf_op jit(solution)/shard_map/ppermute | solution.py:369
  88.6 13.6 %collective-permute-start.8 = (bf16[256,512]{1,0:T(8,128)(2,1)S(1)}, bf16[256,512]{1,0:T(8,128)(2,1)S(1)}, u32[]{:S(2)}, u32[]{:S(2)}) collective-permute-start(bf16[256,512]{1,0:T(8,128)(2,1)S(1)} %get-tuple-element.42), channel_id=1, source_target_pairs={{0,3},{1,0},{2,1},{3,2},{4,7},{5,4},{6,5},{7,6},{8,11},{9,8},{10,9... | collective-permute-start | bytes 786440 | tf_op jit(solution)/shard_map/ppermute | solution.py:369
  91.3 10.8 %collective-permute-start.9 = (bf16[256,512]{1,0:T(8,128)(2,1)S(1)}, bf16[256,512]{1,0:T(8,128)(2,1)S(1)}, u32[]{:S(2)}, u32[]{:S(2)}) collective-permute-start(bf16[256,512]{1,0:T(8,128)(2,1)S(1)} %get-tuple-element.44), channel_id=1, source_target_pairs={{0,1},{1,2},{2,3},{3,0},{4,5},{5,6},{6,7},{7,4},{8,9},{9,10},{10,1... | collective-permute-start | bytes 786440 | tf_op jit(solution)/shard_map/ppermute | solution.py:369
  91.3 7.3 %collective-permute-start.10 = (bf16[256,512]{1,0:T(8,128)(2,1)S(1)}, bf16[256,512]{1,0:T(8,128)(2,1)S(1)}, u32[]{:S(2)}, u32[]{:S(2)}) collective-permute-start(bf16[256,512]{1,0:T(8,128)(2,1)S(1)} %get-tuple-element.46), channel_id=1, source_target_pairs={{0,3},{1,0},{2,1},{3,2},{4,7},{5,4},{6,5},{7,6},{8,11},{9,8},{10,9... | collective-permute-start | bytes 786440 | tf_op jit(solution)/shard_map/ppermute | solution.py:369
  96.4 37.8 %copy-start.4 = (f32[2048]{0:T(1024)S(1)}, f32[2048]{0:T(1024)}, u32[]{:S(2)}) copy-start(f32[2048]{0:T(1024)} %param.34) | copy-start | bytes 24580
  96.5 8.8 %collective-permute-start.7 = (bf16[256,512]{1,0:T(8,128)(2,1)S(1)}, bf16[256,512]{1,0:T(8,128)(2,1)S(1)}, u32[]{:S(2)}, u32[]{:S(2)}) collective-permute-start(bf16[256,512]{1,0:T(8,128)(2,1)S(1)} %add_convert_fusion.1), channel_id=1, source_target_pairs={{0,1},{1,2},{2,3},{3,0},{4,5},{5,6},{6,7},{7,4},{8,9},{9,10},{10,1... | collective-permute-start | bytes 786440 | tf_op jit(solution)/shard_map/ppermute | solution.py:369
  98.6 7.2 %collective-permute-start.11 = (bf16[256,512]{1,0:T(8,128)(2,1)S(1)}, bf16[256,512]{1,0:T(8,128)(2,1)S(1)}, u32[]{:S(2)}, u32[]{:S(2)}) collective-permute-start(bf16[256,512]{1,0:T(8,128)(2,1)S(1)} %add_convert_fusion), channel_id=1, source_target_pairs={{0,3},{1,0},{2,1},{3,2},{4,7},{5,4},{6,5},{7,6},{8,11},{9,8},{10,9... | collective-permute-start | bytes 786440 | tf_op jit(solution)/shard_map/ppermute | solution.py:369

commit v6 on v5

--- a/solution.py
+++ b/solution.py
@@ -79,8 +79,8 @@
 
 
 def mixer_kernel(
-    shift, inputs, log_step, decay_real, freq_imag, in_real, in_imag, out_real, out_imag, skip,
-    message, rates, read, cum_real, cum_imag, local_out,
+    shift, inputs, log_step, decay_real, freq_imag, in_real, in_imag, out_real, out_imag,
+    message, rates, read, cum_real, cum_imag, own_real, own_imag,
 ):
     groups, length = shift.shape
     states = decay_real.shape[1]
@@ -121,7 +121,7 @@
         split(jnp.concatenate([reading(out_real), -reading(out_imag)], axis=0), 2), axis=1
     )
     inverse = 1.0 / (decay * decay + freq * freq)
-    states_real, states_imag = ([], [])
+    last_real, last_imag = ([], [])
     for start in range(0, width, 128):
         cut = slice(start, start + 128)
         a_real, a_imag = rotation(decay[:, cut], freq[:, cut], step[:, cut])
@@ -142,11 +142,10 @@
             by *= 2
         cum_real[:, cut] = a_real
         cum_imag[:, cut] = a_imag
-        states_real.append(s_real)
-        states_imag.append(s_imag)
-    local_out[...] = skip[...] * values.astype(F32) + read_out(
-        jnp.concatenate(states_real, axis=1), jnp.concatenate(states_imag, axis=1), read
-    )
+        own_real[:, cut] = s_real
+        own_imag[:, cut] = s_imag
+        last_real.append(s_real[length - 1 :])
+        last_imag.append(s_imag[length - 1 :])
     lanes = MESSAGE[1] - width
     pick = (width, lanes)
     compress = ones_where(
@@ -157,16 +156,16 @@
     lane = iota(first.shape, 1)
     total = jnp.where(lane < groups, first, jnp.where(lane < 2 * groups, second, third))
     lines = [
-        jnp.concatenate([s[length - 1 :] for s in part] + [last], axis=1)
-        for part, last in ((states_real, total), (states_imag, jnp.zeros_like(total)))
+        jnp.concatenate([*part, rest], axis=1)
+        for part, rest in ((last_real, total), (last_imag, jnp.zeros_like(total)))
     ]
     sent = jnp.concatenate(lines, axis=0)
     message[...] = jnp.broadcast_to(sent[None], message.shape).astype(BF16)
 
 
 def carry_kernel(
-    got, rates, read, cum_real, cum_imag, local_out, out_weight, ids, logits,
-    partial, place, weigh,
+    got, rates, read, cum_real, cum_imag, own_real, own_imag, inputs, skip, out_weight, ids,
+    logits, kept, sent_1, sent_2, sent_3, place, weigh,
 ):
     routing(ids, logits, place, weigh)
     devices = got.shape[0]
@@ -196,11 +195,18 @@
     carry_real = jnp.sum(weight_real * got_real - weight_imag * got_imag, axis=0, keepdims=True)
     carry_imag = jnp.sum(weight_real * got_imag + weight_imag * got_real, axis=0, keepdims=True)
     c_real, c_imag = (cum_real[...], cum_imag[...])
-    result = local_out[...] + read_out(
-        c_real * carry_real - c_imag * carry_imag, c_real * carry_imag + c_imag * carry_real, read
-    )
-    mixed = jax.nn.gelu(result).astype(BF16)
-    partial[...] = dot(mixed, out_weight[...]).astype(BF16)
+    result = skip[...] * inputs[...].astype(F32) + read_out(
+        own_real[...] + (c_real * carry_real - c_imag * carry_imag),
+        own_imag[...] + (c_real * carry_imag + c_imag * carry_real),
+        read,
+    )
+    mixed = jax.nn.gelu(result)
+    rows, length = (kept.shape[0], mixed.shape[0])
+    ahead = lax.rem(length - lax.axis_index("tp") * rows, length)
+    partial = dot(pltpu.roll(mixed, ahead, 0).astype(BF16), out_weight[...])
+    kept[...] = partial[:rows]
+    for by, sent in enumerate((sent_1, sent_2, sent_3), 1):
+        sent[...] = partial[by * rows : (by + 1) * rows].astype(BF16)
 
 
 def routing(ids, logits, place, weigh):
@@ -237,9 +243,11 @@
     return values * lax.rsqrt(jnp.mean(values * values, axis=-1, keepdims=True) + EPS) * gain
 
 
-def project_kernel(parts, residual, post_gain, pre_gain, place, stream, outgoing):
-    rows, width = residual.shape
-    projected = sum(parts[k * rows : (k + 1) * rows, :].astype(F32) for k in range(4))
+def project_kernel(
+    kept, got_1, got_2, got_3, residual, post_gain, pre_gain, place, stream, outgoing
+):
+    width = residual.shape[1]
+    projected = kept[...] + sum(got[...].astype(F32) for got in (got_1, got_2, got_3))
     own = (residual[...].astype(F32) + normalized(projected, post_gain[...])).astype(BF16)
     stream[...] = own
     normed = normalized(own.astype(F32), pre_gain[...]).astype(BF16)
@@ -442,7 +450,7 @@
     length, wide = (mixer_input.shape[0], decay_real.size)
     channels = mixer_input.shape[1]
     slots = 2 * devices
-    message, rates, read, cum_real, cum_imag, local_out = call(
+    message, rates, read, cum_real, cum_imag, own_real, own_imag = call(
         mixer_kernel,
         [
             ((devices, *MESSAGE), BF16),
@@ -450,7 +458,8 @@
             ((2 * wide, 2 * channels), BF16),
             ((length, wide), F32),
             ((length, wide), F32),
-            ((length, channels), F32),
+            ((length, wide), F32),
+            ((length, wide), F32),
         ],
         *map(
             in_hbm,
@@ -464,32 +473,32 @@
                 jnp.swapaxes(in_imag, 1, 2),
                 out_real,
                 out_imag,
-                skip_gain[None],
             ),
         ),
         flops=10**9,
     )
     got = across_sp(message)
-    partial, place, weigh = call(
+    kept, *sent, place, weigh = call(
         carry_kernel,
         [
-            ((length, width), BF16),
+            ((rows, width), F32),
+            *(((rows, width), BF16),) * (quarters - 1),
             ((4 * slots, slots), BF16),
             ((3 * slots, 4 * slots), BF16),
         ],
-        got, rates, read, cum_real, cum_imag, local_out,
+        got, rates, read, cum_real, cum_imag, own_real, own_imag,
+        mixer_input,
+        skip_gain[None],
         out_weight,
         route_ids.T,
         route_logits.T,
         flops=10**9,
     )
-    parts = lax.all_to_all(
-        partial.reshape(quarters, rows, width), "tp", split_axis=0, concat_axis=0, tiled=True
-    )
     stream, outgoing = call(
         project_kernel,
         [((rows, width), BF16), ((4 * slots, width // 4), BF16)],
-        parts.reshape(-1, width),
+        kept,
+        *(shifted(part, by) for by, part in enumerate(sent, 1)),
         residual,
         post_gain[None],
         pre_gain[None],

time: 136 us -> 133 us (0.978)
  blocking collectives: 88.1 us -> 75 us
  starting transfers between devices: 15.4 us -> 21.9 us
  waiting for transfers between devices: 11.7 us -> 16.3 us
    all_to_all x1 -> x0, blocking collectives: 12.6 us -> none  [on_device(): lax.all_to_all(partial.reshape(quarters, rows, width), 'tp', split_axis=0...]
    ppermute x12 -> x15, starting transfers between devices: 15.4 us -> 21.9 us  [shifted(): return lax.ppermute(part, 'tp', [(i, (i + by) % size) for i in range(size)])]
    ppermute x12 -> x15, waiting for transfers between devices: 11.7 us -> 16.3 us  [shifted(): return lax.ppermute(part, 'tp', [(i, (i + by) % size) for i in range(size)])]
  transfers between devices with their start and end apart: 12 -> 15, of which waited for: 4 -> 6; matrix products, arithmetic and copies ran while one was open for 0% -> 0% of each run, Pallas kernels for 9% -> 10%
where the time goes in v6:
time: 133 us
  blocking collectives  75 us (56%)
  starting transfers between devices  21.9 us (16%)
  Pallas kernels  19.6 us (15%)
  waiting for transfers between devices  16.3 us (12%)
    all_to_all x3, blocking collectives, across_sp(): return lax.all_to_all(pieces, 'sp', split_axis=0, concat_axis=0, tiled=True)  75 us
    ppermute x15, starting transfers between devices, shifted(): return lax.ppermute(part, 'tp', [(i, (i + by) % size) for i in range(size)])  21.9 us
    pallas_call x9, Pallas kernels, call(): pl.pallas_call(kernel, out_shape=shapes, in_specs=[left if k in in_place...  19.6 us
    ppermute x15, waiting for transfers between devices, shifted(): return lax.ppermute(part, 'tp', [(i, (i + by) % size) for i in range(size)])  16.3 us
  transfers between devices with their start and end apart: 15, of which 6 were waited for; matrix products, arithmetic and copies ran while one was open for 0% of the time, Pallas kernels for 10%

profile of v6, /device:TPU:1, one launch (start us, length us, event | category | flops | bytes accessed | tf_op | source)
XLA Modules:
  0.0 133.1 jit_solution(15158641055972940172)
XLA Ops:
  0.1 3.3 %shard_map.190 = (bf16[64,2,640]{2,1,0:T(2,128)(2,1)S(1)}, f32[8,512]{1,0:T(8,128)S(1)}, bf16[1024,256]{1,0:T(8,128)(2,1)S(1)}, f32[128,512]{1,0:T(8,128)S(1)}, ...) custom-call(f32[8,128]{1,0:T(8,128)} %bitcast.28, bf16[128,128]{1,0:T(8,128)(2,1)} %inputs.3, ...), custom_call_target="tpu_custom_call" | custom-call | flops 1000000000 | tf_op jit(solution)/shard_map/pallas_call | solution.py:352
  3.3 24.4 %all_to_all.15.got = bf16[64,2,640]{2,1,0:T(2,128)(2,1)S(1)} all-to-all(bf16[64,2,640]{2,1,0:T(2,128)(2,1)S(1)} %get-tuple-element.31), channel_id=1, replica_groups=mesh['sp'=64,'tp'=4] {'sp'}, dimensions={0} | all-to-all | bytes 327680 | tf_op jit(solution)/shard_map/all_to_all | solution.py:372
  27.8 0.0 copy-done
  27.8 0.0 copy-done.8
  27.8 1.7 %shard_map.191 = (f32[32,2048]{1,0:T(8,128)S(1)}, bf16[32,2048]{1,0:T(8,128)(2,1)S(1)}, bf16[32,2048]{1,0:T(8,128)(2,1)S(1)}, bf16[32,2048]{1,0:T(8,128)(2,1)S(1...) custom-call(bf16[64,2,640]{2,1,0:T(2,128)(2,1)S(1)} %all_to_all.15.got, ...), custom_call_target="tpu_custom_call" | custom-call | flops 1000000000 | tf_op jit(solution)/shard_map/pallas_call | solution.py:352
  29.5 1.4 %collective-permute-start = (bf16[32,2048]{1,0:T(8,128)(2,1)S(1)}, bf16[32,2048]{1,0:T(8,128)(2,1)S(1)}, u32[]{:S(2)}, u32[]{:S(2)}) collective-permute-start(bf16[32,2048]{1,0:T(8,128)(2,1)S(1)} %get-tuple-element.39), channel_id=1, source_target_pairs={{0,1},{1,2},{2,3},{3,0},{4,5},{5,6},{6,7},{7,4},{8,9},{9,10},{10,1... | collective-permute-start | bytes 393224 | tf_op jit(solution)/shard_map/ppermute | solution.py:377
  30.9 2.6 %collective-permute-start.1 = (bf16[32,2048]{1,0:T(8,128)(2,1)S(1)}, bf16[32,2048]{1,0:T(8,128)(2,1)S(1)}, u32[]{:S(2)}, u32[]{:S(2)}) collective-permute-start(bf16[32,2048]{1,0:T(8,128)(2,1)S(1)} %get-tuple-element.40), channel_id=1, source_target_pairs={{0,2},{1,3},{2,0},{3,1},{4,6},{5,7},{6,4},{7,5},{8,10},{9,11},{10,... | collective-permute-start | bytes 393224 | tf_op jit(solution)/shard_map/ppermute | solution.py:377
  33.5 1.1 collective-permute-start.2
  34.6 1.0 collective-permute-done.got_1
  35.6 3.9 %collective-permute-done.1.got_2 = bf16[32,2048]{1,0:T(8,128)(2,1)S(1)} collective-permute-done((bf16[32,2048]{1,0:T(8,128)(2,1)S(1)}, bf16[32,2048]{1,0:T(8,128)(2,1)S(1)}, u32[]{:S(2)}, u32[]{:S(2)}) %collective-permute-start.1) | collective-permute-done | bytes 131104 | tf_op jit(solution)/shard_map/ppermute | solution.py:377
  39.5 0.0 collective-permute-done.2.got_3
  39.5 0.0 copy-done.4
  39.6 0.6 shard_map.192
  40.1 22.4 %all_to_all.16 = bf16[64,8,512]{2,1,0:T(8,128)(2,1)S(1)} all-to-all(bf16[64,8,512]{2,1,0:T(8,128)(2,1)S(1)} %bitcast.18), channel_id=1, replica_groups=mesh['sp'=64,'tp'=4] {'sp'}, dimensions={0} | all-to-all | bytes 1048576 | tf_op jit(solution)/shard_map/all_to_all | solution.py:372
  62.5 2.0 %collective-permute-start.7 = (bf16[256,512]{1,0:T(8,128)(2,1)S(1)}, bf16[256,512]{1,0:T(8,128)(2,1)S(1)}, u32[]{:S(2)}, u32[]{:S(2)}) collective-permute-start(bf16[256,512]{1,0:T(8,128)(2,1)S(1)} %get-tuple-element.57.last), channel_id=1, source_target_pairs={{0,3},{1,0},{2,1},{3,2},{4,7},{5,4},{6,5},{7,6},{8,11},{9,8},{10,9... | collective-permute-start | bytes 786440 | tf_op jit(solution)/shard_map/ppermute | solution.py:377
  64.5 0.0 collective-permute-start.5
  64.5 5.6 %collective-permute-done.7.refs_1_ = bf16[256,512]{1,0:T(8,128)(2,1)S(1)} collective-permute-done((bf16[256,512]{1,0:T(8,128)(2,1)S(1)}, bf16[256,512]{1,0:T(8,128)(2,1)S(1)}, u32[]{:S(2)}, u32[]{:S(2)}) %collective-permute-start.7) | collective-permute-done | bytes 262176 | tf_op jit(solution)/shard_map/ppermute | solution.py:377
  70.1 3.1 %collective-permute-start.8 = (bf16[256,512]{1,0:T(8,128)(2,1)S(1)}, bf16[256,512]{1,0:T(8,128)(2,1)S(1)}, u32[]{:S(2)}, u32[]{:S(2)}) collective-permute-start(bf16[256,512]{1,0:T(8,128)(2,1)S(1)} %collective-permute-done.7.refs_1_), channel_id=1, source_target_pairs={{0,3},{1,0},{2,1},{3,2},{4,7},{5,4},{6,5},{7,6},{8,11},{9,8},{10,9... | collective-permute-start | bytes 786440 | tf_op jit(solution)/shard_map/ppermute | solution.py:377
  73.2 0.0 collective-permute-done.5.refs_0_
  73.2 0.0 collective-permute-start.6
  73.2 0.0 collective-permute-start.3
  73.2 2.7 %collective-permute-start.4 = (bf16[256,512]{1,0:T(8,128)(2,1)S(1)}, bf16[256,512]{1,0:T(8,128)(2,1)S(1)}, u32[]{:S(2)}, u32[]{:S(2)}) collective-permute-start(bf16[256,512]{1,0:T(8,128)(2,1)S(1)} %get-tuple-element.58.first), channel_id=1, source_target_pairs={{0,3},{1,0},{2,1},{3,2},{4,7},{5,4},{6,5},{7,6},{8,11},{9,8},{10,9... | collective-permute-start | bytes 786440 | tf_op jit(solution)/shard_map/ppermute | solution.py:377
  75.9 5.4 %shard_map.193 = (bf16[256,512]{1,0:T(8,128)(2,1)S(1)}, bf16[256,512]{1,0:T(8,128)(2,1)S(1)}, bf16[1,2048,896]{2,1,0:T(8,128)(2,1)S(1)}, bf16[1,2048,896]{2,1,0:T(8,128)(2,1)S(1)}, bf16[1,896,2048]{2,1,0:T(8,128)(2,1)S(1)}) custom-call(bf16[256,512]{1,0:T(8,128)(2,1)S(1)} %get-tuple-element.58.first, bf16[256,512]{1,0:T(8,128)(2,1)S(1)} %get-tuple-element.57.last, ...), custom_call_target="tpu_custom_call" | custom-call | flops 1409286144 | tf_op jit(solution)/shard_map/pallas_call | solution.py:352
  81.3 0.0 collective-permute-done.8.refs_1_
  81.3 0.0 collective-permute-done.6.refs_0_
  81.4 2.4 %shard_map.195 = (bf16[256,512]{1,0:T(8,128)(2,1)S(1)}, bf16[256,512]{1,0:T(8,128)(2,1)S(1)}) custom-call(bf16[256,512]{1,0:T(8,128)(2,1)S(1)} %collective-permute-done.6.refs_0_, bf16[256,512]{1,0:T(8,128)(2,1)S(1)} %collective-permute-done.8.refs_1_, bf16[1,2048,896]{2,1,0:T(8,128)(2,1)S(1)} %get-tuple-element.45.refs_2_, ...), custom_call_target="tpu_custom_call" | custom-call | flops 1409286144 | tf_op jit(solution)/shard_map/pallas_call | solution.py:352
  83.8 0.1 collective-permute-start.9
  83.9 2.4 %shard_map.196 = (bf16[256,512]{1,0:T(8,128)(2,1)S(1)}, bf16[256,512]{1,0:T(8,128)(2,1)S(1)}) custom-call(bf16[256,512]{1,0:T(8,128)(2,1)S(1)} %collective-permute-done.5.refs_0_, bf16[256,512]{1,0:T(8,128)(2,1)S(1)} %collective-permute-done.7.refs_1_, bf16[1,2048,896]{2,1,0:T(8,128)(2,1)S(1)} %get-tuple-element.45.refs_2_, ...), custom_call_target="tpu_custom_call" | custom-call | flops 1409286144 | tf_op jit(solution)/shard_map/pallas_call | solution.py:352
  86.3 2.7 %collective-permute-start.11 = (bf16[256,512]{1,0:T(8,128)(2,1)S(1)}, bf16[256,512]{1,0:T(8,128)(2,1)S(1)}, u32[]{:S(2)}, u32[]{:S(2)}) collective-permute-start(bf16[256,512]{1,0:T(8,128)(2,1)S(1)} %get-tuple-element.50), channel_id=1, source_target_pairs={{0,3},{1,0},{2,1},{3,2},{4,7},{5,4},{6,5},{7,6},{8,11},{9,8},{10,9... | collective-permute-start | bytes 786440 | tf_op jit(solution)/shard_map/ppermute | solution.py:377
  89.0 0.0 collective-permute-start.12
  89.0 0.0 collective-permute-done.3.refs_0_
  89.0 2.7 %collective-permute-start.13 = (bf16[256,512]{1,0:T(8,128)(2,1)S(1)}, bf16[256,512]{1,0:T(8,128)(2,1)S(1)}, u32[]{:S(2)}, u32[]{:S(2)}) collective-permute-start(bf16[256,512]{1,0:T(8,128)(2,1)S(1)} %get-tuple-element.54), channel_id=1, source_target_pairs={{0,3},{1,0},{2,1},{3,2},{4,7},{5,4},{6,5},{7,6},{8,11},{9,8},{10,9... | collective-permute-start | bytes 786440 | tf_op jit(solution)/shard_map/ppermute | solution.py:377
  91.7 0.0 collective-permute-done.4.refs_1_
  91.7 2.4 %shard_map.194 = (bf16[256,512]{1,0:T(8,128)(2,1)S(1)}, bf16[256,512]{1,0:T(8,128)(2,1)S(1)}) custom-call(bf16[256,512]{1,0:T(8,128)(2,1)S(1)} %collective-permute-done.3.refs_0_, bf16[256,512]{1,0:T(8,128)(2,1)S(1)} %collective-permute-done.4.refs_1_, bf16[1,2048,896]{2,1,0:T(8,128)(2,1)S(1)} %get-tuple-element.45.refs_2_, ...), custom_call_target="tpu_custom_call" | custom-call | flops 1409286144 | tf_op jit(solution)/shard_map/pallas_call | solution.py:352
  94.1 0.0 copy-start.5
  94.1 0.0 collective-permute-done.9
  94.1 0.1 add_convert_fusion.1
  94.2 0.1 collective-permute-start.10
  94.3 2.0 %collective-permute-done.13 = bf16[256,512]{1,0:T(8,128)(2,1)S(1)} collective-permute-done((bf16[256,512]{1,0:T(8,128)(2,1)S(1)}, bf16[256,512]{1,0:T(8,128)(2,1)S(1)}, u32[]{:S(2)}, u32[]{:S(2)}) %collective-permute-start.13) | collective-permute-done | bytes 262176 | tf_op jit(solution)/shard_map/ppermute | solution.py:377
  96.3 0.1 add_convert_fusion
  96.3 3.5 %collective-permute-start.14 = (bf16[256,512]{1,0:T(8,128)(2,1)S(1)}, bf16[256,512]{1,0:T(8,128)(2,1)S(1)}, u32[]{:S(2)}, u32[]{:S(2)}) collective-permute-start(bf16[256,512]{1,0:T(8,128)(2,1)S(1)} %add_convert_fusion), channel_id=1, source_target_pairs={{0,3},{1,0},{2,1},{3,2},{4,7},{5,4},{6,5},{7,6},{8,11},{9,8},{10,9... | collective-permute-start | bytes 786440 | tf_op jit(solution)/shard_map/ppermute | solution.py:377
  99.8 0.0 collective-permute-done.11.refs_2_
  99.8 0.0 collective-permute-done.12.refs_4_
  99.8 3.2 %collective-permute-done.10.refs_1_ = bf16[256,512]{1,0:T(8,128)(2,1)S(1)} collective-permute-done((bf16[256,512]{1,0:T(8,128)(2,1)S(1)}, bf16[256,512]{1,0:T(8,128)(2,1)S(1)}, u32[]{:S(2)}, u32[]{:S(2)}) %collective-permute-start.10) | collective-permute-done | bytes 262176 | tf_op jit(solution)/shard_map/ppermute | solution.py:377
  103.0 0.5 collective-permute-done.14.refs_5_
  103.6 0.2 shard_map.197
  103.8 28.2 %all_to_all.17 = bf16[64,8,512]{2,1,0:T(8,128)(2,1)S(1)} all-to-all(bf16[64,8,512]{2,1,0:T(8,128)(2,1)S(1)} %bitcast.17), channel_id=1, replica_groups=mesh['sp'=64,'tp'=4] {'sp'}, dimensions={0} | all-to-all | bytes 1048576 | tf_op jit(solution)/shard_map/all_to_all | solution.py:372
  131.9 1.2 shard_map.198
  (15 shorter events, 0.1 us)
Async XLA Ops:
  0.0 27.8 %copy-start.2 = (bf16[128,128]{1,0:T(8,128)(2,1)S(1)}, bf16[128,128]{1,0:T(8,128)(2,1)}, u32[]{:S(2)}) copy-start(bf16[128,128]{1,0:T(8,128)(2,1)} %inputs.3) | copy-start | bytes 98308
  0.0 27.8 %copy-start.7 = (f32[128,2]{0,1:T(2,128)S(1)}, f32[128,2]{0,1:T(2,128)}, u32[]{:S(2)}) copy-start(f32[128,2]{0,1:T(2,128)} %param.36) | copy-start | bytes 3076
  0.0 27.8 %copy-start.6 = (s32[128,2]{0,1:T(2,128)S(1)}, s32[128,2]{0,1:T(2,128)}, u32[]{:S(2)}) copy-start(s32[128,2]{0,1:T(2,128)} %param.35) | copy-start | bytes 3076
  0.0 27.8 %copy-start = (bf16[128,2048]{1,0:T(8,128)(2,1)S(1)}, bf16[128,2048]{1,0:T(8,128)(2,1)}, u32[]{:S(2)}) copy-start(bf16[128,2048]{1,0:T(8,128)(2,1)} %out_weight.1) | copy-start | bytes 1572868
  0.0 27.8 %copy-start.8 = (f32[128]{0:T(128)S(1)}, f32[128]{0:T(128)}, u32[]{:S(2)}) copy-start(f32[128]{0:T(128)} %param.29) | copy-start | bytes 1540
  0.0 39.5 %copy-start.1 = (bf16[32,2048]{1,0:T(8,128)(2,1)S(1)}, bf16[32,2048]{1,0:T(8,128)(2,1)}, u32[]{:S(2)}) copy-start(bf16[32,2048]{1,0:T(8,128)(2,1)} %residual.1) | copy-start | bytes 393220
  0.0 39.5 %copy-start.3 = (f32[2048]{0:T(1024)S(1)}, f32[2048]{0:T(1024)}, u32[]{:S(2)}) copy-start(f32[2048]{0:T(1024)} %param.32) | copy-start | bytes 24580
  0.0 39.5 %copy-start.4 = (f32[2048]{0:T(1024)S(1)}, f32[2048]{0:T(1024)}, u32[]{:S(2)}) copy-start(f32[2048]{0:T(1024)} %param.33) | copy-start | bytes 24580
  29.5 6.1 %collective-permute-start = (bf16[32,2048]{1,0:T(8,128)(2,1)S(1)}, bf16[32,2048]{1,0:T(8,128)(2,1)S(1)}, u32[]{:S(2)}, u32[]{:S(2)}) collective-permute-start(bf16[32,2048]{1,0:T(8,128)(2,1)S(1)} %get-tuple-element.39), channel_id=1, source_target_pairs={{0,1},{1,2},{2,3},{3,0},{4,5},{5,6},{6,7},{7,4},{8,9},{9,10},{10,1... | collective-permute-start | bytes 393224 | tf_op jit(solution)/shard_map/ppermute | solution.py:377
  30.9 8.6 %collective-permute-start.1 = (bf16[32,2048]{1,0:T(8,128)(2,1)S(1)}, bf16[32,2048]{1,0:T(8,128)(2,1)S(1)}, u32[]{:S(2)}, u32[]{:S(2)}) collective-permute-start(bf16[32,2048]{1,0:T(8,128)(2,1)S(1)} %get-tuple-element.40), channel_id=1, source_target_pairs={{0,2},{1,3},{2,0},{3,1},{4,6},{5,7},{6,4},{7,5},{8,10},{9,11},{10,... | collective-permute-start | bytes 393224 | tf_op jit(solution)/shard_map/ppermute | solution.py:377
  33.5 6.0 %collective-permute-start.2 = (bf16[32,2048]{1,0:T(8,128)(2,1)S(1)}, bf16[32,2048]{1,0:T(8,128)(2,1)S(1)}, u32[]{:S(2)}, u32[]{:S(2)}) collective-permute-start(bf16[32,2048]{1,0:T(8,128)(2,1)S(1)} %get-tuple-element.41), channel_id=1, source_target_pairs={{0,3},{1,0},{2,1},{3,2},{4,7},{5,4},{6,5},{7,6},{8,11},{9,8},{10,9... | collective-permute-start | bytes 393224 | tf_op jit(solution)/shard_map/ppermute | solution.py:377
  62.5 7.5 %collective-permute-start.7 = (bf16[256,512]{1,0:T(8,128)(2,1)S(1)}, bf16[256,512]{1,0:T(8,128)(2,1)S(1)}, u32[]{:S(2)}, u32[]{:S(2)}) collective-permute-start(bf16[256,512]{1,0:T(8,128)(2,1)S(1)} %get-tuple-element.57.last), channel_id=1, source_target_pairs={{0,3},{1,0},{2,1},{3,2},{4,7},{5,4},{6,5},{7,6},{8,11},{9,8},{10,9... | collective-permute-start | bytes 786440 | tf_op jit(solution)/shard_map/ppermute | solution.py:377
  64.5 8.7 %collective-permute-start.5 = (bf16[256,512]{1,0:T(8,128)(2,1)S(1)}, bf16[256,512]{1,0:T(8,128)(2,1)S(1)}, u32[]{:S(2)}, u32[]{:S(2)}) collective-permute-start(bf16[256,512]{1,0:T(8,128)(2,1)S(1)} %get-tuple-element.58.first), channel_id=1, source_target_pairs={{0,1},{1,2},{2,3},{3,0},{4,5},{5,6},{6,7},{7,4},{8,9},{9,10},{10,1... | collective-permute-start | bytes 786440 | tf_op jit(solution)/shard_map/ppermute | solution.py:377
  70.1 11.2 %collective-permute-start.8 = (bf16[256,512]{1,0:T(8,128)(2,1)S(1)}, bf16[256,512]{1,0:T(8,128)(2,1)S(1)}, u32[]{:S(2)}, u32[]{:S(2)}) collective-permute-start(bf16[256,512]{1,0:T(8,128)(2,1)S(1)} %collective-permute-done.7.refs_1_), channel_id=1, source_target_pairs={{0,3},{1,0},{2,1},{3,2},{4,7},{5,4},{6,5},{7,6},{8,11},{9,8},{10,9... | collective-permute-start | bytes 786440 | tf_op jit(solution)/shard_map/ppermute | solution.py:377
  73.2 8.2 %collective-permute-start.6 = (bf16[256,512]{1,0:T(8,128)(2,1)S(1)}, bf16[256,512]{1,0:T(8,128)(2,1)S(1)}, u32[]{:S(2)}, u32[]{:S(2)}) collective-permute-start(bf16[256,512]{1,0:T(8,128)(2,1)S(1)} %collective-permute-done.5.refs_0_), channel_id=1, source_target_pairs={{0,1},{1,2},{2,3},{3,0},{4,5},{5,6},{6,7},{7,4},{8,9},{9,10},{10,1... | collective-permute-start | bytes 786440 | tf_op jit(solution)/shard_map/ppermute | solution.py:377
  73.2 15.8 %collective-permute-start.3 = (bf16[256,512]{1,0:T(8,128)(2,1)S(1)}, bf16[256,512]{1,0:T(8,128)(2,1)S(1)}, u32[]{:S(2)}, u32[]{:S(2)}) collective-permute-start(bf16[256,512]{1,0:T(8,128)(2,1)S(1)} %get-tuple-element.57.last), channel_id=1, source_target_pairs={{0,1},{1,2},{2,3},{3,0},{4,5},{5,6},{6,7},{7,4},{8,9},{9,10},{10,1... | collective-permute-start | bytes 786440 | tf_op jit(solution)/shard_map/ppermute | solution.py:377
  73.2 18.5 %collective-permute-start.4 = (bf16[256,512]{1,0:T(8,128)(2,1)S(1)}, bf16[256,512]{1,0:T(8,128)(2,1)S(1)}, u32[]{:S(2)}, u32[]{:S(2)}) collective-permute-start(bf16[256,512]{1,0:T(8,128)(2,1)S(1)} %get-tuple-element.58.first), channel_id=1, source_target_pairs={{0,3},{1,0},{2,1},{3,2},{4,7},{5,4},{6,5},{7,6},{8,11},{9,8},{10,9... | collective-permute-start | bytes 786440 | tf_op jit(solution)/shard_map/ppermute | solution.py:377
  83.8 10.4 %collective-permute-start.9 = (bf16[256,512]{1,0:T(8,128)(2,1)S(1)}, bf16[256,512]{1,0:T(8,128)(2,1)S(1)}, u32[]{:S(2)}, u32[]{:S(2)}) collective-permute-start(bf16[256,512]{1,0:T(8,128)(2,1)S(1)} %get-tuple-element.49), channel_id=1, source_target_pairs={{0,1},{1,2},{2,3},{3,0},{4,5},{5,6},{6,7},{7,4},{8,9},{9,10},{10,1... | collective-permute-start | bytes 786440 | tf_op jit(solution)/shard_map/ppermute | solution.py:377
  86.3 13.6 %collective-permute-start.11 = (bf16[256,512]{1,0:T(8,128)(2,1)S(1)}, bf16[256,512]{1,0:T(8,128)(2,1)S(1)}, u32[]{:S(2)}, u32[]{:S(2)}) collective-permute-start(bf16[256,512]{1,0:T(8,128)(2,1)S(1)} %get-tuple-element.50), channel_id=1, source_target_pairs={{0,3},{1,0},{2,1},{3,2},{4,7},{5,4},{6,5},{7,6},{8,11},{9,8},{10,9... | collective-permute-start | bytes 786440 | tf_op jit(solution)/shard_map/ppermute | solution.py:377
  89.0 10.8 %collective-permute-start.12 = (bf16[256,512]{1,0:T(8,128)(2,1)S(1)}, bf16[256,512]{1,0:T(8,128)(2,1)S(1)}, u32[]{:S(2)}, u32[]{:S(2)}) collective-permute-start(bf16[256,512]{1,0:T(8,128)(2,1)S(1)} %get-tuple-element.52), channel_id=1, source_target_pairs={{0,1},{1,2},{2,3},{3,0},{4,5},{5,6},{6,7},{7,4},{8,9},{9,10},{10,1... | collective-permute-start | bytes 786440 | tf_op jit(solution)/shard_map/ppermute | solution.py:377
  89.0 7.2 %collective-permute-start.13 = (bf16[256,512]{1,0:T(8,128)(2,1)S(1)}, bf16[256,512]{1,0:T(8,128)(2,1)S(1)}, u32[]{:S(2)}, u32[]{:S(2)}) collective-permute-start(bf16[256,512]{1,0:T(8,128)(2,1)S(1)} %get-tuple-element.54), channel_id=1, source_target_pairs={{0,3},{1,0},{2,1},{3,2},{4,7},{5,4},{6,5},{7,6},{8,11},{9,8},{10,9... | collective-permute-start | bytes 786440 | tf_op jit(solution)/shard_map/ppermute | solution.py:377
  94.1 37.8 %copy-start.5 = (f32[2048]{0:T(1024)S(1)}, f32[2048]{0:T(1024)}, u32[]{:S(2)}) copy-start(f32[2048]{0:T(1024)} %param.34) | copy-start | bytes 24580
  94.2 8.8 %collective-permute-start.10 = (bf16[256,512]{1,0:T(8,128)(2,1)S(1)}, bf16[256,512]{1,0:T(8,128)(2,1)S(1)}, u32[]{:S(2)}, u32[]{:S(2)}) collective-permute-start(bf16[256,512]{1,0:T(8,128)(2,1)S(1)} %add_convert_fusion.1), channel_id=1, source_target_pairs={{0,1},{1,2},{2,3},{3,0},{4,5},{5,6},{6,7},{7,4},{8,9},{9,10},{10,1... | collective-permute-start | bytes 786440 | tf_op jit(solution)/shard_map/ppermute | solution.py:377
  96.3 7.2 %collective-permute-start.14 = (bf16[256,512]{1,0:T(8,128)(2,1)S(1)}, bf16[256,512]{1,0:T(8,128)(2,1)S(1)}, u32[]{:S(2)}, u32[]{:S(2)}) collective-permute-start(bf16[256,512]{1,0:T(8,128)(2,1)S(1)} %add_convert_fusion), channel_id=1, source_target_pairs={{0,3},{1,0},{2,1},{3,2},{4,7},{5,4},{6,5},{7,6},{8,11},{9,8},{10,9... | collective-permute-start | bytes 786440 | tf_op jit(solution)/shard_map/ppermute | solution.py:377

commit v7 on v6

--- a/solution.py
+++ b/solution.py
@@ -164,10 +164,9 @@
 
 
 def carry_kernel(
-    got, rates, read, cum_real, cum_imag, own_real, own_imag, inputs, skip, out_weight, ids,
-    logits, kept, sent_1, sent_2, sent_3, place, weigh,
+    got, rates, read, cum_real, cum_imag, own_real, own_imag, inputs, skip, out_weight,
+    kept, sent_1, sent_2, sent_3,
 ):
-    routing(ids, logits, place, weigh)
     devices = got.shape[0]
     width = rates.shape[1]
     lanes = MESSAGE[1] - width
@@ -209,7 +208,7 @@
         sent[...] = partial[by * rows : (by + 1) * rows].astype(BF16)
 
 
-def routing(ids, logits, place, weigh):
+def route_kernel(ids, logits, place, weigh):
     slots = ids.shape[1]
     tall = (slots, slots)
     rows = slots // 4
@@ -478,21 +477,24 @@
         flops=10**9,
     )
     got = across_sp(message)
-    kept, *sent, place, weigh = call(
+    kept, *sent = call(
         carry_kernel,
         [
             ((rows, width), F32),
             *(((rows, width), BF16),) * (quarters - 1),
-            ((4 * slots, slots), BF16),
-            ((3 * slots, 4 * slots), BF16),
         ],
         got, rates, read, cum_real, cum_imag, own_real, own_imag,
         mixer_input,
         skip_gain[None],
         out_weight,
+        flops=10**9,
+    )
+    place, weigh = call(
+        route_kernel,
+        [((4 * slots, slots), BF16), ((3 * slots, 4 * slots), BF16)],
         route_ids.T,
         route_logits.T,
-        flops=10**9,
+        flops=10**8,
     )
     stream, outgoing = call(
         project_kernel,

time: 133 us -> 133 us (level)
    pallas_call x9 -> x10, Pallas kernels: 19.6 us -> 19.8 us  [call(): pl.pallas_call(kernel, out_shape=shapes, in_specs=[left if k in in_place...]
where the time goes in v7:
time: 133 us
  blocking collectives  75 us (56%)
  starting transfers between devices  21.9 us (16%)
  Pallas kernels  19.8 us (15%)
  waiting for transfers between devices  15.7 us (12%)
    all_to_all x3, blocking collectives, across_sp(): return lax.all_to_all(pieces, 'sp', split_axis=0, concat_axis=0, tiled=True)  75 us
    ppermute x15, starting transfers between devices, shifted(): return lax.ppermute(part, 'tp', [(i, (i + by) % size) for i in range(size)])  21.9 us
    pallas_call x10, Pallas kernels, call(): pl.pallas_call(kernel, out_shape=shapes, in_specs=[left if k in in_place...  19.8 us
    ppermute x15, waiting for transfers between devices, shifted(): return lax.ppermute(part, 'tp', [(i, (i + by) % size) for i in range(size)])  15.7 us
  transfers between devices with their start and end apart: 15, of which 6 were waited for; matrix products, arithmetic and copies ran while one was open for 0% of the time, Pallas kernels for 10%

profile of v7, /device:TPU:1, one launch (start us, length us, event | category | flops | bytes accessed | tf_op | source)
XLA Modules:
  0.0 132.8 jit_solution(1998122598584521577)
XLA Ops:
  0.1 3.3 %shard_map.190 = (bf16[64,2,640]{2,1,0:T(2,128)(2,1)S(1)}, f32[8,512]{1,0:T(8,128)S(1)}, bf16[1024,256]{1,0:T(8,128)(2,1)S(1)}, f32[128,512]{1,0:T(8,128)S(1)}, ...) custom-call(f32[8,128]{1,0:T(8,128)} %bitcast.28, bf16[128,128]{1,0:T(8,128)(2,1)} %inputs.3, ...), custom_call_target="tpu_custom_call" | custom-call | flops 1000000000 | tf_op jit(solution)/shard_map/pallas_call | solution.py:351
  3.3 24.4 %all_to_all.15.got = bf16[64,2,640]{2,1,0:T(2,128)(2,1)S(1)} all-to-all(bf16[64,2,640]{2,1,0:T(2,128)(2,1)S(1)} %get-tuple-element.31), channel_id=1, replica_groups=mesh['sp'=64,'tp'=4] {'sp'}, dimensions={0} | all-to-all | bytes 327680 | tf_op jit(solution)/shard_map/all_to_all | solution.py:371
  27.8 0.0 copy-done.2
  27.8 0.0 copy-done.8
  27.8 1.4 %shard_map.191 = (f32[32,2048]{1,0:T(8,128)S(1)}, bf16[32,2048]{1,0:T(8,128)(2,1)S(1)}, bf16[32,2048]{1,0:T(8,128)(2,1)S(1)}, bf16[32,2048]{1,0:T(8,128)(2,1)S(1)}) custom-call(bf16[64,2,640]{2,1,0:T(2,128)(2,1)S(1)} %all_to_all.15.got, f32[8,512]{1,0:T(8,128)S(1)} %get-tuple-element.32.rates, bf16[1024,256]{1,0:T(8,128)(2,1)S(1)} %get-tuple-element.33.read, ...), custom_call_target="tpu_custom_call" | custom-call | flops 1000000000 | tf_op jit(solution)/shard_map/pallas_call | solution.py:351
  29.2 1.4 %collective-permute-start = (bf16[32,2048]{1,0:T(8,128)(2,1)S(1)}, bf16[32,2048]{1,0:T(8,128)(2,1)S(1)}, u32[]{:S(2)}, u32[]{:S(2)}) collective-permute-start(bf16[32,2048]{1,0:T(8,128)(2,1)S(1)} %get-tuple-element.39), channel_id=1, source_target_pairs={{0,1},{1,2},{2,3},{3,0},{4,5},{5,6},{6,7},{7,4},{8,9},{9,10},{10,1... | collective-permute-start | bytes 393224 | tf_op jit(solution)/shard_map/ppermute | solution.py:376
  30.6 2.6 %collective-permute-start.1 = (bf16[32,2048]{1,0:T(8,128)(2,1)S(1)}, bf16[32,2048]{1,0:T(8,128)(2,1)S(1)}, u32[]{:S(2)}, u32[]{:S(2)}) collective-permute-start(bf16[32,2048]{1,0:T(8,128)(2,1)S(1)} %get-tuple-element.40), channel_id=1, source_target_pairs={{0,2},{1,3},{2,0},{3,1},{4,6},{5,7},{6,4},{7,5},{8,10},{9,11},{10,... | collective-permute-start | bytes 393224 | tf_op jit(solution)/shard_map/ppermute | solution.py:376
  33.2 1.1 collective-permute-start.2
  34.3 0.5 shard_map.192
  34.9 0.5 collective-permute-done.got_1
  35.3 3.9 %collective-permute-done.1.got_2 = bf16[32,2048]{1,0:T(8,128)(2,1)S(1)} collective-permute-done((bf16[32,2048]{1,0:T(8,128)(2,1)S(1)}, bf16[32,2048]{1,0:T(8,128)(2,1)S(1)}, u32[]{:S(2)}, u32[]{:S(2)}) %collective-permute-start.1) | collective-permute-done | bytes 131104 | tf_op jit(solution)/shard_map/ppermute | solution.py:376
  39.2 0.0 collective-permute-done.2.got_3
  39.3 0.6 shard_map.193
  39.8 22.4 %all_to_all.16 = bf16[64,8,512]{2,1,0:T(8,128)(2,1)S(1)} all-to-all(bf16[64,8,512]{2,1,0:T(8,128)(2,1)S(1)} %bitcast.18), channel_id=1, replica_groups=mesh['sp'=64,'tp'=4] {'sp'}, dimensions={0} | all-to-all | bytes 1048576 | tf_op jit(solution)/shard_map/all_to_all | solution.py:371
  62.2 2.0 %collective-permute-start.7 = (bf16[256,512]{1,0:T(8,128)(2,1)S(1)}, bf16[256,512]{1,0:T(8,128)(2,1)S(1)}, u32[]{:S(2)}, u32[]{:S(2)}) collective-permute-start(bf16[256,512]{1,0:T(8,128)(2,1)S(1)} %get-tuple-element.57.last), channel_id=1, source_target_pairs={{0,3},{1,0},{2,1},{3,2},{4,7},{5,4},{6,5},{7,6},{8,11},{9,8},{10,9... | collective-permute-start | bytes 786440 | tf_op jit(solution)/shard_map/ppermute | solution.py:376
  64.2 0.0 collective-permute-start.5
  64.2 5.6 %collective-permute-done.7.refs_1_ = bf16[256,512]{1,0:T(8,128)(2,1)S(1)} collective-permute-done((bf16[256,512]{1,0:T(8,128)(2,1)S(1)}, bf16[256,512]{1,0:T(8,128)(2,1)S(1)}, u32[]{:S(2)}, u32[]{:S(2)}) %collective-permute-start.7) | collective-permute-done | bytes 262176 | tf_op jit(solution)/shard_map/ppermute | solution.py:376
  69.8 3.1 %collective-permute-start.8 = (bf16[256,512]{1,0:T(8,128)(2,1)S(1)}, bf16[256,512]{1,0:T(8,128)(2,1)S(1)}, u32[]{:S(2)}, u32[]{:S(2)}) collective-permute-start(bf16[256,512]{1,0:T(8,128)(2,1)S(1)} %collective-permute-done.7.refs_1_), channel_id=1, source_target_pairs={{0,3},{1,0},{2,1},{3,2},{4,7},{5,4},{6,5},{7,6},{8,11},{9,8},{10,9... | collective-permute-start | bytes 786440 | tf_op jit(solution)/shard_map/ppermute | solution.py:376
  72.9 0.0 collective-permute-done.5.refs_0_
  72.9 0.0 collective-permute-start.6
  72.9 0.0 collective-permute-start.3
  72.9 2.7 %collective-permute-start.4 = (bf16[256,512]{1,0:T(8,128)(2,1)S(1)}, bf16[256,512]{1,0:T(8,128)(2,1)S(1)}, u32[]{:S(2)}, u32[]{:S(2)}) collective-permute-start(bf16[256,512]{1,0:T(8,128)(2,1)S(1)} %get-tuple-element.58.first), channel_id=1, source_target_pairs={{0,3},{1,0},{2,1},{3,2},{4,7},{5,4},{6,5},{7,6},{8,11},{9,8},{10,9... | collective-permute-start | bytes 786440 | tf_op jit(solution)/shard_map/ppermute | solution.py:376
  75.6 5.5 %shard_map.194 = (bf16[256,512]{1,0:T(8,128)(2,1)S(1)}, bf16[256,512]{1,0:T(8,128)(2,1)S(1)}, bf16[1,2048,896]{2,1,0:T(8,128)(2,1)S(1)}, bf16[1,2048,896]{2,1,0:T(8,128)(2,1)S(1)}, bf16[1,896,2048]{2,1,0:T(8,128)(2,1)S(1)}) custom-call(bf16[256,512]{1,0:T(8,128)(2,1)S(1)} %get-tuple-element.58.first, bf16[256,512]{1,0:T(8,128)(2,1)S(1)} %get-tuple-element.57.last, ...), custom_call_target="tpu_custom_call" | custom-call | flops 1409286144 | tf_op jit(solution)/shard_map/pallas_call | solution.py:351
  81.0 0.0 collective-permute-done.8.refs_1_
  81.1 0.0 collective-permute-done.6.refs_0_
  81.1 2.4 %shard_map.196 = (bf16[256,512]{1,0:T(8,128)(2,1)S(1)}, bf16[256,512]{1,0:T(8,128)(2,1)S(1)}) custom-call(bf16[256,512]{1,0:T(8,128)(2,1)S(1)} %collective-permute-done.6.refs_0_, bf16[256,512]{1,0:T(8,128)(2,1)S(1)} %collective-permute-done.8.refs_1_, bf16[1,2048,896]{2,1,0:T(8,128)(2,1)S(1)} %get-tuple-element.45.refs_2_, ...), custom_call_target="tpu_custom_call" | custom-call | flops 1409286144 | tf_op jit(solution)/shard_map/pallas_call | solution.py:351
  83.5 0.1 collective-permute-start.9
  83.6 2.4 %shard_map.197 = (bf16[256,512]{1,0:T(8,128)(2,1)S(1)}, bf16[256,512]{1,0:T(8,128)(2,1)S(1)}) custom-call(bf16[256,512]{1,0:T(8,128)(2,1)S(1)} %collective-permute-done.5.refs_0_, bf16[256,512]{1,0:T(8,128)(2,1)S(1)} %collective-permute-done.7.refs_1_, bf16[1,2048,896]{2,1,0:T(8,128)(2,1)S(1)} %get-tuple-element.45.refs_2_, ...), custom_call_target="tpu_custom_call" | custom-call | flops 1409286144 | tf_op jit(solution)/shard_map/pallas_call | solution.py:351
  86.0 2.7 %collective-permute-start.11 = (bf16[256,512]{1,0:T(8,128)(2,1)S(1)}, bf16[256,512]{1,0:T(8,128)(2,1)S(1)}, u32[]{:S(2)}, u32[]{:S(2)}) collective-permute-start(bf16[256,512]{1,0:T(8,128)(2,1)S(1)} %get-tuple-element.50), channel_id=1, source_target_pairs={{0,3},{1,0},{2,1},{3,2},{4,7},{5,4},{6,5},{7,6},{8,11},{9,8},{10,9... | collective-permute-start | bytes 786440 | tf_op jit(solution)/shard_map/ppermute | solution.py:376
  88.7 0.0 collective-permute-start.12
  88.7 0.0 collective-permute-done.3.refs_0_
  88.7 2.7 %collective-permute-start.13 = (bf16[256,512]{1,0:T(8,128)(2,1)S(1)}, bf16[256,512]{1,0:T(8,128)(2,1)S(1)}, u32[]{:S(2)}, u32[]{:S(2)}) collective-permute-start(bf16[256,512]{1,0:T(8,128)(2,1)S(1)} %get-tuple-element.54), channel_id=1, source_target_pairs={{0,3},{1,0},{2,1},{3,2},{4,7},{5,4},{6,5},{7,6},{8,11},{9,8},{10,9... | collective-permute-start | bytes 786440 | tf_op jit(solution)/shard_map/ppermute | solution.py:376
  91.4 0.0 collective-permute-done.4.refs_1_
  91.4 2.4 %shard_map.195 = (bf16[256,512]{1,0:T(8,128)(2,1)S(1)}, bf16[256,512]{1,0:T(8,128)(2,1)S(1)}) custom-call(bf16[256,512]{1,0:T(8,128)(2,1)S(1)} %collective-permute-done.3.refs_0_, bf16[256,512]{1,0:T(8,128)(2,1)S(1)} %collective-permute-done.4.refs_1_, bf16[1,2048,896]{2,1,0:T(8,128)(2,1)S(1)} %get-tuple-element.45.refs_2_, ...), custom_call_target="tpu_custom_call" | custom-call | flops 1409286144 | tf_op jit(solution)/shard_map/pallas_call | solution.py:351
  93.8 0.0 copy-start.5
  93.8 0.0 collective-permute-done.9
  93.8 0.1 add_convert_fusion.1
  93.9 0.1 collective-permute-start.10
  94.0 2.0 %collective-permute-done.13 = bf16[256,512]{1,0:T(8,128)(2,1)S(1)} collective-permute-done((bf16[256,512]{1,0:T(8,128)(2,1)S(1)}, bf16[256,512]{1,0:T(8,128)(2,1)S(1)}, u32[]{:S(2)}, u32[]{:S(2)}) %collective-permute-start.13) | collective-permute-done | bytes 262176 | tf_op jit(solution)/shard_map/ppermute | solution.py:376
  96.0 0.1 add_convert_fusion
  96.1 3.5 %collective-permute-start.14 = (bf16[256,512]{1,0:T(8,128)(2,1)S(1)}, bf16[256,512]{1,0:T(8,128)(2,1)S(1)}, u32[]{:S(2)}, u32[]{:S(2)}) collective-permute-start(bf16[256,512]{1,0:T(8,128)(2,1)S(1)} %add_convert_fusion), channel_id=1, source_target_pairs={{0,3},{1,0},{2,1},{3,2},{4,7},{5,4},{6,5},{7,6},{8,11},{9,8},{10,9... | collective-permute-start | bytes 786440 | tf_op jit(solution)/shard_map/ppermute | solution.py:376
  99.6 0.0 collective-permute-done.11.refs_2_
  99.6 0.0 collective-permute-done.12.refs_4_
  99.6 3.1 %collective-permute-done.10.refs_1_ = bf16[256,512]{1,0:T(8,128)(2,1)S(1)} collective-permute-done((bf16[256,512]{1,0:T(8,128)(2,1)S(1)}, bf16[256,512]{1,0:T(8,128)(2,1)S(1)}, u32[]{:S(2)}, u32[]{:S(2)}) %collective-permute-start.10) | collective-permute-done | bytes 262176 | tf_op jit(solution)/shard_map/ppermute | solution.py:376
  102.7 0.6 collective-permute-done.14.refs_5_
  103.3 0.2 shard_map.198
  103.5 28.1 %all_to_all.17 = bf16[64,8,512]{2,1,0:T(8,128)(2,1)S(1)} all-to-all(bf16[64,8,512]{2,1,0:T(8,128)(2,1)S(1)} %bitcast.17), channel_id=1, replica_groups=mesh['sp'=64,'tp'=4] {'sp'}, dimensions={0} | all-to-all | bytes 1048576 | tf_op jit(solution)/shard_map/all_to_all | solution.py:371
  131.6 1.2 shard_map.199
  (16 shorter events, 0.1 us)
Async XLA Ops:
  0.0 27.8 %copy-start.2 = (bf16[128,128]{1,0:T(8,128)(2,1)S(1)}, bf16[128,128]{1,0:T(8,128)(2,1)}, u32[]{:S(2)}) copy-start(bf16[128,128]{1,0:T(8,128)(2,1)} %inputs.3) | copy-start | bytes 98308
  0.0 27.8 %copy-start = (bf16[128,2048]{1,0:T(8,128)(2,1)S(1)}, bf16[128,2048]{1,0:T(8,128)(2,1)}, u32[]{:S(2)}) copy-start(bf16[128,2048]{1,0:T(8,128)(2,1)} %out_weight.1) | copy-start | bytes 1572868
  0.0 27.8 %copy-start.8 = (f32[128]{0:T(128)S(1)}, f32[128]{0:T(128)}, u32[]{:S(2)}) copy-start(f32[128]{0:T(128)} %param.29) | copy-start | bytes 1540
  0.0 34.3 %copy-start.6 = (s32[128,2]{0,1:T(2,128)S(1)}, s32[128,2]{0,1:T(2,128)}, u32[]{:S(2)}) copy-start(s32[128,2]{0,1:T(2,128)} %param.35) | copy-start | bytes 3076
  0.0 34.3 %copy-start.7 = (f32[128,2]{0,1:T(2,128)S(1)}, f32[128,2]{0,1:T(2,128)}, u32[]{:S(2)}) copy-start(f32[128,2]{0,1:T(2,128)} %param.36) | copy-start | bytes 3076
  0.0 39.2 %copy-start.1 = (bf16[32,2048]{1,0:T(8,128)(2,1)S(1)}, bf16[32,2048]{1,0:T(8,128)(2,1)}, u32[]{:S(2)}) copy-start(bf16[32,2048]{1,0:T(8,128)(2,1)} %residual.1) | copy-start | bytes 393220
  0.0 39.2 %copy-start.3 = (f32[2048]{0:T(1024)S(1)}, f32[2048]{0:T(1024)}, u32[]{:S(2)}) copy-start(f32[2048]{0:T(1024)} %param.32) | copy-start | bytes 24580
  0.0 39.2 %copy-start.4 = (f32[2048]{0:T(1024)S(1)}, f32[2048]{0:T(1024)}, u32[]{:S(2)}) copy-start(f32[2048]{0:T(1024)} %param.33) | copy-start | bytes 24580
  29.2 6.1 %collective-permute-start = (bf16[32,2048]{1,0:T(8,128)(2,1)S(1)}, bf16[32,2048]{1,0:T(8,128)(2,1)S(1)}, u32[]{:S(2)}, u32[]{:S(2)}) collective-permute-start(bf16[32,2048]{1,0:T(8,128)(2,1)S(1)} %get-tuple-element.39), channel_id=1, source_target_pairs={{0,1},{1,2},{2,3},{3,0},{4,5},{5,6},{6,7},{7,4},{8,9},{9,10},{10,1... | collective-permute-start | bytes 393224 | tf_op jit(solution)/shard_map/ppermute | solution.py:376
  30.6 8.6 %collective-permute-start.1 = (bf16[32,2048]{1,0:T(8,128)(2,1)S(1)}, bf16[32,2048]{1,0:T(8,128)(2,1)S(1)}, u32[]{:S(2)}, u32[]{:S(2)}) collective-permute-start(bf16[32,2048]{1,0:T(8,128)(2,1)S(1)} %get-tuple-element.40), channel_id=1, source_target_pairs={{0,2},{1,3},{2,0},{3,1},{4,6},{5,7},{6,4},{7,5},{8,10},{9,11},{10,... | collective-permute-start | bytes 393224 | tf_op jit(solution)/shard_map/ppermute | solution.py:376
  33.2 6.0 %collective-permute-start.2 = (bf16[32,2048]{1,0:T(8,128)(2,1)S(1)}, bf16[32,2048]{1,0:T(8,128)(2,1)S(1)}, u32[]{:S(2)}, u32[]{:S(2)}) collective-permute-start(bf16[32,2048]{1,0:T(8,128)(2,1)S(1)} %get-tuple-element.41), channel_id=1, source_target_pairs={{0,3},{1,0},{2,1},{3,2},{4,7},{5,4},{6,5},{7,6},{8,11},{9,8},{10,9... | collective-permute-start | bytes 393224 | tf_op jit(solution)/shard_map/ppermute | solution.py:376
  62.2 7.5 %collective-permute-start.7 = (bf16[256,512]{1,0:T(8,128)(2,1)S(1)}, bf16[256,512]{1,0:T(8,128)(2,1)S(1)}, u32[]{:S(2)}, u32[]{:S(2)}) collective-permute-start(bf16[256,512]{1,0:T(8,128)(2,1)S(1)} %get-tuple-element.57.last), channel_id=1, source_target_pairs={{0,3},{1,0},{2,1},{3,2},{4,7},{5,4},{6,5},{7,6},{8,11},{9,8},{10,9... | collective-permute-start | bytes 786440 | tf_op jit(solution)/shard_map/ppermute | solution.py:376
  64.2 8.7 %collective-permute-start.5 = (bf16[256,512]{1,0:T(8,128)(2,1)S(1)}, bf16[256,512]{1,0:T(8,128)(2,1)S(1)}, u32[]{:S(2)}, u32[]{:S(2)}) collective-permute-start(bf16[256,512]{1,0:T(8,128)(2,1)S(1)} %get-tuple-element.58.first), channel_id=1, source_target_pairs={{0,1},{1,2},{2,3},{3,0},{4,5},{5,6},{6,7},{7,4},{8,9},{9,10},{10,1... | collective-permute-start | bytes 786440 | tf_op jit(solution)/shard_map/ppermute | solution.py:376
  69.8 11.3 %collective-permute-start.8 = (bf16[256,512]{1,0:T(8,128)(2,1)S(1)}, bf16[256,512]{1,0:T(8,128)(2,1)S(1)}, u32[]{:S(2)}, u32[]{:S(2)}) collective-permute-start(bf16[256,512]{1,0:T(8,128)(2,1)S(1)} %collective-permute-done.7.refs_1_), channel_id=1, source_target_pairs={{0,3},{1,0},{2,1},{3,2},{4,7},{5,4},{6,5},{7,6},{8,11},{9,8},{10,9... | collective-permute-start | bytes 786440 | tf_op jit(solution)/shard_map/ppermute | solution.py:376
  72.9 8.2 %collective-permute-start.6 = (bf16[256,512]{1,0:T(8,128)(2,1)S(1)}, bf16[256,512]{1,0:T(8,128)(2,1)S(1)}, u32[]{:S(2)}, u32[]{:S(2)}) collective-permute-start(bf16[256,512]{1,0:T(8,128)(2,1)S(1)} %collective-permute-done.5.refs_0_), channel_id=1, source_target_pairs={{0,1},{1,2},{2,3},{3,0},{4,5},{5,6},{6,7},{7,4},{8,9},{9,10},{10,1... | collective-permute-start | bytes 786440 | tf_op jit(solution)/shard_map/ppermute | solution.py:376
  72.9 15.8 %collective-permute-start.3 = (bf16[256,512]{1,0:T(8,128)(2,1)S(1)}, bf16[256,512]{1,0:T(8,128)(2,1)S(1)}, u32[]{:S(2)}, u32[]{:S(2)}) collective-permute-start(bf16[256,512]{1,0:T(8,128)(2,1)S(1)} %get-tuple-element.57.last), channel_id=1, source_target_pairs={{0,1},{1,2},{2,3},{3,0},{4,5},{5,6},{6,7},{7,4},{8,9},{9,10},{10,1... | collective-permute-start | bytes 786440 | tf_op jit(solution)/shard_map/ppermute | solution.py:376
  72.9 18.5 %collective-permute-start.4 = (bf16[256,512]{1,0:T(8,128)(2,1)S(1)}, bf16[256,512]{1,0:T(8,128)(2,1)S(1)}, u32[]{:S(2)}, u32[]{:S(2)}) collective-permute-start(bf16[256,512]{1,0:T(8,128)(2,1)S(1)} %get-tuple-element.58.first), channel_id=1, source_target_pairs={{0,3},{1,0},{2,1},{3,2},{4,7},{5,4},{6,5},{7,6},{8,11},{9,8},{10,9... | collective-permute-start | bytes 786440 | tf_op jit(solution)/shard_map/ppermute | solution.py:376
  83.5 10.4 %collective-permute-start.9 = (bf16[256,512]{1,0:T(8,128)(2,1)S(1)}, bf16[256,512]{1,0:T(8,128)(2,1)S(1)}, u32[]{:S(2)}, u32[]{:S(2)}) collective-permute-start(bf16[256,512]{1,0:T(8,128)(2,1)S(1)} %get-tuple-element.49), channel_id=1, source_target_pairs={{0,1},{1,2},{2,3},{3,0},{4,5},{5,6},{6,7},{7,4},{8,9},{9,10},{10,1... | collective-permute-start | bytes 786440 | tf_op jit(solution)/shard_map/ppermute | solution.py:376
  86.0 13.6 %collective-permute-start.11 = (bf16[256,512]{1,0:T(8,128)(2,1)S(1)}, bf16[256,512]{1,0:T(8,128)(2,1)S(1)}, u32[]{:S(2)}, u32[]{:S(2)}) collective-permute-start(bf16[256,512]{1,0:T(8,128)(2,1)S(1)} %get-tuple-element.50), channel_id=1, source_target_pairs={{0,3},{1,0},{2,1},{3,2},{4,7},{5,4},{6,5},{7,6},{8,11},{9,8},{10,9... | collective-permute-start | bytes 786440 | tf_op jit(solution)/shard_map/ppermute | solution.py:376
  88.7 10.8 %collective-permute-start.12 = (bf16[256,512]{1,0:T(8,128)(2,1)S(1)}, bf16[256,512]{1,0:T(8,128)(2,1)S(1)}, u32[]{:S(2)}, u32[]{:S(2)}) collective-permute-start(bf16[256,512]{1,0:T(8,128)(2,1)S(1)} %get-tuple-element.52), channel_id=1, source_target_pairs={{0,1},{1,2},{2,3},{3,0},{4,5},{5,6},{6,7},{7,4},{8,9},{9,10},{10,1... | collective-permute-start | bytes 786440 | tf_op jit(solution)/shard_map/ppermute | solution.py:376
  88.7 7.3 %collective-permute-start.13 = (bf16[256,512]{1,0:T(8,128)(2,1)S(1)}, bf16[256,512]{1,0:T(8,128)(2,1)S(1)}, u32[]{:S(2)}, u32[]{:S(2)}) collective-permute-start(bf16[256,512]{1,0:T(8,128)(2,1)S(1)} %get-tuple-element.54), channel_id=1, source_target_pairs={{0,3},{1,0},{2,1},{3,2},{4,7},{5,4},{6,5},{7,6},{8,11},{9,8},{10,9... | collective-permute-start | bytes 786440 | tf_op jit(solution)/shard_map/ppermute | solution.py:376
  93.8 37.8 %copy-start.5 = (f32[2048]{0:T(1024)S(1)}, f32[2048]{0:T(1024)}, u32[]{:S(2)}) copy-start(f32[2048]{0:T(1024)} %param.34) | copy-start | bytes 24580
  93.9 8.8 %collective-permute-start.10 = (bf16[256,512]{1,0:T(8,128)(2,1)S(1)}, bf16[256,512]{1,0:T(8,128)(2,1)S(1)}, u32[]{:S(2)}, u32[]{:S(2)}) collective-permute-start(bf16[256,512]{1,0:T(8,128)(2,1)S(1)} %add_convert_fusion.1), channel_id=1, source_target_pairs={{0,1},{1,2},{2,3},{3,0},{4,5},{5,6},{6,7},{7,4},{8,9},{9,10},{10,1... | collective-permute-start | bytes 786440 | tf_op jit(solution)/shard_map/ppermute | solution.py:376
  96.1 7.2 %collective-permute-start.14 = (bf16[256,512]{1,0:T(8,128)(2,1)S(1)}, bf16[256,512]{1,0:T(8,128)(2,1)S(1)}, u32[]{:S(2)}, u32[]{:S(2)}) collective-permute-start(bf16[256,512]{1,0:T(8,128)(2,1)S(1)} %add_convert_fusion), channel_id=1, source_target_pairs={{0,3},{1,0},{2,1},{3,2},{4,7},{5,4},{6,5},{7,6},{8,11},{9,8},{10,9... | collective-permute-start | bytes 786440 | tf_op jit(solution)/shard_map/ppermute | solution.py:376

commit v8 on v7

--- a/solution.py
+++ b/solution.py
@@ -255,8 +255,7 @@
     outgoing[...] = dot(place[...], stacked).astype(BF16)
 
 
-def expert_kernel(halves, weights, results, arrived=None):
-    gate, up, down = weights
+def hidden_rows(halves, gate, up, arrived=None):
     count = len(halves) // 2
     lines, cut = (2 * halves[0].shape[0], halves[0].shape[1])
     slots = lines // 4
@@ -281,46 +280,66 @@
             gate_hidden = gate_hidden + dot(part, gate[0, span, :])
             arrived(1, q)
             up_hidden = up_hidden + dot(part, up[0, span, :])
-    active = (jax.nn.silu(gate_hidden) * up_hidden).astype(BF16)
+    return (jax.nn.silu(gate_hidden) * up_hidden).astype(BF16)
+
+
+def down_rows(active, down, results, arrived=None):
+    lines, cut = (2 * results[0].shape[0], results[0].shape[1])
+    slots = lines // 4
+    square = (lines, lines)
     made = []
     for q in range(4):
         if arrived is not None:
-            arrived(2, q)
+            arrived(q)
         made.append(dot(active, down[0, :, q * cut : (q + 1) * cut]).astype(BF16))
     in_lines = ones_where(
         iota(square, 1) == (iota(square, 0) % 4) * slots + iota(square, 0) // 4, BF16
     )
-    for k in range(count):
+    for k in range(len(results) // 2):
         stacked = jnp.concatenate([m[k * slots : (k + 1) * slots] for m in made], axis=0)
         product = dot(in_lines, stacked).astype(BF16)
         results[2 * k][...] = product[: lines // 2]
         results[2 * k + 1][...] = product[lines // 2 :]
 
 
-def own_rows_kernel(first, last, gate, up, down, made_first, made_last, *held):
-    *weights, semaphores = held
+def own_rows_kernel(first, last, gate, up, active, gate_held, up_held, semaphores):
     cut = first.shape[1]
 
     def fetch(which, q):
-        source = (gate, up, down)[which]
-        span = pl.ds(q * cut, cut)
-        place = (0, slice(None), span) if which == 2 else (0, span, slice(None))
+        source, held = ((gate, gate_held), (up, up_held))[which]
+        place = (0, pl.ds(q * cut, cut), slice(None))
         return pltpu.make_async_copy(
-            source.at[place], weights[which].at[place], semaphores.at[which * 4 + q]
+            source.at[place], held.at[place], semaphores.at[which * 4 + q]
         )
 
     for q in range(4):
         fetch(0, q).start()
         fetch(1, q).start()
+    active[...] = hidden_rows(
+        (first, last), gate_held, up_held, lambda which, q: fetch(which, q).wait()
+    )
+
+
+def near_rows_kernel(
+    first, last, own_active, gate, up, down, made_first, made_last, own_first, own_last, down_held,
+    semaphores,
+):
+    cut = first.shape[1]
+
+    def fetch(q):
+        place = (0, slice(None), pl.ds(q * cut, cut))
+        return pltpu.make_async_copy(down.at[place], down_held.at[place], semaphores.at[q])
+
     for q in range(4):
-        fetch(2, q).start()
-    expert_kernel(
-        (first, last), weights, (made_first, made_last), lambda which, q: fetch(which, q).wait()
-    )
-
-
-def other_rows_kernel(count, *refs):
-    expert_kernel(refs[:count], refs[count : count + 3], refs[count + 3 : 2 * count + 3])
+        fetch(q).start()
+    active = jnp.concatenate([hidden_rows((first, last), gate, up), own_active[...]], axis=0)
+    down_rows(
+        active, down_held, (made_first, made_last, own_first, own_last), lambda q: fetch(q).wait()
+    )
+
+
+def other_rows_kernel(first, last, gate, up, down, made_first, made_last):
+    down_rows(hidden_rows((first, last), gate, up), down, (made_first, made_last))
 
 
 def total_kernel(*refs):
@@ -388,25 +407,38 @@
     left_first, right_last = (shifted(first, 1), shifted(last, -1))
     left_last, right_first = (shifted(last, 1), shifted(first, -1))
     across_first, across_last = (shifted(left_first, 1), shifted(right_last, -1))
-    own_first, own_last, *held = call(
+    gate, up, down = weights
+    active, gate_held, up_held = call(
         own_rows_kernel,
-        [(half, BF16), (half, BF16), *(pltpu.VMEM(w.shape, w.dtype) for w in weights)],
+        [((lines // 4, gate.shape[2]), BF16), (gate.shape, BF16), (up.shape, BF16)],
         first,
         last,
-        *(in_hbm(w) for w in weights),
-        flops=work,
-        in_place=(2, 3, 4),
-        scratch=[pltpu.SemaphoreType.DMA((12,))],
+        in_hbm(gate),
+        in_hbm(up),
+        flops=work * 2 // 3,
+        in_place=(2, 3),
+        scratch=[pltpu.SemaphoreType.DMA((8,))],
+    )
+    to_left_first, to_right_last, own_first, own_last, down_held = call(
+        near_rows_kernel,
+        [*((half, BF16),) * 4, (down.shape, BF16)],
+        left_first,
+        right_last,
+        active,
+        gate_held,
+        up_held,
+        in_hbm(down),
+        flops=work * 4 // 3,
+        in_place=(5,),
+        scratch=[pltpu.SemaphoreType.DMA((4,))],
     )
 
     def part(*halves):
-        count = len(halves)
         return call(
-            lambda *refs: other_rows_kernel(count, *refs), [(half, BF16)] * count,
-            *halves, *held, flops=work * count // 2,
+            other_rows_kernel, [(half, BF16)] * 2,
+            *halves, gate_held, up_held, down_held, flops=work,
         )
 
-    to_left_first, to_right_last = part(left_first, right_last)
     from_left_last, from_right_first = (shifted(to_right_last, 1), shifted(to_left_first, -1))
     to_left_last, to_right_first = part(left_last, right_first)
     far_first, far_last = part(across_first, across_last)

time: 133 us -> 135 us (1.015)
  waiting for transfers between devices: 15.7 us -> 19.9 us
  blocking collectives: 75 us -> 73.1 us
    ppermute x15, waiting for transfers between devices: 15.7 us -> 19.9 us  [shifted(): return lax.ppermute(part, 'tp', [(i, (i + by) % size) for i in range(size)])]
    all_to_all x3, blocking collectives: 75 us -> 73.1 us  [across_sp(): return lax.all_to_all(pieces, 'sp', split_axis=0, concat_axis=0, tiled=True)]
  transfers between devices with their start and end apart: 15 -> 15, of which waited for: 6 -> 8; matrix products, arithmetic and copies ran while one was open for 0% -> 0% of each run, Pallas kernels for 10% -> 10%
where the time goes in v8:
time: 135 us; the launch traced here: 134 us
  blocking collectives  73.1 us (54%)
  starting transfers between devices  20.7 us (15%)
  Pallas kernels  20.2 us (15%)
  waiting for transfers between devices  19.9 us (15%)
    all_to_all x3, blocking collectives, across_sp(): return lax.all_to_all(pieces, 'sp', split_axis=0, concat_axis=0, tiled=True)  73.1 us
    ppermute x15, starting transfers between devices, shifted(): return lax.ppermute(part, 'tp', [(i, (i + by) % size) for i in range(size)])  20.7 us
    pallas_call x10, Pallas kernels, call(): pl.pallas_call(kernel, out_shape=shapes, in_specs=[left if k in in_place...  20.2 us
    ppermute x15, waiting for transfers between devices, shifted(): return lax.ppermute(part, 'tp', [(i, (i + by) % size) for i in range(size)])  19.9 us
  transfers between devices with their start and end apart: 15, of which 8 were waited for; matrix products, arithmetic and copies ran while one was open for 0% of the time, Pallas kernels for 10%

profile of v8, /device:TPU:1, one launch (start us, length us, event | category | flops | bytes accessed | tf_op | source)
XLA Modules:
  0.0 134.4 jit_solution(13822382347020202362)
XLA Ops:
  0.1 3.3 %shard_map.190 = (bf16[64,2,640]{2,1,0:T(2,128)(2,1)S(1)}, f32[8,512]{1,0:T(8,128)S(1)}, bf16[1024,256]{1,0:T(8,128)(2,1)S(1)}, f32[128,512]{1,0:T(8,128)S(1)}, ...) custom-call(f32[8,128]{1,0:T(8,128)} %bitcast.28, bf16[128,128]{1,0:T(8,128)(2,1)} %inputs.3, ...), custom_call_target="tpu_custom_call" | custom-call | flops 1000000000 | tf_op jit(solution)/shard_map/pallas_call | solution.py:370
  3.4 24.4 %all_to_all.15.got = bf16[64,2,640]{2,1,0:T(2,128)(2,1)S(1)} all-to-all(bf16[64,2,640]{2,1,0:T(2,128)(2,1)S(1)} %get-tuple-element.32), channel_id=1, replica_groups=mesh['sp'=64,'tp'=4] {'sp'}, dimensions={0} | all-to-all | bytes 327680 | tf_op jit(solution)/shard_map/all_to_all | solution.py:390
  27.8 0.0 copy-done.2
  27.8 1.4 %shard_map.191 = (f32[32,2048]{1,0:T(8,128)S(1)}, bf16[32,2048]{1,0:T(8,128)(2,1)S(1)}, bf16[32,2048]{1,0:T(8,128)(2,1)S(1)}, bf16[32,2048]{1,0:T(8,128)(2,1)S(1)}) custom-call(bf16[64,2,640]{2,1,0:T(2,128)(2,1)S(1)} %all_to_all.15.got, f32[8,512]{1,0:T(8,128)S(1)} %get-tuple-element.33.rates, bf16[1024,256]{1,0:T(8,128)(2,1)S(1)} %get-tuple-element.34.read, ...), custom_call_target="tpu_custom_call" | custom-call | flops 1000000000 | tf_op jit(solution)/shard_map/pallas_call | solution.py:370
  29.3 1.4 %collective-permute-start = (bf16[32,2048]{1,0:T(8,128)(2,1)S(1)}, bf16[32,2048]{1,0:T(8,128)(2,1)S(1)}, u32[]{:S(2)}, u32[]{:S(2)}) collective-permute-start(bf16[32,2048]{1,0:T(8,128)(2,1)S(1)} %get-tuple-element.40), channel_id=1, source_target_pairs={{0,1},{1,2},{2,3},{3,0},{4,5},{5,6},{6,7},{7,4},{8,9},{9,10},{10,1... | collective-permute-start | bytes 393224 | tf_op jit(solution)/shard_map/ppermute | solution.py:395
  30.6 2.6 %collective-permute-start.1 = (bf16[32,2048]{1,0:T(8,128)(2,1)S(1)}, bf16[32,2048]{1,0:T(8,128)(2,1)S(1)}, u32[]{:S(2)}, u32[]{:S(2)}) collective-permute-start(bf16[32,2048]{1,0:T(8,128)(2,1)S(1)} %get-tuple-element.41), channel_id=1, source_target_pairs={{0,2},{1,3},{2,0},{3,1},{4,6},{5,7},{6,4},{7,5},{8,10},{9,11},{10,... | collective-permute-start | bytes 393224 | tf_op jit(solution)/shard_map/ppermute | solution.py:395
  33.2 1.1 collective-permute-start.2
  34.3 0.0 copy-done.6
  34.3 0.5 shard_map.192
  34.9 0.5 collective-permute-done.got_1
  35.3 3.9 %collective-permute-done.1.got_2 = bf16[32,2048]{1,0:T(8,128)(2,1)S(1)} collective-permute-done((bf16[32,2048]{1,0:T(8,128)(2,1)S(1)}, bf16[32,2048]{1,0:T(8,128)(2,1)S(1)}, u32[]{:S(2)}, u32[]{:S(2)}) %collective-permute-start.1) | collective-permute-done | bytes 131104 | tf_op jit(solution)/shard_map/ppermute | solution.py:395
  39.3 0.0 collective-permute-done.2.got_3
  39.3 0.6 shard_map.193
  39.8 22.4 %all_to_all.16 = bf16[64,8,512]{2,1,0:T(8,128)(2,1)S(1)} all-to-all(bf16[64,8,512]{2,1,0:T(8,128)(2,1)S(1)} %bitcast.18), channel_id=1, replica_groups=mesh['sp'=64,'tp'=4] {'sp'}, dimensions={0} | all-to-all | bytes 1048576 | tf_op jit(solution)/shard_map/all_to_all | solution.py:390
  62.3 1.0 collective-permute-start.3
  63.3 1.7 %collective-permute-start.4 = (bf16[256,512]{1,0:T(8,128)(2,1)S(1)}, bf16[256,512]{1,0:T(8,128)(2,1)S(1)}, u32[]{:S(2)}, u32[]{:S(2)}) collective-permute-start(bf16[256,512]{1,0:T(8,128)(2,1)S(1)} %get-tuple-element.59.last), channel_id=1, source_target_pairs={{0,3},{1,0},{2,1},{3,2},{4,7},{5,4},{6,5},{7,6},{8,11},{9,8},{10,9... | collective-permute-start | bytes 786440 | tf_op jit(solution)/shard_map/ppermute | solution.py:395
  65.0 0.0 collective-permute-start.5
  65.0 2.7 %collective-permute-start.6 = (bf16[256,512]{1,0:T(8,128)(2,1)S(1)}, bf16[256,512]{1,0:T(8,128)(2,1)S(1)}, u32[]{:S(2)}, u32[]{:S(2)}) collective-permute-start(bf16[256,512]{1,0:T(8,128)(2,1)S(1)} %get-tuple-element.60.first), channel_id=1, source_target_pairs={{0,3},{1,0},{2,1},{3,2},{4,7},{5,4},{6,5},{7,6},{8,11},{9,8},{10,9... | collective-permute-start | bytes 786440 | tf_op jit(solution)/shard_map/ppermute | solution.py:395
  67.7 3.3 %collective-permute-done.3.first = bf16[256,512]{1,0:T(8,128)(2,1)S(1)} collective-permute-done((bf16[256,512]{1,0:T(8,128)(2,1)S(1)}, bf16[256,512]{1,0:T(8,128)(2,1)S(1)}, u32[]{:S(2)}, u32[]{:S(2)}) %collective-permute-start.3) | collective-permute-done | bytes 262176 | tf_op jit(solution)/shard_map/ppermute | solution.py:395
  71.0 0.0 collective-permute-start.7
  71.0 0.0 collective-permute-done.4.last
  71.0 2.7 %collective-permute-start.8 = (bf16[256,512]{1,0:T(8,128)(2,1)S(1)}, bf16[256,512]{1,0:T(8,128)(2,1)S(1)}, u32[]{:S(2)}, u32[]{:S(2)}) collective-permute-start(bf16[256,512]{1,0:T(8,128)(2,1)S(1)} %collective-permute-done.4.last), channel_id=1, source_target_pairs={{0,3},{1,0},{2,1},{3,2},{4,7},{5,4},{6,5},{7,6},{8,11},{9,8},{10,9... | collective-permute-start | bytes 786440 | tf_op jit(solution)/shard_map/ppermute | solution.py:395
  73.7 3.9 %shard_map.194 = (bf16[128,896]{1,0:T(8,128)(2,1)S(1)}, bf16[1,2048,896]{2,1,0:T(8,128)(2,1)S(1)}, bf16[1,2048,896]{2,1,0:T(8,128)(2,1)S(1)}) custom-call(bf16[256,512]{1,0:T(8,128)(2,1)S(1)} %get-tuple-element.60.first, bf16[256,512]{1,0:T(8,128)(2,1)S(1)} %get-tuple-element.59.last, bf16[1,2048,896]{2,1,0:T(8,128)(2,1)} %gate.1, bf16[1,2048,896]{2,1,0:T(8,128)(2,1)} %up.1), custom_call_target="tpu_custom_call" | custom-call | flops 939524096 | tf_op jit(solution)/shard_map/pallas_call | solution.py:370
  77.6 4.4 %shard_map.195 = (bf16[256,512]{1,0:T(8,128)(2,1)S(1)}, bf16[256,512]{1,0:T(8,128)(2,1)S(1)}, bf16[256,512]{1,0:T(8,128)(2,1)S(1)}, bf16[256,512]{1,0:T(8,128)(2,1)S(1)}, bf16[1,896,2048]{2,1,0:T(8,128)(2,1)S(1)}) custom-call(bf16[256,512]{1,0:T(8,128)(2,1)S(1)} %collective-permute-done.3.first, bf16[256,512]{1,0:T(8,128)(2,1)S(1)} %collective-permute-done.4.last, ...), custom_call_target="tpu_custom_call" | custom-call | flops 1879048192 | tf_op jit(solution)/shard_map/pallas_call | solution.py:370
  82.0 0.3 collective-permute-done.7.first
  82.3 0.0 collective-permute-done.8.last
  82.3 2.4 %shard_map.197 = (bf16[256,512]{1,0:T(8,128)(2,1)S(1)}, bf16[256,512]{1,0:T(8,128)(2,1)S(1)}) custom-call(bf16[256,512]{1,0:T(8,128)(2,1)S(1)} %collective-permute-done.7.first, bf16[256,512]{1,0:T(8,128)(2,1)S(1)} %collective-permute-done.8.last, bf16[1,2048,896]{2,1,0:T(8,128)(2,1)S(1)} %get-tuple-element.46.gate, ...), custom_call_target="tpu_custom_call" | custom-call | flops 1409286144 | tf_op jit(solution)/shard_map/pallas_call | solution.py:370
  84.7 2.5 %collective-permute-start.13 = (bf16[256,512]{1,0:T(8,128)(2,1)S(1)}, bf16[256,512]{1,0:T(8,128)(2,1)S(1)}, u32[]{:S(2)}, u32[]{:S(2)}) collective-permute-start(bf16[256,512]{1,0:T(8,128)(2,1)S(1)} %get-tuple-element.56), channel_id=1, source_target_pairs={{0,3},{1,0},{2,1},{3,2},{4,7},{5,4},{6,5},{7,6},{8,11},{9,8},{10,9... | collective-permute-start | bytes 786440 | tf_op jit(solution)/shard_map/ppermute | solution.py:395
  87.1 0.1 collective-permute-start.11
  87.2 1.4 %collective-permute-start.12 = (bf16[256,512]{1,0:T(8,128)(2,1)S(1)}, bf16[256,512]{1,0:T(8,128)(2,1)S(1)}, u32[]{:S(2)}, u32[]{:S(2)}) collective-permute-start(bf16[256,512]{1,0:T(8,128)(2,1)S(1)} %get-tuple-element.54), channel_id=1, source_target_pairs={{0,1},{1,2},{2,3},{3,0},{4,5},{5,6},{6,7},{7,4},{8,9},{9,10},{10,1... | collective-permute-start | bytes 786440 | tf_op jit(solution)/shard_map/ppermute | solution.py:395
  88.6 0.0 collective-permute-done.5.first
  88.6 0.0 collective-permute-start.9
  88.6 0.0 collective-permute-done.6.last
  88.6 2.4 %shard_map.196 = (bf16[256,512]{1,0:T(8,128)(2,1)S(1)}, bf16[256,512]{1,0:T(8,128)(2,1)S(1)}) custom-call(bf16[256,512]{1,0:T(8,128)(2,1)S(1)} %collective-permute-done.5.first, bf16[256,512]{1,0:T(8,128)(2,1)S(1)} %collective-permute-done.6.last, bf16[1,2048,896]{2,1,0:T(8,128)(2,1)S(1)} %get-tuple-element.46.gate, ...), custom_call_target="tpu_custom_call" | custom-call | flops 1409286144 | tf_op jit(solution)/shard_map/pallas_call | solution.py:370
  91.0 0.0 copy-start.5
  91.1 0.2 collective-permute-done.13
  91.3 0.1 add_convert_fusion
  91.4 3.5 %collective-permute-start.14 = (bf16[256,512]{1,0:T(8,128)(2,1)S(1)}, bf16[256,512]{1,0:T(8,128)(2,1)S(1)}, u32[]{:S(2)}, u32[]{:S(2)}) collective-permute-start(bf16[256,512]{1,0:T(8,128)(2,1)S(1)} %add_convert_fusion), channel_id=1, source_target_pairs={{0,3},{1,0},{2,1},{3,2},{4,7},{5,4},{6,5},{7,6},{8,11},{9,8},{10,9... | collective-permute-start | bytes 786440 | tf_op jit(solution)/shard_map/ppermute | solution.py:395
  94.8 5.3 %collective-permute-done.9 = bf16[256,512]{1,0:T(8,128)(2,1)S(1)} collective-permute-done((bf16[256,512]{1,0:T(8,128)(2,1)S(1)}, bf16[256,512]{1,0:T(8,128)(2,1)S(1)}, u32[]{:S(2)}, u32[]{:S(2)}) %collective-permute-start.9) | collective-permute-done | bytes 262176 | tf_op jit(solution)/shard_map/ppermute | solution.py:395
  100.1 0.1 add_convert_fusion.1
  100.2 0.1 collective-permute-start.10
  100.3 0.0 collective-permute-done.11.refs_2_
  100.3 0.0 collective-permute-done.12.refs_4_
  100.3 2.2 %collective-permute-done.14.refs_5_ = bf16[256,512]{1,0:T(8,128)(2,1)S(1)} collective-permute-done((bf16[256,512]{1,0:T(8,128)(2,1)S(1)}, bf16[256,512]{1,0:T(8,128)(2,1)S(1)}, u32[]{:S(2)}, u32[]{:S(2)}) %collective-permute-start.14) | collective-permute-done | bytes 262176 | tf_op jit(solution)/shard_map/ppermute | solution.py:395
  102.5 4.2 %collective-permute-done.10.refs_1_ = bf16[256,512]{1,0:T(8,128)(2,1)S(1)} collective-permute-done((bf16[256,512]{1,0:T(8,128)(2,1)S(1)}, bf16[256,512]{1,0:T(8,128)(2,1)S(1)}, u32[]{:S(2)}, u32[]{:S(2)}) %collective-permute-start.10) | collective-permute-done | bytes 262176 | tf_op jit(solution)/shard_map/ppermute | solution.py:395
  106.7 0.2 shard_map.198
  106.9 26.3 %all_to_all.17 = bf16[64,8,512]{2,1,0:T(8,128)(2,1)S(1)} all-to-all(bf16[64,8,512]{2,1,0:T(8,128)(2,1)S(1)} %bitcast.17), channel_id=1, replica_groups=mesh['sp'=64,'tp'=4] {'sp'}, dimensions={0} | all-to-all | bytes 1048576 | tf_op jit(solution)/shard_map/all_to_all | solution.py:390
  133.2 1.2 shard_map.199
  (16 shorter events, 0.1 us)
Async XLA Ops:
  0.0 27.8 %copy-start.2 = (bf16[128,128]{1,0:T(8,128)(2,1)S(1)}, bf16[128,128]{1,0:T(8,128)(2,1)}, u32[]{:S(2)}) copy-start(bf16[128,128]{1,0:T(8,128)(2,1)} %inputs.3) | copy-start | bytes 98308
  0.0 27.8 %copy-start.8 = (f32[128]{0:T(128)S(1)}, f32[128]{0:T(128)}, u32[]{:S(2)}) copy-start(f32[128]{0:T(128)} %param.29) | copy-start | bytes 1540
  0.0 27.8 %copy-start = (bf16[128,2048]{1,0:T(8,128)(2,1)S(1)}, bf16[128,2048]{1,0:T(8,128)(2,1)}, u32[]{:S(2)}) copy-start(bf16[128,2048]{1,0:T(8,128)(2,1)} %out_weight.1) | copy-start | bytes 1572868
  0.0 34.3 %copy-start.6 = (s32[128,2]{0,1:T(2,128)S(1)}, s32[128,2]{0,1:T(2,128)}, u32[]{:S(2)}) copy-start(s32[128,2]{0,1:T(2,128)} %param.35) | copy-start | bytes 3076
  0.0 34.3 %copy-start.7 = (f32[128,2]{0,1:T(2,128)S(1)}, f32[128,2]{0,1:T(2,128)}, u32[]{:S(2)}) copy-start(f32[128,2]{0,1:T(2,128)} %param.36) | copy-start | bytes 3076
  0.0 39.2 %copy-start.1 = (bf16[32,2048]{1,0:T(8,128)(2,1)S(1)}, bf16[32,2048]{1,0:T(8,128)(2,1)}, u32[]{:S(2)}) copy-start(bf16[32,2048]{1,0:T(8,128)(2,1)} %residual.1) | copy-start | bytes 393220
  0.0 39.2 %copy-start.3 = (f32[2048]{0:T(1024)S(1)}, f32[2048]{0:T(1024)}, u32[]{:S(2)}) copy-start(f32[2048]{0:T(1024)} %param.32) | copy-start | bytes 24580
  0.0 39.2 %copy-start.4 = (f32[2048]{0:T(1024)S(1)}, f32[2048]{0:T(1024)}, u32[]{:S(2)}) copy-start(f32[2048]{0:T(1024)} %param.33) | copy-start | bytes 24580
  29.3 6.1 %collective-permute-start = (bf16[32,2048]{1,0:T(8,128)(2,1)S(1)}, bf16[32,2048]{1,0:T(8,128)(2,1)S(1)}, u32[]{:S(2)}, u32[]{:S(2)}) collective-permute-start(bf16[32,2048]{1,0:T(8,128)(2,1)S(1)} %get-tuple-element.40), channel_id=1, source_target_pairs={{0,1},{1,2},{2,3},{3,0},{4,5},{5,6},{6,7},{7,4},{8,9},{9,10},{10,1... | collective-permute-start | bytes 393224 | tf_op jit(solution)/shard_map/ppermute | solution.py:395
  30.6 8.6 %collective-permute-start.1 = (bf16[32,2048]{1,0:T(8,128)(2,1)S(1)}, bf16[32,2048]{1,0:T(8,128)(2,1)S(1)}, u32[]{:S(2)}, u32[]{:S(2)}) collective-permute-start(bf16[32,2048]{1,0:T(8,128)(2,1)S(1)} %get-tuple-element.41), channel_id=1, source_target_pairs={{0,2},{1,3},{2,0},{3,1},{4,6},{5,7},{6,4},{7,5},{8,10},{9,11},{10,... | collective-permute-start | bytes 393224 | tf_op jit(solution)/shard_map/ppermute | solution.py:395
  33.2 6.0 %collective-permute-start.2 = (bf16[32,2048]{1,0:T(8,128)(2,1)S(1)}, bf16[32,2048]{1,0:T(8,128)(2,1)S(1)}, u32[]{:S(2)}, u32[]{:S(2)}) collective-permute-start(bf16[32,2048]{1,0:T(8,128)(2,1)S(1)} %get-tuple-element.42), channel_id=1, source_target_pairs={{0,3},{1,0},{2,1},{3,2},{4,7},{5,4},{6,5},{7,6},{8,11},{9,8},{10,9... | collective-permute-start | bytes 393224 | tf_op jit(solution)/shard_map/ppermute | solution.py:395
  62.3 8.8 %collective-permute-start.3 = (bf16[256,512]{1,0:T(8,128)(2,1)S(1)}, bf16[256,512]{1,0:T(8,128)(2,1)S(1)}, u32[]{:S(2)}, u32[]{:S(2)}) collective-permute-start(bf16[256,512]{1,0:T(8,128)(2,1)S(1)} %get-tuple-element.60.first), channel_id=1, source_target_pairs={{0,1},{1,2},{2,3},{3,0},{4,5},{5,6},{6,7},{7,4},{8,9},{9,10},{10,1... | collective-permute-start | bytes 786440 | tf_op jit(solution)/shard_map/ppermute | solution.py:395
  63.3 7.7 %collective-permute-start.4 = (bf16[256,512]{1,0:T(8,128)(2,1)S(1)}, bf16[256,512]{1,0:T(8,128)(2,1)S(1)}, u32[]{:S(2)}, u32[]{:S(2)}) collective-permute-start(bf16[256,512]{1,0:T(8,128)(2,1)S(1)} %get-tuple-element.59.last), channel_id=1, source_target_pairs={{0,3},{1,0},{2,1},{3,2},{4,7},{5,4},{6,5},{7,6},{8,11},{9,8},{10,9... | collective-permute-start | bytes 786440 | tf_op jit(solution)/shard_map/ppermute | solution.py:395
  65.0 23.6 %collective-permute-start.5 = (bf16[256,512]{1,0:T(8,128)(2,1)S(1)}, bf16[256,512]{1,0:T(8,128)(2,1)S(1)}, u32[]{:S(2)}, u32[]{:S(2)}) collective-permute-start(bf16[256,512]{1,0:T(8,128)(2,1)S(1)} %get-tuple-element.59.last), channel_id=1, source_target_pairs={{0,1},{1,2},{2,3},{3,0},{4,5},{5,6},{6,7},{7,4},{8,9},{9,10},{10,1... | collective-permute-start | bytes 786440 | tf_op jit(solution)/shard_map/ppermute | solution.py:395
  65.0 23.6 %collective-permute-start.6 = (bf16[256,512]{1,0:T(8,128)(2,1)S(1)}, bf16[256,512]{1,0:T(8,128)(2,1)S(1)}, u32[]{:S(2)}, u32[]{:S(2)}) collective-permute-start(bf16[256,512]{1,0:T(8,128)(2,1)S(1)} %get-tuple-element.60.first), channel_id=1, source_target_pairs={{0,3},{1,0},{2,1},{3,2},{4,7},{5,4},{6,5},{7,6},{8,11},{9,8},{10,9... | collective-permute-start | bytes 786440 | tf_op jit(solution)/shard_map/ppermute | solution.py:395
  71.0 11.2 %collective-permute-start.7 = (bf16[256,512]{1,0:T(8,128)(2,1)S(1)}, bf16[256,512]{1,0:T(8,128)(2,1)S(1)}, u32[]{:S(2)}, u32[]{:S(2)}) collective-permute-start(bf16[256,512]{1,0:T(8,128)(2,1)S(1)} %collective-permute-done.3.first), channel_id=1, source_target_pairs={{0,1},{1,2},{2,3},{3,0},{4,5},{5,6},{6,7},{7,4},{8,9},{9,10},{10,1... | collective-permute-start | bytes 786440 | tf_op jit(solution)/shard_map/ppermute | solution.py:395
  71.0 11.2 %collective-permute-start.8 = (bf16[256,512]{1,0:T(8,128)(2,1)S(1)}, bf16[256,512]{1,0:T(8,128)(2,1)S(1)}, u32[]{:S(2)}, u32[]{:S(2)}) collective-permute-start(bf16[256,512]{1,0:T(8,128)(2,1)S(1)} %collective-permute-done.4.last), channel_id=1, source_target_pairs={{0,3},{1,0},{2,1},{3,2},{4,7},{5,4},{6,5},{7,6},{8,11},{9,8},{10,9... | collective-permute-start | bytes 786440 | tf_op jit(solution)/shard_map/ppermute | solution.py:395
  84.7 6.6 %collective-permute-start.13 = (bf16[256,512]{1,0:T(8,128)(2,1)S(1)}, bf16[256,512]{1,0:T(8,128)(2,1)S(1)}, u32[]{:S(2)}, u32[]{:S(2)}) collective-permute-start(bf16[256,512]{1,0:T(8,128)(2,1)S(1)} %get-tuple-element.56), channel_id=1, source_target_pairs={{0,3},{1,0},{2,1},{3,2},{4,7},{5,4},{6,5},{7,6},{8,11},{9,8},{10,9... | collective-permute-start | bytes 786440 | tf_op jit(solution)/shard_map/ppermute | solution.py:395
  87.1 13.1 %collective-permute-start.11 = (bf16[256,512]{1,0:T(8,128)(2,1)S(1)}, bf16[256,512]{1,0:T(8,128)(2,1)S(1)}, u32[]{:S(2)}, u32[]{:S(2)}) collective-permute-start(bf16[256,512]{1,0:T(8,128)(2,1)S(1)} %get-tuple-element.52), channel_id=1, source_target_pairs={{0,3},{1,0},{2,1},{3,2},{4,7},{5,4},{6,5},{7,6},{8,11},{9,8},{10,9... | collective-permute-start | bytes 786440 | tf_op jit(solution)/shard_map/ppermute | solution.py:395
  87.2 13.1 %collective-permute-start.12 = (bf16[256,512]{1,0:T(8,128)(2,1)S(1)}, bf16[256,512]{1,0:T(8,128)(2,1)S(1)}, u32[]{:S(2)}, u32[]{:S(2)}) collective-permute-start(bf16[256,512]{1,0:T(8,128)(2,1)S(1)} %get-tuple-element.54), channel_id=1, source_target_pairs={{0,1},{1,2},{2,3},{3,0},{4,5},{5,6},{6,7},{7,4},{8,9},{9,10},{10,1... | collective-permute-start | bytes 786440 | tf_op jit(solution)/shard_map/ppermute | solution.py:395
  88.6 11.5 %collective-permute-start.9 = (bf16[256,512]{1,0:T(8,128)(2,1)S(1)}, bf16[256,512]{1,0:T(8,128)(2,1)S(1)}, u32[]{:S(2)}, u32[]{:S(2)}) collective-permute-start(bf16[256,512]{1,0:T(8,128)(2,1)S(1)} %get-tuple-element.51), channel_id=1, source_target_pairs={{0,1},{1,2},{2,3},{3,0},{4,5},{5,6},{6,7},{7,4},{8,9},{9,10},{10,1... | collective-permute-start | bytes 786440 | tf_op jit(solution)/shard_map/ppermute | solution.py:395
  91.0 42.2 %copy-start.5 = (f32[2048]{0:T(1024)S(1)}, f32[2048]{0:T(1024)}, u32[]{:S(2)}) copy-start(f32[2048]{0:T(1024)} %param.34) | copy-start | bytes 24580
  91.4 11.2 %collective-permute-start.14 = (bf16[256,512]{1,0:T(8,128)(2,1)S(1)}, bf16[256,512]{1,0:T(8,128)(2,1)S(1)}, u32[]{:S(2)}, u32[]{:S(2)}) collective-permute-start(bf16[256,512]{1,0:T(8,128)(2,1)S(1)} %add_convert_fusion), channel_id=1, source_target_pairs={{0,3},{1,0},{2,1},{3,2},{4,7},{5,4},{6,5},{7,6},{8,11},{9,8},{10,9... | collective-permute-start | bytes 786440 | tf_op jit(solution)/shard_map/ppermute | solution.py:395
  100.2 6.5 %collective-permute-start.10 = (bf16[256,512]{1,0:T(8,128)(2,1)S(1)}, bf16[256,512]{1,0:T(8,128)(2,1)S(1)}, u32[]{:S(2)}, u32[]{:S(2)}) collective-permute-start(bf16[256,512]{1,0:T(8,128)(2,1)S(1)} %add_convert_fusion.1), channel_id=1, source_target_pairs={{0,1},{1,2},{2,3},{3,0},{4,5},{5,6},{6,7},{7,4},{8,9},{9,10},{10,1... | collective-permute-start | bytes 786440 | tf_op jit(solution)/shard_map/ppermute | solution.py:395

commit v9 on v7

--- a/solution.py
+++ b/solution.py
@@ -52,9 +52,6 @@
 
 
 def delayed(values, by, fill):
-    if by >= 8:
-        head = jnp.full((by, values.shape[1]), fill, F32)
-        return jnp.concatenate([head, values[: values.shape[0] - by]], axis=0)
     return jnp.where(iota(values.shape, 0) >= by, pltpu.roll(values, by, 0), fill)
 
 
@@ -132,13 +129,25 @@
         s_imag = coef_real * into_imag[:, cut] + coef_imag * into_real[:, cut]
         by = 1
         while by < length:
-            p_real, p_imag = (delayed(s_real, by, 0.0), delayed(s_imag, by, 0.0))
-            b_real, b_imag = (delayed(a_real, by, 1.0), delayed(a_imag, by, 0.0))
-            s_real, s_imag = (
+            keep = by if by >= 8 else 0
+            whole = (s_real, s_imag, a_real, a_imag)
+            s_real, s_imag, a_real, a_imag = (part[keep:] for part in whole)
+            if keep:
+                p_real, p_imag, b_real, b_imag = (part[: length - by] for part in whole)
+            else:
+                p_real, p_imag = (delayed(s_real, by, 0.0), delayed(s_imag, by, 0.0))
+                b_real, b_imag = (delayed(a_real, by, 1.0), delayed(a_imag, by, 0.0))
+            s_real, s_imag, a_real, a_imag = (
                 s_real + a_real * p_real - a_imag * p_imag,
                 s_imag + a_real * p_imag + a_imag * p_real,
+                a_real * b_real - a_imag * b_imag,
+                a_real * b_imag + a_imag * b_real,
             )
-            a_real, a_imag = (a_real * b_real - a_imag * b_imag, a_real * b_imag + a_imag * b_real)
+            if keep:
+                s_real, s_imag, a_real, a_imag = (
+                    jnp.concatenate([before[:keep], after], axis=0)
+                    for before, after in zip(whole, (s_real, s_imag, a_real, a_imag))
+                )
             by *= 2
         cum_real[:, cut] = a_real
         cum_imag[:, cut] = a_imag
@@ -233,7 +242,7 @@
     weight = (is_first * first + is_second * (1.0 - first)) * kept
     back = (slots, slots * 4)
     repeat = ones_where(iota(back, 1) // 4 == iota(back, 0), BF16)
-    took = dot(jnp.concatenate(split(weight, 3), axis=0), repeat)
+    took = dot(jnp.concatenate(split(weight, 2), axis=0), repeat)
     fits = iota(took.shape, 1) % 4 == (iota(took.shape, 0) % slots) // rows
     weigh[...] = jnp.where(fits, took, 0.0).astype(BF16)
 
@@ -334,8 +343,8 @@
 def combine_kernel(results, weigh, stream, final_gain, out):
     rows = stream.shape[0]
     mixture = dot(weigh[...], results[...])
-    height = mixture.shape[0] // 3
-    mixture = (mixture[:height] + mixture[height : 2 * height]) + mixture[2 * height :]
+    height = mixture.shape[0] // 2
+    mixture = mixture[:height] + mixture[height:]
     mixture = jnp.concatenate([mixture[q * rows : (q + 1) * rows] for q in range(4)], axis=1)
     out[...] = (stream[...].astype(F32) + normalized(mixture, final_gain[...])).astype(BF16)
 
@@ -491,7 +500,7 @@
     )
     place, weigh = call(
         route_kernel,
-        [((4 * slots, slots), BF16), ((3 * slots, 4 * slots), BF16)],
+        [((4 * slots, slots), BF16), ((2 * slots, 4 * slots), BF16)],
         route_ids.T,
         route_logits.T,
         flops=10**8,

time: 133 us -> 133 us (level)
  no operation moved by 1% of the time
where the time goes in v9:
time: 133 us
  blocking collectives  75 us (56%)
  starting transfers between devices  21.9 us (16%)
  Pallas kernels  19.6 us (15%)
  waiting for transfers between devices  15.7 us (12%)
    all_to_all x3, blocking collectives, across_sp(): return lax.all_to_all(pieces, 'sp', split_axis=0, concat_axis=0, tiled=True)  75 us
    ppermute x15, starting transfers between devices, shifted(): return lax.ppermute(part, 'tp', [(i, (i + by) % size) for i in range(size)])  21.9 us
    pallas_call x10, Pallas kernels, call(): pl.pallas_call(kernel, out_shape=shapes, in_specs=[left if k in in_place...  19.6 us
    ppermute x15, waiting for transfers between devices, shifted(): return lax.ppermute(part, 'tp', [(i, (i + by) % size) for i in range(size)])  15.7 us
  transfers between devices with their start and end apart: 15, of which 6 were waited for; matrix products, arithmetic and copies ran while one was open for 0% of the time, Pallas kernels for 10%

profile of v9, /device:TPU:1, one launch (start us, length us, event | category | flops | bytes accessed | tf_op | source)
XLA Modules:
  0.0 132.6 jit_solution(6623496434340846780)
XLA Ops:
  0.1 3.2 %shard_map.190 = (bf16[64,2,640]{2,1,0:T(2,128)(2,1)S(1)}, f32[8,512]{1,0:T(8,128)S(1)}, bf16[1024,256]{1,0:T(8,128)(2,1)S(1)}, f32[128,512]{1,0:T(8,128)S(1)}, ...) custom-call(f32[8,128]{1,0:T(8,128)} %bitcast.28, bf16[128,128]{1,0:T(8,128)(2,1)} %inputs.3, ...), custom_call_target="tpu_custom_call" | custom-call | flops 1000000000 | tf_op jit(solution)/shard_map/pallas_call | solution.py:360
  3.2 24.4 %all_to_all.15.got = bf16[64,2,640]{2,1,0:T(2,128)(2,1)S(1)} all-to-all(bf16[64,2,640]{2,1,0:T(2,128)(2,1)S(1)} %get-tuple-element.31), channel_id=1, replica_groups=mesh['sp'=64,'tp'=4] {'sp'}, dimensions={0} | all-to-all | bytes 327680 | tf_op jit(solution)/shard_map/all_to_all | solution.py:380
  27.7 0.0 copy-done.2
  27.7 1.4 %shard_map.191 = (f32[32,2048]{1,0:T(8,128)S(1)}, bf16[32,2048]{1,0:T(8,128)(2,1)S(1)}, bf16[32,2048]{1,0:T(8,128)(2,1)S(1)}, bf16[32,2048]{1,0:T(8,128)(2,1)S(1)}) custom-call(bf16[64,2,640]{2,1,0:T(2,128)(2,1)S(1)} %all_to_all.15.got, f32[8,512]{1,0:T(8,128)S(1)} %get-tuple-element.32.rates, bf16[1024,256]{1,0:T(8,128)(2,1)S(1)} %get-tuple-element.33.read, ...), custom_call_target="tpu_custom_call" | custom-call | flops 1000000000 | tf_op jit(solution)/shard_map/pallas_call | solution.py:360
  29.1 1.4 %collective-permute-start = (bf16[32,2048]{1,0:T(8,128)(2,1)S(1)}, bf16[32,2048]{1,0:T(8,128)(2,1)S(1)}, u32[]{:S(2)}, u32[]{:S(2)}) collective-permute-start(bf16[32,2048]{1,0:T(8,128)(2,1)S(1)} %get-tuple-element.39), channel_id=1, source_target_pairs={{0,1},{1,2},{2,3},{3,0},{4,5},{5,6},{6,7},{7,4},{8,9},{9,10},{10,1... | collective-permute-start | bytes 393224 | tf_op jit(solution)/shard_map/ppermute | solution.py:385
  30.5 2.6 %collective-permute-start.1 = (bf16[32,2048]{1,0:T(8,128)(2,1)S(1)}, bf16[32,2048]{1,0:T(8,128)(2,1)S(1)}, u32[]{:S(2)}, u32[]{:S(2)}) collective-permute-start(bf16[32,2048]{1,0:T(8,128)(2,1)S(1)} %get-tuple-element.40), channel_id=1, source_target_pairs={{0,2},{1,3},{2,0},{3,1},{4,6},{5,7},{6,4},{7,5},{8,10},{9,11},{10,... | collective-permute-start | bytes 393224 | tf_op jit(solution)/shard_map/ppermute | solution.py:385
  33.1 1.1 collective-permute-start.2
  34.2 0.5 shard_map.192
  34.7 0.5 collective-permute-done.got_1
  35.2 3.9 %collective-permute-done.1.got_2 = bf16[32,2048]{1,0:T(8,128)(2,1)S(1)} collective-permute-done((bf16[32,2048]{1,0:T(8,128)(2,1)S(1)}, bf16[32,2048]{1,0:T(8,128)(2,1)S(1)}, u32[]{:S(2)}, u32[]{:S(2)}) %collective-permute-start.1) | collective-permute-done | bytes 131104 | tf_op jit(solution)/shard_map/ppermute | solution.py:385
  39.1 0.0 collective-permute-done.2.got_3
  39.1 0.0 copy-done.4
  39.1 0.6 shard_map.193
  39.7 22.4 %all_to_all.16 = bf16[64,8,512]{2,1,0:T(8,128)(2,1)S(1)} all-to-all(bf16[64,8,512]{2,1,0:T(8,128)(2,1)S(1)} %bitcast.18), channel_id=1, replica_groups=mesh['sp'=64,'tp'=4] {'sp'}, dimensions={0} | all-to-all | bytes 1048576 | tf_op jit(solution)/shard_map/all_to_all | solution.py:380
  62.1 2.0 %collective-permute-start.7 = (bf16[256,512]{1,0:T(8,128)(2,1)S(1)}, bf16[256,512]{1,0:T(8,128)(2,1)S(1)}, u32[]{:S(2)}, u32[]{:S(2)}) collective-permute-start(bf16[256,512]{1,0:T(8,128)(2,1)S(1)} %get-tuple-element.57.last), channel_id=1, source_target_pairs={{0,3},{1,0},{2,1},{3,2},{4,7},{5,4},{6,5},{7,6},{8,11},{9,8},{10,9... | collective-permute-start | bytes 786440 | tf_op jit(solution)/shard_map/ppermute | solution.py:385
  64.1 0.0 collective-permute-start.5
  64.1 5.6 %collective-permute-done.7.refs_1_ = bf16[256,512]{1,0:T(8,128)(2,1)S(1)} collective-permute-done((bf16[256,512]{1,0:T(8,128)(2,1)S(1)}, bf16[256,512]{1,0:T(8,128)(2,1)S(1)}, u32[]{:S(2)}, u32[]{:S(2)}) %collective-permute-start.7) | collective-permute-done | bytes 262176 | tf_op jit(solution)/shard_map/ppermute | solution.py:385
  69.7 3.1 %collective-permute-start.8 = (bf16[256,512]{1,0:T(8,128)(2,1)S(1)}, bf16[256,512]{1,0:T(8,128)(2,1)S(1)}, u32[]{:S(2)}, u32[]{:S(2)}) collective-permute-start(bf16[256,512]{1,0:T(8,128)(2,1)S(1)} %collective-permute-done.7.refs_1_), channel_id=1, source_target_pairs={{0,3},{1,0},{2,1},{3,2},{4,7},{5,4},{6,5},{7,6},{8,11},{9,8},{10,9... | collective-permute-start | bytes 786440 | tf_op jit(solution)/shard_map/ppermute | solution.py:385
  72.8 0.0 collective-permute-done.5.refs_0_
  72.8 0.0 collective-permute-start.6
  72.8 0.0 collective-permute-start.3
  72.8 2.7 %collective-permute-start.4 = (bf16[256,512]{1,0:T(8,128)(2,1)S(1)}, bf16[256,512]{1,0:T(8,128)(2,1)S(1)}, u32[]{:S(2)}, u32[]{:S(2)}) collective-permute-start(bf16[256,512]{1,0:T(8,128)(2,1)S(1)} %get-tuple-element.58.first), channel_id=1, source_target_pairs={{0,3},{1,0},{2,1},{3,2},{4,7},{5,4},{6,5},{7,6},{8,11},{9,8},{10,9... | collective-permute-start | bytes 786440 | tf_op jit(solution)/shard_map/ppermute | solution.py:385
  75.5 5.5 %shard_map.194 = (bf16[256,512]{1,0:T(8,128)(2,1)S(1)}, bf16[256,512]{1,0:T(8,128)(2,1)S(1)}, bf16[1,2048,896]{2,1,0:T(8,128)(2,1)S(1)}, bf16[1,2048,896]{2,1,0:T(8,128)(2,1)S(1)}, bf16[1,896,2048]{2,1,0:T(8,128)(2,1)S(1)}) custom-call(bf16[256,512]{1,0:T(8,128)(2,1)S(1)} %get-tuple-element.58.first, bf16[256,512]{1,0:T(8,128)(2,1)S(1)} %get-tuple-element.57.last, ...), custom_call_target="tpu_custom_call" | custom-call | flops 1409286144 | tf_op jit(solution)/shard_map/pallas_call | solution.py:360
  80.9 0.0 collective-permute-done.8.refs_1_
  80.9 0.0 collective-permute-done.6.refs_0_
  81.0 2.4 %shard_map.196 = (bf16[256,512]{1,0:T(8,128)(2,1)S(1)}, bf16[256,512]{1,0:T(8,128)(2,1)S(1)}) custom-call(bf16[256,512]{1,0:T(8,128)(2,1)S(1)} %collective-permute-done.6.refs_0_, bf16[256,512]{1,0:T(8,128)(2,1)S(1)} %collective-permute-done.8.refs_1_, bf16[1,2048,896]{2,1,0:T(8,128)(2,1)S(1)} %get-tuple-element.45.refs_2_, ...), custom_call_target="tpu_custom_call" | custom-call | flops 1409286144 | tf_op jit(solution)/shard_map/pallas_call | solution.py:360
  83.4 0.1 collective-permute-start.9
  83.5 2.4 %shard_map.197 = (bf16[256,512]{1,0:T(8,128)(2,1)S(1)}, bf16[256,512]{1,0:T(8,128)(2,1)S(1)}) custom-call(bf16[256,512]{1,0:T(8,128)(2,1)S(1)} %collective-permute-done.5.refs_0_, bf16[256,512]{1,0:T(8,128)(2,1)S(1)} %collective-permute-done.7.refs_1_, bf16[1,2048,896]{2,1,0:T(8,128)(2,1)S(1)} %get-tuple-element.45.refs_2_, ...), custom_call_target="tpu_custom_call" | custom-call | flops 1409286144 | tf_op jit(solution)/shard_map/pallas_call | solution.py:360
  85.9 2.7 %collective-permute-start.11 = (bf16[256,512]{1,0:T(8,128)(2,1)S(1)}, bf16[256,512]{1,0:T(8,128)(2,1)S(1)}, u32[]{:S(2)}, u32[]{:S(2)}) collective-permute-start(bf16[256,512]{1,0:T(8,128)(2,1)S(1)} %get-tuple-element.50), channel_id=1, source_target_pairs={{0,3},{1,0},{2,1},{3,2},{4,7},{5,4},{6,5},{7,6},{8,11},{9,8},{10,9... | collective-permute-start | bytes 786440 | tf_op jit(solution)/shard_map/ppermute | solution.py:385
  88.6 0.0 collective-permute-start.12
  88.6 0.0 collective-permute-done.3.refs_0_
  88.6 2.7 %collective-permute-start.13 = (bf16[256,512]{1,0:T(8,128)(2,1)S(1)}, bf16[256,512]{1,0:T(8,128)(2,1)S(1)}, u32[]{:S(2)}, u32[]{:S(2)}) collective-permute-start(bf16[256,512]{1,0:T(8,128)(2,1)S(1)} %get-tuple-element.54), channel_id=1, source_target_pairs={{0,3},{1,0},{2,1},{3,2},{4,7},{5,4},{6,5},{7,6},{8,11},{9,8},{10,9... | collective-permute-start | bytes 786440 | tf_op jit(solution)/shard_map/ppermute | solution.py:385
  91.3 0.0 collective-permute-done.4.refs_1_
  91.3 2.4 %shard_map.195 = (bf16[256,512]{1,0:T(8,128)(2,1)S(1)}, bf16[256,512]{1,0:T(8,128)(2,1)S(1)}) custom-call(bf16[256,512]{1,0:T(8,128)(2,1)S(1)} %collective-permute-done.3.refs_0_, bf16[256,512]{1,0:T(8,128)(2,1)S(1)} %collective-permute-done.4.refs_1_, bf16[1,2048,896]{2,1,0:T(8,128)(2,1)S(1)} %get-tuple-element.45.refs_2_, ...), custom_call_target="tpu_custom_call" | custom-call | flops 1409286144 | tf_op jit(solution)/shard_map/pallas_call | solution.py:360
  93.7 0.0 copy-start.5
  93.7 0.0 collective-permute-done.9
  93.7 0.1 add_convert_fusion.1
  93.8 0.1 collective-permute-start.10
  93.9 2.0 %collective-permute-done.13 = bf16[256,512]{1,0:T(8,128)(2,1)S(1)} collective-permute-done((bf16[256,512]{1,0:T(8,128)(2,1)S(1)}, bf16[256,512]{1,0:T(8,128)(2,1)S(1)}, u32[]{:S(2)}, u32[]{:S(2)}) %collective-permute-start.13) | collective-permute-done | bytes 262176 | tf_op jit(solution)/shard_map/ppermute | solution.py:385
  95.9 0.1 add_convert_fusion
  96.0 3.5 %collective-permute-start.14 = (bf16[256,512]{1,0:T(8,128)(2,1)S(1)}, bf16[256,512]{1,0:T(8,128)(2,1)S(1)}, u32[]{:S(2)}, u32[]{:S(2)}) collective-permute-start(bf16[256,512]{1,0:T(8,128)(2,1)S(1)} %add_convert_fusion), channel_id=1, source_target_pairs={{0,3},{1,0},{2,1},{3,2},{4,7},{5,4},{6,5},{7,6},{8,11},{9,8},{10,9... | collective-permute-start | bytes 786440 | tf_op jit(solution)/shard_map/ppermute | solution.py:385
  99.4 0.0 collective-permute-done.11.refs_2_
  99.4 0.0 collective-permute-done.12.refs_4_
  99.5 3.1 %collective-permute-done.10.refs_1_ = bf16[256,512]{1,0:T(8,128)(2,1)S(1)} collective-permute-done((bf16[256,512]{1,0:T(8,128)(2,1)S(1)}, bf16[256,512]{1,0:T(8,128)(2,1)S(1)}, u32[]{:S(2)}, u32[]{:S(2)}) %collective-permute-start.10) | collective-permute-done | bytes 262176 | tf_op jit(solution)/shard_map/ppermute | solution.py:385
  102.6 0.6 collective-permute-done.14.refs_5_
  103.2 0.2 shard_map.198
  103.4 28.1 %all_to_all.17 = bf16[64,8,512]{2,1,0:T(8,128)(2,1)S(1)} all-to-all(bf16[64,8,512]{2,1,0:T(8,128)(2,1)S(1)} %bitcast.17), channel_id=1, replica_groups=mesh['sp'=64,'tp'=4] {'sp'}, dimensions={0} | all-to-all | bytes 1048576 | tf_op jit(solution)/shard_map/all_to_all | solution.py:380
  131.5 1.1 shard_map.199
  (16 shorter events, 0.1 us)
Async XLA Ops:
  0.0 27.7 %copy-start.2 = (bf16[128,128]{1,0:T(8,128)(2,1)S(1)}, bf16[128,128]{1,0:T(8,128)(2,1)}, u32[]{:S(2)}) copy-start(bf16[128,128]{1,0:T(8,128)(2,1)} %inputs.3) | copy-start | bytes 98308
  0.0 27.7 %copy-start = (bf16[128,2048]{1,0:T(8,128)(2,1)S(1)}, bf16[128,2048]{1,0:T(8,128)(2,1)}, u32[]{:S(2)}) copy-start(bf16[128,2048]{1,0:T(8,128)(2,1)} %out_weight.1) | copy-start | bytes 1572868
  0.0 27.7 %copy-start.8 = (f32[128]{0:T(128)S(1)}, f32[128]{0:T(128)}, u32[]{:S(2)}) copy-start(f32[128]{0:T(128)} %param.29) | copy-start | bytes 1540
  0.0 34.2 %copy-start.6 = (s32[128,2]{0,1:T(2,128)S(1)}, s32[128,2]{0,1:T(2,128)}, u32[]{:S(2)}) copy-start(s32[128,2]{0,1:T(2,128)} %param.35) | copy-start | bytes 3076
  0.0 34.2 %copy-start.7 = (f32[128,2]{0,1:T(2,128)S(1)}, f32[128,2]{0,1:T(2,128)}, u32[]{:S(2)}) copy-start(f32[128,2]{0,1:T(2,128)} %param.36) | copy-start | bytes 3076
  0.0 39.1 %copy-start.1 = (bf16[32,2048]{1,0:T(8,128)(2,1)S(1)}, bf16[32,2048]{1,0:T(8,128)(2,1)}, u32[]{:S(2)}) copy-start(bf16[32,2048]{1,0:T(8,128)(2,1)} %residual.1) | copy-start | bytes 393220
  0.0 39.1 %copy-start.3 = (f32[2048]{0:T(1024)S(1)}, f32[2048]{0:T(1024)}, u32[]{:S(2)}) copy-start(f32[2048]{0:T(1024)} %param.32) | copy-start | bytes 24580
  0.0 39.1 %copy-start.4 = (f32[2048]{0:T(1024)S(1)}, f32[2048]{0:T(1024)}, u32[]{:S(2)}) copy-start(f32[2048]{0:T(1024)} %param.33) | copy-start | bytes 24580
  29.1 6.1 %collective-permute-start = (bf16[32,2048]{1,0:T(8,128)(2,1)S(1)}, bf16[32,2048]{1,0:T(8,128)(2,1)S(1)}, u32[]{:S(2)}, u32[]{:S(2)}) collective-permute-start(bf16[32,2048]{1,0:T(8,128)(2,1)S(1)} %get-tuple-element.39), channel_id=1, source_target_pairs={{0,1},{1,2},{2,3},{3,0},{4,5},{5,6},{6,7},{7,4},{8,9},{9,10},{10,1... | collective-permute-start | bytes 393224 | tf_op jit(solution)/shard_map/ppermute | solution.py:385
  30.5 8.6 %collective-permute-start.1 = (bf16[32,2048]{1,0:T(8,128)(2,1)S(1)}, bf16[32,2048]{1,0:T(8,128)(2,1)S(1)}, u32[]{:S(2)}, u32[]{:S(2)}) collective-permute-start(bf16[32,2048]{1,0:T(8,128)(2,1)S(1)} %get-tuple-element.40), channel_id=1, source_target_pairs={{0,2},{1,3},{2,0},{3,1},{4,6},{5,7},{6,4},{7,5},{8,10},{9,11},{10,... | collective-permute-start | bytes 393224 | tf_op jit(solution)/shard_map/ppermute | solution.py:385
  33.1 6.0 %collective-permute-start.2 = (bf16[32,2048]{1,0:T(8,128)(2,1)S(1)}, bf16[32,2048]{1,0:T(8,128)(2,1)S(1)}, u32[]{:S(2)}, u32[]{:S(2)}) collective-permute-start(bf16[32,2048]{1,0:T(8,128)(2,1)S(1)} %get-tuple-element.41), channel_id=1, source_target_pairs={{0,3},{1,0},{2,1},{3,2},{4,7},{5,4},{6,5},{7,6},{8,11},{9,8},{10,9... | collective-permute-start | bytes 393224 | tf_op jit(solution)/shard_map/ppermute | solution.py:385
  62.1 7.5 %collective-permute-start.7 = (bf16[256,512]{1,0:T(8,128)(2,1)S(1)}, bf16[256,512]{1,0:T(8,128)(2,1)S(1)}, u32[]{:S(2)}, u32[]{:S(2)}) collective-permute-start(bf16[256,512]{1,0:T(8,128)(2,1)S(1)} %get-tuple-element.57.last), channel_id=1, source_target_pairs={{0,3},{1,0},{2,1},{3,2},{4,7},{5,4},{6,5},{7,6},{8,11},{9,8},{10,9... | collective-permute-start | bytes 786440 | tf_op jit(solution)/shard_map/ppermute | solution.py:385
  64.1 8.7 %collective-permute-start.5 = (bf16[256,512]{1,0:T(8,128)(2,1)S(1)}, bf16[256,512]{1,0:T(8,128)(2,1)S(1)}, u32[]{:S(2)}, u32[]{:S(2)}) collective-permute-start(bf16[256,512]{1,0:T(8,128)(2,1)S(1)} %get-tuple-element.58.first), channel_id=1, source_target_pairs={{0,1},{1,2},{2,3},{3,0},{4,5},{5,6},{6,7},{7,4},{8,9},{9,10},{10,1... | collective-permute-start | bytes 786440 | tf_op jit(solution)/shard_map/ppermute | solution.py:385
  69.7 11.3 %collective-permute-start.8 = (bf16[256,512]{1,0:T(8,128)(2,1)S(1)}, bf16[256,512]{1,0:T(8,128)(2,1)S(1)}, u32[]{:S(2)}, u32[]{:S(2)}) collective-permute-start(bf16[256,512]{1,0:T(8,128)(2,1)S(1)} %collective-permute-done.7.refs_1_), channel_id=1, source_target_pairs={{0,3},{1,0},{2,1},{3,2},{4,7},{5,4},{6,5},{7,6},{8,11},{9,8},{10,9... | collective-permute-start | bytes 786440 | tf_op jit(solution)/shard_map/ppermute | solution.py:385
  72.8 8.2 %collective-permute-start.6 = (bf16[256,512]{1,0:T(8,128)(2,1)S(1)}, bf16[256,512]{1,0:T(8,128)(2,1)S(1)}, u32[]{:S(2)}, u32[]{:S(2)}) collective-permute-start(bf16[256,512]{1,0:T(8,128)(2,1)S(1)} %collective-permute-done.5.refs_0_), channel_id=1, source_target_pairs={{0,1},{1,2},{2,3},{3,0},{4,5},{5,6},{6,7},{7,4},{8,9},{9,10},{10,1... | collective-permute-start | bytes 786440 | tf_op jit(solution)/shard_map/ppermute | solution.py:385
  72.8 15.8 %collective-permute-start.3 = (bf16[256,512]{1,0:T(8,128)(2,1)S(1)}, bf16[256,512]{1,0:T(8,128)(2,1)S(1)}, u32[]{:S(2)}, u32[]{:S(2)}) collective-permute-start(bf16[256,512]{1,0:T(8,128)(2,1)S(1)} %get-tuple-element.57.last), channel_id=1, source_target_pairs={{0,1},{1,2},{2,3},{3,0},{4,5},{5,6},{6,7},{7,4},{8,9},{9,10},{10,1... | collective-permute-start | bytes 786440 | tf_op jit(solution)/shard_map/ppermute | solution.py:385
  72.8 18.5 %collective-permute-start.4 = (bf16[256,512]{1,0:T(8,128)(2,1)S(1)}, bf16[256,512]{1,0:T(8,128)(2,1)S(1)}, u32[]{:S(2)}, u32[]{:S(2)}) collective-permute-start(bf16[256,512]{1,0:T(8,128)(2,1)S(1)} %get-tuple-element.58.first), channel_id=1, source_target_pairs={{0,3},{1,0},{2,1},{3,2},{4,7},{5,4},{6,5},{7,6},{8,11},{9,8},{10,9... | collective-permute-start | bytes 786440 | tf_op jit(solution)/shard_map/ppermute | solution.py:385
  83.4 10.4 %collective-permute-start.9 = (bf16[256,512]{1,0:T(8,128)(2,1)S(1)}, bf16[256,512]{1,0:T(8,128)(2,1)S(1)}, u32[]{:S(2)}, u32[]{:S(2)}) collective-permute-start(bf16[256,512]{1,0:T(8,128)(2,1)S(1)} %get-tuple-element.49), channel_id=1, source_target_pairs={{0,1},{1,2},{2,3},{3,0},{4,5},{5,6},{6,7},{7,4},{8,9},{9,10},{10,1... | collective-permute-start | bytes 786440 | tf_op jit(solution)/shard_map/ppermute | solution.py:385
  85.9 13.6 %collective-permute-start.11 = (bf16[256,512]{1,0:T(8,128)(2,1)S(1)}, bf16[256,512]{1,0:T(8,128)(2,1)S(1)}, u32[]{:S(2)}, u32[]{:S(2)}) collective-permute-start(bf16[256,512]{1,0:T(8,128)(2,1)S(1)} %get-tuple-element.50), channel_id=1, source_target_pairs={{0,3},{1,0},{2,1},{3,2},{4,7},{5,4},{6,5},{7,6},{8,11},{9,8},{10,9... | collective-permute-start | bytes 786440 | tf_op jit(solution)/shard_map/ppermute | solution.py:385
  88.6 10.8 %collective-permute-start.12 = (bf16[256,512]{1,0:T(8,128)(2,1)S(1)}, bf16[256,512]{1,0:T(8,128)(2,1)S(1)}, u32[]{:S(2)}, u32[]{:S(2)}) collective-permute-start(bf16[256,512]{1,0:T(8,128)(2,1)S(1)} %get-tuple-element.52), channel_id=1, source_target_pairs={{0,1},{1,2},{2,3},{3,0},{4,5},{5,6},{6,7},{7,4},{8,9},{9,10},{10,1... | collective-permute-start | bytes 786440 | tf_op jit(solution)/shard_map/ppermute | solution.py:385
  88.6 7.3 %collective-permute-start.13 = (bf16[256,512]{1,0:T(8,128)(2,1)S(1)}, bf16[256,512]{1,0:T(8,128)(2,1)S(1)}, u32[]{:S(2)}, u32[]{:S(2)}) collective-permute-start(bf16[256,512]{1,0:T(8,128)(2,1)S(1)} %get-tuple-element.54), channel_id=1, source_target_pairs={{0,3},{1,0},{2,1},{3,2},{4,7},{5,4},{6,5},{7,6},{8,11},{9,8},{10,9... | collective-permute-start | bytes 786440 | tf_op jit(solution)/shard_map/ppermute | solution.py:385
  93.7 37.8 %copy-start.5 = (f32[2048]{0:T(1024)S(1)}, f32[2048]{0:T(1024)}, u32[]{:S(2)}) copy-start(f32[2048]{0:T(1024)} %param.34) | copy-start | bytes 24580
  93.8 8.8 %collective-permute-start.10 = (bf16[256,512]{1,0:T(8,128)(2,1)S(1)}, bf16[256,512]{1,0:T(8,128)(2,1)S(1)}, u32[]{:S(2)}, u32[]{:S(2)}) collective-permute-start(bf16[256,512]{1,0:T(8,128)(2,1)S(1)} %add_convert_fusion.1), channel_id=1, source_target_pairs={{0,1},{1,2},{2,3},{3,0},{4,5},{5,6},{6,7},{7,4},{8,9},{9,10},{10,1... | collective-permute-start | bytes 786440 | tf_op jit(solution)/shard_map/ppermute | solution.py:385
  96.0 7.2 %collective-permute-start.14 = (bf16[256,512]{1,0:T(8,128)(2,1)S(1)}, bf16[256,512]{1,0:T(8,128)(2,1)S(1)}, u32[]{:S(2)}, u32[]{:S(2)}) collective-permute-start(bf16[256,512]{1,0:T(8,128)(2,1)S(1)} %add_convert_fusion), channel_id=1, source_target_pairs={{0,3},{1,0},{2,1},{3,2},{4,7},{5,4},{6,5},{7,6},{8,11},{9,8},{10,9... | collective-permute-start | bytes 786440 | tf_op jit(solution)/shard_map/ppermute | solution.py:385
